TPU v7x, 256 devices: a whole 4x4x8 slice. The times are simulated.
256 devices in a mesh: st: 64 (over z, y, core), tp: 4 (over x).
Axes of the slice: x: 4, y: 4, z: 8, core: 2. Of those that a mesh axis runs over, the one named last changes fastest.
Arguments:
- tokens: bfloat16 [24576, 2048], P('st', 'tp'), may hold values from -6 to 6
- cotangent: bfloat16 [24576, 1024], P('st', 'tp'), may hold values from -48 to 48
- mix_query: bfloat16 [24576, 1024], P('st', 'tp'), may hold values from -6 to 6
- mix_key: bfloat16 [24576, 1024], P('st', 'tp'), may hold values from -6 to 6
- mix_value: bfloat16 [24576, 1024], P('st', 'tp'), may hold values from -24 to 24
- beta_pre: float32 [8, 24576], P('tp', 'st'), may hold values from -9 to 9
- decay_pre: float32 [8, 24576], P('tp', 'st'), may hold values from -8 to 6
- decay_rate: float32 [8], P('tp'), may hold values from 0.001 to 0.06
- passages: bfloat16 [1024, 64, 2048], P('st'), may hold values from -16 to 16
- passage_ids: int32 [384, 4], P('st'), may hold values from 0 to 1023, as said below
- query_weight: bfloat16 [2048, 1024], P(None, 'tp'), may hold values from -0.125 to 0.125
- key_weight: bfloat16 [2048, 1024], P(None, 'tp'), may hold values from -0.125 to 0.125
- value_weight: bfloat16 [2048, 1024], P(None, 'tp'), may hold values from -0.125 to 0.125
- gate_weight: bfloat16 [4, 2048], P('tp'), may hold values from -0.125 to 0.125
Outputs:
- token_grad: bfloat16 [24576, 2048], P('st', 'tp')
- passage_grad: bfloat16 [1024, 64, 2048], P('st', None, 'tp')
- key_weight_grad: float32 [2048, 1024], P('st', 'tp')
Inputs may be any that keep to these rules, and one draw needn't show every extreme that they name: Passage p is stored on index p // 16 of st. The rows of passage_ids read by one index of st name at most 1 passages stored on any one index of st, and exactly 1 on some.
All inputs are finite; a program needn't handle non-finite values.
Results may differ from a plain program's by a relative error of at most 0.012.
The roundings to bfloat16 on the way count: a program that leaves them out, or rounds other values in their place, can miss the bound.
Values may be sent and summed in bfloat16 or wider, within the bound.
A program may use at most 128 MiB of HBM per device.

v0:
```python
import jax
import jax.numpy as jnp
from jax import lax
from jax.sharding import Mesh
from jax.sharding import PartitionSpec as P

SPAN = 64
ST = ("st_0", "st_1", "st_2")


NORM_FLOOR = 1.0
SCORE_GAIN = 4.0
CONTRACT_LAST = (((1,), (1,)), ((), ()))
CONTRACT_FIRST = (((0,), (0,)), ((), ()))


def joined_along(parts, dim):
    lengths = list(parts.shape[1:])
    lengths[dim] *= parts.shape[0]
    return jnp.moveaxis(parts, 0, dim).reshape(lengths)


def copy_for_each(shard, axis):
    copies = jnp.broadcast_to(shard, (lax.axis_size(axis), *shard.shape))
    return lax.all_to_all(copies, axis, split_axis=0, concat_axis=0, tiled=True)


def gather_directly(shard, axis, dim):
    return joined_along(copy_for_each(shard, axis), dim)


def in_blocks(shard, dim, devices):
    before, after = (shard.shape[:dim], shard.shape[dim + 1 :])
    return jnp.moveaxis(shard.reshape(*before, devices, -1, *after), dim, 0)


def sum_at_owner(shard, axis, dim):
    parts = in_blocks(shard, dim, lax.axis_size(axis))
    arrived = lax.all_to_all(parts, axis, split_axis=0, concat_axis=0, tiled=True)
    return arrived.astype(jnp.float32).sum(axis=0)


def sum_by_axis(shard, axes, dim):
    for axis in axes:
        shard = lax.psum_scatter(shard, axis, scatter_dimension=dim, tiled=True)
    return shard


def neumann_inverse(strict_part):
    span_size = strict_part.shape[-1]
    unit_eye = jnp.eye(span_size, dtype=jnp.float32)
    running = unit_eye - strict_part
    power_term = strict_part
    for _ in range(span_size.bit_length() - 2):
        power_term = jnp.einsum("...ij,...jk->...ik", power_term, power_term)
        running = jnp.einsum("...ij,...jk->...ik", running, unit_eye + power_term)
    return running


def delta_mixer(queries, keys_in, values_in, strength, log_decay):
    heads_n, length, key_dim = queries.shape
    blocks_n = length // SPAN

    def to_blocks(tensor):
        return tensor.reshape(heads_n, blocks_n, SPAN, *tensor.shape[2:])

    queries, keys_in, values_in = (to_blocks(queries), to_blocks(keys_in), to_blocks(values_in))
    strength, log_decay = (to_blocks(strength), to_blocks(log_decay))
    cumulative = jnp.cumsum(log_decay, axis=-1)
    position = jnp.arange(SPAN)
    inclusive = position[:, None] >= position[None, :]
    strictly = position[:, None] > position[None, :]
    spread = jnp.where(inclusive, cumulative[..., :, None] - cumulative[..., None, :], -jnp.inf)
    decay_map = jnp.exp(spread)
    key_gram = jnp.einsum("hncd,hnmd->hncm", keys_in, keys_in)
    strict_part = jnp.where(strictly, strength[..., :, None] * key_gram * decay_map, 0.0)
    inverse = neumann_inverse(strict_part)
    fresh_vals = jnp.einsum("hncm,hnme->hnce", inverse, values_in * strength[..., None])
    correction = jnp.einsum(
        "hncm,hnmd->hncd", inverse, keys_in * (strength * jnp.exp(cumulative))[..., None]
    )
    attend_map = jnp.where(
        inclusive, jnp.einsum("hncd,hnmd->hncm", queries, keys_in) * decay_map, 0.0
    )
    query_dec = queries * jnp.exp(cumulative)[..., None]
    key_dec = keys_in * jnp.exp(cumulative[..., -1:] - cumulative)[..., None]
    carry_decay = jnp.exp(cumulative[..., -1])

    def advance(memory_state, inputs):
        fresh_blk, correct_blk, attend_blk, query_blk, key_blk, decay_blk = inputs
        new_values = fresh_blk - jnp.einsum("hcd,hde->hce", correct_blk, memory_state)
        output = jnp.einsum("hcd,hde->hce", query_blk, memory_state) + jnp.einsum(
            "hcm,hme->hce", attend_blk, new_values
        )
        memory_state = memory_state * decay_blk[:, None, None] + jnp.einsum(
            "hcd,hce->hde", key_blk, new_values
        )
        return (memory_state, output)

    stacked = tuple(
        (
            jnp.moveaxis(tensor, 1, 0)
            for tensor in (fresh_vals, correction, attend_map, query_dec, key_dec, carry_decay)
        )
    )
    initial = jnp.zeros((heads_n, key_dim, values_in.shape[-1]), jnp.float32)
    _, outputs = lax.scan(advance, initial, stacked)
    return jnp.transpose(outputs, (1, 0, 2, 3)).reshape(heads_n, length, -1)


def mixer_output(query_raw, key_raw, value_raw, beta_raw, decay_raw, rate_vals):
    length = query_raw.shape[0]
    heads_n = beta_raw.shape[0]

    def heads_first(matrix):
        return jnp.transpose(matrix.astype(jnp.float32).reshape(length, heads_n, -1), (1, 0, 2))

    queries = heads_first(query_raw)
    keys_in = heads_first(key_raw)
    values_in = heads_first(value_raw)
    queries = (
        queries
        * lax.rsqrt(jnp.sum(queries * queries, axis=-1, keepdims=True) + NORM_FLOOR)
        * queries.shape[-1] ** (-0.5)
    )
    keys_in = keys_in * lax.rsqrt(jnp.sum(keys_in * keys_in, axis=-1, keepdims=True) + NORM_FLOOR)
    strength = jax.nn.sigmoid(beta_raw)
    log_decay = -rate_vals[:, None] * jax.nn.softplus(decay_raw)
    mixer_out = delta_mixer(queries, keys_in, values_in, strength, log_decay)
    return jnp.transpose(mixer_out, (1, 0, 2)).reshape(length, -1)


def request_slots(id_rows, pass_count):
    owners = id_rows // pass_count
    local_idx = id_rows % pass_count
    req_count = id_rows.shape[-1]
    req_order = jnp.arange(req_count, dtype=jnp.int32)
    earlier = (owners[..., :, None] == owners[..., None, :]) & (
        req_order[None, :] < req_order[:, None]
    )
    ranks = jnp.sum(earlier.astype(jnp.int32), axis=-1, dtype=jnp.int32)
    return (owners, local_idx, ranks)


def body(
    tokens,
    cotangent,
    mix_query,
    mix_key,
    mix_value,
    beta_pre,
    decay_pre,
    decay_rate,
    passages,
    passage_ids,
    query_weight,
    key_weight,
    value_weight,
    gate_weight,
):
    tok_rows = tokens.shape[0]
    model_width = query_weight.shape[0]
    head_dim = query_weight.shape[1]
    pass_local = passages.shape[0]
    span_rows = passages.shape[1]
    blocks_n = passage_ids.shape[0]
    per_block = passage_ids.shape[1]
    block_rows = tok_rows // blocks_n
    req_count = blocks_n * per_block
    st_count = lax.axis_size(ST)
    my_owner = lax.axis_index(ST)
    cap_count = max(1, req_count // st_count)
    slot_total = st_count * cap_count
    score_scale = SCORE_GAIN * head_dim ** (-0.5)
    req_order = jnp.arange(req_count, dtype=jnp.int32)
    every_id = gather_directly(passage_ids, ST, 0).reshape(st_count, req_count)
    all_owner, all_local, all_rank = request_slots(every_id, pass_local)
    cap_iota = jnp.arange(cap_count, dtype=jnp.int32)
    wanted = (all_owner == my_owner)[:, None, :] & (all_rank[:, None, :] == cap_iota[None, :, None])
    slot_used = jnp.any(wanted, axis=-1)
    slot_local = jnp.sum(jnp.where(wanted, all_local[:, None, :], 0), axis=-1, dtype=jnp.int32)
    flat_rows = passages.reshape(pass_local * span_rows, model_width)
    key_low = lax.optimization_barrier(
        jnp.dot(flat_rows, key_weight, preferred_element_type=jnp.float32).astype(jnp.bfloat16)
    )
    value_all = jnp.dot(flat_rows, value_weight, preferred_element_type=jnp.float32).astype(
        jnp.bfloat16
    )
    key_float = key_low.astype(jnp.float32)
    key_scale = lax.rsqrt(jnp.mean(key_float * key_float, axis=-1, keepdims=True) + NORM_FLOOR)
    key_hat = (key_float * key_scale).astype(jnp.bfloat16)
    packed = jnp.concatenate([key_hat, value_all], axis=-1).reshape(
        pass_local, span_rows, 2 * head_dim
    )
    send_rows = jnp.where(
        slot_used[:, :, None, None], packed[slot_local], jnp.zeros((), jnp.bfloat16)
    )
    arrived = lax.all_to_all(send_rows, ST, split_axis=0, concat_axis=0, tiled=True).reshape(
        slot_total, span_rows, 2 * head_dim
    )
    shard_piece = lax.all_gather(tokens, "tp", axis=1, tiled=True)
    query_acc = jnp.dot(shard_piece, query_weight, preferred_element_type=jnp.float32)
    gate_acc = lax.dot_general(
        shard_piece, gate_weight, CONTRACT_LAST, preferred_element_type=jnp.float32
    )
    query_low = lax.optimization_barrier(query_acc.astype(jnp.bfloat16))
    query_float = query_low.astype(jnp.float32)
    query_scale = lax.rsqrt(
        jnp.mean(query_float * query_float, axis=-1, keepdims=True) + NORM_FLOOR
    )
    query_hat = (query_float * query_scale).astype(jnp.bfloat16)
    gate_open = jax.nn.sigmoid(gate_acc[:, 0])
    mixer_out = mixer_output(mix_query, mix_key, mix_value, beta_pre, decay_pre, decay_rate)
    own_owner, own_local, own_rank = request_slots(passage_ids.reshape(req_count), pass_local)
    slot_of = own_owner * cap_count + own_rank
    mine_rows = arrived[slot_of]
    key_rows = mine_rows[:, :, :head_dim].reshape(blocks_n, per_block * span_rows, head_dim)
    value_rows = mine_rows[:, :, head_dim:].reshape(blocks_n, per_block * span_rows, head_dim)
    query_blocks = query_hat.reshape(blocks_n, block_rows, head_dim)
    scores = (
        jnp.einsum("bid,bjd->bij", query_blocks, key_rows, preferred_element_type=jnp.float32)
        * score_scale
    )
    exp_scores = jnp.exp(scores)
    attn_probs = exp_scores / jnp.sum(exp_scores, axis=-1, keepdims=True)
    probs_low = attn_probs.astype(jnp.bfloat16)
    retrieved = jnp.einsum(
        "bij,bjd->bid", probs_low, value_rows, preferred_element_type=jnp.float32
    ).reshape(tok_rows, head_dim)
    grad_out = cotangent.astype(jnp.float32)
    grad_ret = (gate_open[:, None] * grad_out).astype(jnp.bfloat16)
    gate_grad = jnp.sum(grad_out * (retrieved - mixer_out), axis=-1) * gate_open * (1.0 - gate_open)
    grad_blocks = grad_ret.reshape(blocks_n, block_rows, head_dim)
    grad_probs = jnp.einsum(
        "bid,bjd->bij", grad_blocks, value_rows, preferred_element_type=jnp.float32
    )
    score_grad = (
        attn_probs * (grad_probs - jnp.sum(grad_probs * attn_probs, axis=-1, keepdims=True))
    ).astype(jnp.bfloat16)
    slot_match = slot_of[None, :] == jnp.arange(slot_total, dtype=jnp.int32)[:, None]
    slot_filled = jnp.any(slot_match, axis=-1)
    slot_req = jnp.sum(jnp.where(slot_match, req_order[None, :], 0), axis=-1, dtype=jnp.int32)
    key_term = (
        score_scale
        * jnp.einsum("bij,bid->bjd", score_grad, query_blocks, preferred_element_type=jnp.float32)
    ).astype(jnp.bfloat16)
    value_term = jnp.einsum(
        "bij,bid->bjd", probs_low, grad_blocks, preferred_element_type=jnp.float32
    ).astype(jnp.bfloat16)
    reply_rows = jnp.concatenate([key_term, value_term], axis=-1).reshape(
        req_count, span_rows, 2 * head_dim
    )
    reply_slots = jnp.where(
        slot_filled[:, None, None], reply_rows[slot_req], jnp.zeros((), jnp.bfloat16)
    ).reshape(st_count, cap_count, span_rows, 2 * head_dim)
    reply_back = lax.all_to_all(reply_slots, ST, split_axis=0, concat_axis=0, tiled=True).astype(
        jnp.float32
    )
    key_part = reply_back[..., :head_dim]
    value_part = reply_back[..., head_dim:]
    qhat_grad = score_scale * jnp.einsum(
        "bij,bjd->bid", score_grad, key_rows, preferred_element_type=jnp.float32
    ).reshape(tok_rows, head_dim)
    query_grad = (
        query_scale * qhat_grad
        - query_scale**3 * query_float * jnp.mean(query_float * qhat_grad, axis=-1, keepdims=True)
    ).astype(jnp.bfloat16)
    token_term = (
        lax.dot_general(query_grad, query_weight, CONTRACT_LAST, preferred_element_type=jnp.float32)
        + gate_grad[:, None] * gate_weight[0].astype(jnp.float32)[None, :]
    )
    token_grad = sum_at_owner(token_term.astype(jnp.bfloat16), "tp", 1).astype(jnp.bfloat16)
    pass_iota = jnp.arange(pass_local, dtype=jnp.int32)
    onehot = (
        (slot_local.reshape(slot_total)[None, :] == pass_iota[:, None])
        & slot_used.reshape(slot_total)[None, :]
    ).astype(jnp.float32)
    key_grad_hat = jnp.dot(onehot, key_part.reshape(slot_total, span_rows * head_dim)).reshape(
        pass_local * span_rows, head_dim
    )
    value_grad_sum = jnp.dot(onehot, value_part.reshape(slot_total, span_rows * head_dim)).reshape(
        pass_local * span_rows, head_dim
    )
    key_grad = (
        key_scale * key_grad_hat
        - key_scale**3 * key_float * jnp.mean(key_float * key_grad_hat, axis=-1, keepdims=True)
    ).astype(jnp.bfloat16)
    value_grad_low = value_grad_sum.astype(jnp.bfloat16)
    row_term = lax.dot_general(
        key_grad, key_weight, CONTRACT_LAST, preferred_element_type=jnp.float32
    ) + lax.dot_general(
        value_grad_low, value_weight, CONTRACT_LAST, preferred_element_type=jnp.float32
    )
    passage_grad = sum_at_owner(
        row_term.reshape(pass_local, span_rows, model_width).astype(jnp.bfloat16), "tp", 2
    ).astype(jnp.bfloat16)
    weight_term = lax.dot_general(
        flat_rows, key_grad, CONTRACT_FIRST, preferred_element_type=jnp.float32
    )
    key_weight_grad = sum_by_axis(weight_term, ST, 0)
    return (token_grad, passage_grad, key_weight_grad)


def solution(mesh):
    torus = Mesh(mesh.devices.reshape(8, 4, 2, mesh.shape["tp"]), ("st_0", "st_1", "st_2", "tp"))
    return jax.shard_map(
        body,
        mesh=torus,
        in_specs=(
            P(ST, "tp"),
            P(ST, "tp"),
            P(ST, "tp"),
            P(ST, "tp"),
            P(ST, "tp"),
            P("tp", ST),
            P("tp", ST),
            P("tp"),
            P(ST, None, None),
            P(ST, None),
            P(None, "tp"),
            P(None, "tp"),
            P(None, "tp"),
            P("tp", None),
        ),
        out_specs=(P(ST, "tp"), P(ST, None, "tp"), P(ST, "tp")),
        check_vma=False,
    )
```

profile of v0, /device:TPU:1, one launch (start us, length us, event | category | flops | bytes accessed | tf_op | source)
XLA Modules:
  0.0 397.8 jit_solution(1694725914471764700)
XLA Ops:
  9.3 13.3 %all-to-all-start = ((s32[64,6,4]{1,2,0:T(4,128)}), s32[64,6,4]{1,2,0:T(4,128)}, u32[]{:S(2)}, u32[]{:S(2)}) async-start(s32[64,6,4]{1,2,0:T(4,128)} %broadcast_in_dim.61), calls=%async_computation | async-start | bytes 262144 | tf_op jit(solution)/shard_map/all_to_all | solution.py:25
  34.0 3.9 convolution_convert_fusion.2
  48.2 2.8 gather_fusion
  51.0 4.5 %fusion.25 = bf16[64,1,64,512]{3,2,1,0:T(8,128)(2,1)} fusion(bf16[64,64,512]{2,1,0:T(8,128)(2,1)} %gather_fusion, pred[64]{0:T(512)(128)(4,1)S(1)} %copy-done.18), kind=kLoop, calls=%fused_computation.36 | loop fusion | flops 2097152 | bytes 8388672 | tf_op jit(solution)/shard_map/jit(_where)/select_n | solution.py:195
  55.5 10.5 %all-to-all-start.1 = ((bf16[64,1,64,512]{3,2,1,0:T(8,128)(2,1)}), bf16[64,1,64,512]{3,2,1,0:T(8,128)(2,1)}, u32[]{:S(2)}, u32[]{:S(2)}) async-start(bf16[64,1,64,512]{3,2,1,0:T(8,128)(2,1)} %fusion.25), calls=%async_computation.1 | async-start | bytes 8388608 | tf_op jit(solution)/shard_map/all_to_all | solution.py:198
  66.0 26.3 %while.13 = (s32[]{:T(128)}, f32[2,128,128]{2,1,0:T(8,128)S(1)}, f32[6,2,64,128]{3,2,0,1:T(8,128)S(1)}, f32[6,2]{1,0:T(8,128)}, bf16[6,2,64,128]{3,2,0,1:T(8,128...) while((s32[]{:T(128)}, f32[2,128,128]{2,1,0:T(8,128)S(1)}, ...), condition=%wide.region_13.14_spmd.clone, body=%wide.region_12.13_spmd.clone.sunk | while | flops 14893059 | bytes 1018532 | solution.py:107
  99.6 61.1 %all-to-all-done.1 = bf16[64,1,64,512]{3,2,1,0:T(8,128)(2,1)} async-done(((bf16[64,1,64,512]{3,2,1,0:T(8,128)(2,1)}), bf16[64,1,64,512]{3,2,1,0:T(8,128)(2,1)}, u32[]{:S(2)}, u32[]{:S(2)}) %all-to-all-start.1) | async-done | bytes 4194336 | tf_op jit(solution)/shard_map/all_to_all | solution.py:198
  160.7 3.0 gather_fusion.1
  172.2 2.6 convolution_convert_fusion.1
  180.5 2.9 gather_fusion.2
  183.4 4.5 %fusion.24 = bf16[64,1,64,512]{3,2,1,0:T(8,128)(2,1)} fusion(bf16[64,64,512]{2,1,0:T(8,128)(2,1)} %gather_fusion.2, pred[64]{0:T(512)(128)(4,1)S(1)} %copy-done.26), kind=kLoop, calls=%fused_computation.34 | loop fusion | flops 2097152 | bytes 8388672 | tf_op jit(solution)/shard_map/jit(_where)/select_n | solution.py:253
  187.9 7.3 %all-to-all-start.3 = ((bf16[64,1,64,512]{3,2,1,0:T(8,128)(2,1)}), bf16[64,1,64,512]{3,2,1,0:T(8,128)(2,1)}, u32[]{:S(2)}, u32[]{:S(2)}) async-start(bf16[64,1,64,512]{3,2,1,0:T(8,128)(2,1)} %fusion.24), calls=%async_computation.3 | async-start | bytes 8388608 | tf_op jit(solution)/shard_map/all_to_all | solution.py:256
  196.0 94.1 %all-to-all-done.3 = bf16[64,1,64,512]{3,2,1,0:T(8,128)(2,1)} async-done(((bf16[64,1,64,512]{3,2,1,0:T(8,128)(2,1)}), bf16[64,1,64,512]{3,2,1,0:T(8,128)(2,1)}, u32[]{:S(2)}, u32[]{:S(2)}) %all-to-all-start.3) | async-done | bytes 4194336 | tf_op jit(solution)/shard_map/all_to_all | solution.py:256
  290.1 4.1 %fusion.106 = (bf16[64,1,64,256]{3,2,1,0:T(8,128)(2,1)}, bf16[64,1,64,256]{3,2,1,0:T(8,128)(2,1)S(1)}) fusion(bf16[64,1,64,512]{3,2,1,0:T(8,128)(2,1)} %all-to-all-done.3), kind=kLoop, calls=%fused_computation.199 | loop fusion | bytes 8388608 | tf_op jit(solution)/shard_map/slice | solution.py:260
  298.5 5.0 %convolution_bitcast_fusion = f32[2048,256]{0,1:T(8,128)} fusion(bf16[1024,2048]{1,0:T(8,128)(2,1)} %bitcast.234, bf16[1024,256]{1,0:T(8,128)(2,1)S(1)} %convolution_convert_fusion.3, f32[1024,256]{1,0:T(8,128)S(1)} %reshape.488, f32[1024]{0:T(1024)S(1)} %broadcast_multiply_fusion, f32[1024]{0:T(1024)S(1)} %get-tuple-element.194, ...), kind=kOutput, calls=%fused_computation.39 | convolution fusion | flops 1075314688 | bytes 7876608 | tf_op jit(solution)/shard_map/dot_general | solution.py:297
  306.8 4.6 %all-to-all-start.2 = ((bf16[4,384,512]{2,1,0:T(8,128)(2,1)}), bf16[4,384,512]{2,1,0:T(8,128)(2,1)}, u32[]{:S(2)}, u32[]{:S(2)}) async-start(bf16[4,384,512]{2,1,0:T(8,128)(2,1)} %bitcast.232), calls=%async_computation.2 | async-start | bytes 3145728 | tf_op jit(solution)/shard_map/all_to_all | solution.py:39
  311.4 3.0 copy.213
  318.8 3.3 add_convert_fusion
  322.1 7.9 %convert_element_type.117 = bf16[16,64,4,512]{3,2,1,0:T(4,128)(2,1)} reshape(bf16[1024,2048]{1,0:T(8,128)(2,1)} %add_convert_fusion) | data formatting | bytes 8388608 | tf_op jit(solution)/shard_map/convert_element_type | solution.py:295
  329.9 5.2 %copy.216 = bf16[16,64,4,512]{3,1,0,2:T(8,128)(2,1)} copy(bf16[16,64,4,512]{3,2,1,0:T(4,128)(2,1)} %convert_element_type.117) | data formatting | bytes 8388608 | tf_op jit(solution)/shard_map/convert_element_type | solution.py:295
  335.1 4.8 %all-to-all-start.4 = ((bf16[4,16,64,512]{3,2,1,0:T(8,128)(2,1)}), bf16[4,16,64,512]{3,2,1,0:T(8,128)(2,1)}, u32[]{:S(2)}, u32[]{:S(2)}) async-start(bf16[4,16,64,512]{3,2,1,0:T(8,128)(2,1)} %bitcast.221), calls=%async_computation.4 | async-start | bytes 8388608 | tf_op jit(solution)/shard_map/all_to_all | solution.py:39
  341.9 25.6 %reduce-scatter.10.cloned.1.call-done = f32[64,256]{1,0:T(8,128)} async-done(((f32[256,256]{1,0:T(8,128)}), f32[64,256]{1,0:T(8,128)}) %reduce-scatter.10.cloned.1.call-update) | async-done | bytes 65552
  370.0 17.1 %all-to-all-done.4 = bf16[4,16,64,512]{3,2,1,0:T(8,128)(2,1)} async-done(((bf16[4,16,64,512]{3,2,1,0:T(8,128)(2,1)}), bf16[4,16,64,512]{3,2,1,0:T(8,128)(2,1)}, u32[]{:S(2)}, u32[]{:S(2)}) %all-to-all-start.4) | async-done | bytes 4194336 | tf_op jit(solution)/shard_map/all_to_all | solution.py:39
  387.1 4.2 %reduce_sum.164 = bf16[16,64,512]{2,1,0:T(8,128)(2,1)} reduce(bf16[4,16,64,512]{3,2,1,0:T(8,128)(2,1)} %all-to-all-done.4, bf16[]{:T(256)} %constant.112.clone.1), dimensions={0}, to_apply=%region_19.20 | reduce | flops 1572864 | bytes 5242882 | tf_op jit(solution)/shard_map/reduce_sum | solution.py:40
  (199 shorter events, 88.0 us)
Async XLA Ops:
  7.2 30.8 %copy-start = (bf16[2048,256]{1,0:T(8,128)(2,1)S(1)}, bf16[2048,256]{1,0:T(8,128)(2,1)}, u32[]{:S(2)}) copy-start(bf16[2048,256]{1,0:T(8,128)(2,1)} %param.27) | copy-start | bytes 3145732
  7.2 88.6 %all-gather.2.cloned.1.call-start = ((), (), s32[]{:S(2)}) async-start(), calls=%async_computation.8 | async-start | bytes 1966080 | tf_op jit(solution)/shard_map/all_gather | solution.py:201
  9.3 33.9 %all-to-all-start = ((s32[64,6,4]{1,2,0:T(4,128)}), s32[64,6,4]{1,2,0:T(4,128)}, u32[]{:S(2)}, u32[]{:S(2)}) async-start(s32[64,6,4]{1,2,0:T(4,128)} %broadcast_in_dim.61), calls=%async_computation | async-start | bytes 262144 | tf_op jit(solution)/shard_map/all_to_all | solution.py:25
  22.6 7.4 %copy-start.12 = (pred[64,64]{1,0:T(8,128)(4,1)}, pred[64,64]{1,0:T(8,128)(4,1)S(1)}, u32[]{:S(2)}) copy-start(pred[64,64]{1,0:T(8,128)(4,1)S(1)} %get-tuple-element.203) | copy-start | bytes 12292
  34.0 4.0 copy-start.3
  48.2 2.8 copy-start.18
  55.5 105.2 %all-to-all-start.1 = ((bf16[64,1,64,512]{3,2,1,0:T(8,128)(2,1)}), bf16[64,1,64,512]{3,2,1,0:T(8,128)(2,1)}, u32[]{:S(2)}, u32[]{:S(2)}) async-start(bf16[64,1,64,512]{3,2,1,0:T(8,128)(2,1)} %fusion.25), calls=%async_computation.1 | async-start | bytes 8388608 | tf_op jit(solution)/shard_map/all_to_all | solution.py:198
  66.0 26.3 %copy-start.20 = (s32[6,4]{0,1:T(4,128)S(1)}, s32[6,4]{0,1:T(4,128)}, u32[]{:S(2)}) copy-start(s32[6,4]{0,1:T(4,128)} %param.25) | copy-start | bytes 292
  92.3 6.0 %copy-start.14 = (bf16[1,2048]{1,0:T(2,128)(2,1)S(1)}, bf16[1,2048]{1,0:T(2,128)(2,1)}, u32[]{:S(2)}) copy-start(bf16[1,2048]{1,0:T(2,128)(2,1)} %param.29) | copy-start | bytes 12292
  164.7 5.1 %copy-start.8 = (f32[384,256]{1,0:T(8,128)S(1)}, f32[384,256]{1,0:T(8,128)}, u32[]{:S(2)}) copy-start(f32[384,256]{1,0:T(8,128)} %copy.183) | copy-start | bytes 1179652
  166.7 8.1 %copy-start.4 = (bf16[24,64,256]{2,1,0:T(8,128)(2,1)S(1)}, bf16[24,64,256]{2,1,0:T(8,128)(2,1)}, u32[]{:S(2)}) copy-start(bf16[24,64,256]{2,1,0:T(8,128)(2,1)} %get-tuple-element.187) | copy-start | bytes 2359300
  180.5 2.9 copy-start.26
  187.9 7.4 %copy-start.15 = (bf16[1,2048]{1,0:T(2,128)(2,1)S(1)}, bf16[1,2048]{1,0:T(2,128)(2,1)}, u32[]{:S(2)}) copy-start(bf16[1,2048]{1,0:T(2,128)(2,1)} %param.29) | copy-start | bytes 12292
  187.9 7.4 %copy-start.2 = (bf16[24,64,256]{2,1,0:T(8,128)(2,1)S(1)}, bf16[24,64,256]{2,1,0:T(8,128)(2,1)}, u32[]{:S(2)}) copy-start(bf16[24,64,256]{2,1,0:T(8,128)(2,1)} %copy-done.1) | copy-start | bytes 2359300
  187.9 7.4 %copy-start.6 = (bf16[6,64,256]{2,1,0:T(8,128)(2,1)S(1)}, bf16[6,64,256]{2,1,0:T(8,128)(2,1)}, u32[]{:S(2)}) copy-start(bf16[6,64,256]{2,1,0:T(8,128)(2,1)} %copy-done.5) | copy-start | bytes 589828
  187.9 7.8 %copy-start.22 = (f32[384]{0:T(512)S(1)}, f32[384]{0:T(512)}, u32[]{:S(2)}) copy-start(f32[384]{0:T(512)} %get-tuple-element.196) | copy-start | bytes 4612
  187.9 7.9 %copy-start.23 = (f32[384]{0:T(512)S(1)}, f32[384]{0:T(512)}, u32[]{:S(2)}) copy-start(f32[384]{0:T(512)} %get-tuple-element.197) | copy-start | bytes 4612
  187.9 102.2 %all-to-all-start.3 = ((bf16[64,1,64,512]{3,2,1,0:T(8,128)(2,1)}), bf16[64,1,64,512]{3,2,1,0:T(8,128)(2,1)}, u32[]{:S(2)}, u32[]{:S(2)}) async-start(bf16[64,1,64,512]{3,2,1,0:T(8,128)(2,1)} %fusion.24), calls=%async_computation.3 | async-start | bytes 8388608 | tf_op jit(solution)/shard_map/all_to_all | solution.py:256
  195.2 144.8 %reduce-scatter.8.cloned.1.call-start = ((), (), s32[]{:S(2)}) async-start(), calls=%async_computation.9 | async-start | bytes 2359296 | tf_op jit(solution)/shard_map/reduce_scatter | solution.py:45
  298.5 5.1 %copy-start.21 = (f32[384]{0:T(512)S(1)}, f32[384]{0:T(512)}, u32[]{:S(2)}) copy-start(f32[384]{0:T(512)} %get-tuple-element.189) | copy-start | bytes 4612
  306.8 28.3 %all-to-all-start.2 = ((bf16[4,384,512]{2,1,0:T(8,128)(2,1)}), bf16[4,384,512]{2,1,0:T(8,128)(2,1)}, u32[]{:S(2)}, u32[]{:S(2)}) async-start(bf16[4,384,512]{2,1,0:T(8,128)(2,1)} %bitcast.232), calls=%async_computation.2 | async-start | bytes 3145728 | tf_op jit(solution)/shard_map/all_to_all | solution.py:39
  335.1 52.0 %all-to-all-start.4 = ((bf16[4,16,64,512]{3,2,1,0:T(8,128)(2,1)}), bf16[4,16,64,512]{3,2,1,0:T(8,128)(2,1)}, u32[]{:S(2)}, u32[]{:S(2)}) async-start(bf16[4,16,64,512]{3,2,1,0:T(8,128)(2,1)} %bitcast.221), calls=%async_computation.4 | async-start | bytes 8388608 | tf_op jit(solution)/shard_map/all_to_all | solution.py:39
  339.9 27.5 %reduce-scatter.10.cloned.1.call-start = ((), (), s32[]{:S(2)}) async-start(), calls=%async_computation.10 | async-start | bytes 327680
  341.8 49.5 %reduce-scatter.12.cloned.1.call-start = ((), (), s32[]{:S(2)}) async-start(), calls=%async_computation.11 | async-start | bytes 98304
  (12 other events, 19.6 us)
Sparse Core Ops, SparseCore 0:
  9.8 32.6 all-gather.1
  303.7 35.7 reduce-scatter.7
  343.8 23.5 reduce-scatter.9
  370.3 14.8 reduce-scatter.11
where the time goes:
time: 402 us; the launch traced here: 398 us
  waiting for transfers between devices  199 us (50%)
  matrix products  56.4 us (14%)
  local copies, waits for them, and re-layouts  55.9 us (14%)
  starting transfers between devices  40.7 us (10%)
  other arithmetic  31.7 us (8%)
  between operations  14.5 us (4%)
    all_to_all x1, waiting for transfers between devices, body(): lax.all_to_all(reply_slots, ST, split_axis=0, concat_axis=0, tiled=True)  94.1 us
    all_to_all x1, waiting for transfers between devices, body(): lax.all_to_all(send_rows, ST, split_axis=0, concat_axis=0, tiled=True)  61.1 us
    unnamed x6, waiting for transfers between devices  26.3 us
    all_to_all x2, waiting for transfers between devices, sum_at_owner(): lax.all_to_all(parts, axis, split_axis=0, concat_axis=0, tiled=True)  17.1 us
    all_to_all x1, starting transfers between devices, copy_for_each(): return lax.all_to_all(copies, axis, split_axis=0, concat_axis=0, tiled=True)  13.3 us
    convert_element_type x2, local copies, waits for them, and re-layouts, body(): row_term.reshape(pass_local, span_rows, model_width).astype(jnp.bfloat16)  13 us
    unnamed x61, local copies, waits for them, and re-layouts  12.7 us
    all_to_all x1, starting transfers between devices, body(): lax.all_to_all(send_rows, ST, split_axis=0, concat_axis=0, tiled=True)  10.5 us
  transfers between devices with their start and end apart: 9, of which 4 were waited for; matrix products, arithmetic and copies ran while one was open for 26% of the time, Pallas kernels for 0%

commit v1 on v0

v1 whole, which is shorter than its diff:
```python
import functools

import jax
import jax.numpy as jnp
from jax import lax
from jax.experimental import pallas as pl
from jax.experimental.pallas import tpu as pltpu
from jax.sharding import Mesh
from jax.sharding import PartitionSpec as P

SPAN = 64
ST = ("st_0", "st_1", "st_2")
MESH = pl.DeviceIdType.MESH
NZ, NY, NX = 8, 4, 4
VMEM = pltpu.VMEM
F32, BF16 = jnp.float32, jnp.bfloat16

NORM_FLOOR = 1.0
SCORE_GAIN = 4.0
CONTRACT_LAST = (((1,), (1,)), ((), ()))
CONTRACT_FIRST = (((0,), (0,)), ((), ()))


def place():
    return (lax.axis_index("st_0"), lax.axis_index("st_1"), lax.axis_index("st_2"), lax.axis_index("tp"))


def wrap(value, size):
    return lax.rem(value + size, size)


class Copies:
    def __init__(self):
        self.started = []

    def make(self, src, dst, send, recv, where):
        return pltpu.make_async_remote_copy(
            src_ref=src, dst_ref=dst, send_sem=send, recv_sem=recv, device_id=where, device_id_type=MESH
        )

    def start(self, src, dst, send, recv, where):
        copy = self.make(src, dst, send, recv, where)
        copy.start()
        self.started.append(copy)

    def arrived(self, dst, send, recv, where):
        self.make(dst, dst, send, recv, where).wait_recv()

    def finish(self):
        for copy in self.started:
            copy.wait_send()


def greet(peers):
    barrier = pltpu.get_barrier_semaphore()
    for peer in peers:
        pl.semaphore_signal(barrier, inc=1, device_id=peer, device_id_type=MESH)
    pl.semaphore_wait(barrier, len(peers))


def column_peers(z, c):
    me = z * 2 + c
    peers = []
    for step in range(1, 2 * NZ):
        other = wrap(me + step, 2 * NZ)
        peers.append({"st_0": other // 2, "st_2": lax.rem(other, 2)})
    return peers


def gather_kernel(
    pas, wk, wv, tok, wq, gw, cot, tbl,
    kv, qa, ca, tl, klow, qlow, grow,
    toks, xs, xr, ys, yr, zs, zr, ps, pr, ts, tr,
):
    z, y, c, x = place()
    me = z * 2 + c
    up, down = {"st_0": wrap(z + 1, NZ)}, {"st_0": wrap(z - 1, NZ)}
    east, west = {"st_1": wrap(y + 1, NY)}, {"st_1": wrap(y - 1, NY)}
    front, back = {"tp": wrap(x + 1, NX)}, {"tp": wrap(x - 1, NX)}
    partner = {"st_2": 1 - c}
    peers = column_peers(z, c)
    greet(peers + [east, west, front, back])
    copies = Copies()
    half = 192
    zdirs, ydirs, xdirs = (up, down), (east, west), (front, back)

    def rows_of(ref, slot, h):
        return ref.at[slot, pl.ds(h * half, half), :]

    def z_send(k, ref, d, h):
        for way in (0, 1):
            if d == 4 and h != way:
                continue
            owner = wrap(z - (d - 1), NZ) if way == 0 else wrap(z + (d - 1), NZ)
            piece = rows_of(ref, owner * 2 + c, h)
            at = (d - 1) * 2 + h if d < 4 else 6
            copies.start(piece, piece, zs.at[k, way, at], zr.at[k, way, at], zdirs[way])

    def z_take(k, ref, d):
        for h in (0, 1):
            for way in (0, 1):
                if d == 4 and h != way:
                    continue
                owner = wrap(z - d, NZ) if way == 0 else wrap(z + d, NZ)
                piece = rows_of(ref, owner * 2 + c, h)
                at = (d - 1) * 2 + h if d < 4 else 6
                copies.arrived(piece, zs.at[k, way, at], zr.at[k, way, at], zdirs[way])
                if d < 3 or (d == 3 and h == way):
                    nxt = d * 2 + h if d < 3 else 6
                    copies.start(piece, piece, zs.at[k, way, nxt], zr.at[k, way, nxt], zdirs[way])
                to = 2 + way * 7 + at
                copies.start(piece, piece, ps.at[k, to], pr.at[k, to], partner)

    def own_send(k, ref):
        for h in (0, 1):
            z_send(k, ref, 1, h)
        for h in (0, 1):
            piece = rows_of(ref, me, h)
            copies.start(piece, piece, ps.at[k, h], pr.at[k, h], partner)

    def partner_take(k, ref):
        theirs = 1 - c
        for h in (0, 1):
            piece = rows_of(ref, z * 2 + theirs, h)
            copies.arrived(piece, ps.at[k, h], pr.at[k, h], partner)
        for d in (1, 2, 3, 4):
            for h in (0, 1):
                for way in (0, 1):
                    if d == 4 and h != way:
                        continue
                    owner = wrap(z - d, NZ) if way == 0 else wrap(z + d, NZ)
                    to = 2 + way * 7 + ((d - 1) * 2 + h if d < 4 else 6)
                    piece = rows_of(ref, owner * 2 + theirs, h)
                    copies.arrived(piece, ps.at[k, to], pr.at[k, to], partner)

    toks[x] = tok[...]
    for way in (0, 1):
        for h in (0, 1):
            piece = rows_of(toks, x, h)
            copies.start(piece, piece, xs.at[way, h], xr.at[way, h], xdirs[way])
    ca[me] = cot[...]
    own_send(0, ca)

    rows = 256

    def kv_rows(i):
        return kv.at[y, pl.ds(i * rows, rows), :]

    for i in range(4):
        block = pas[pl.ds(i * rows, rows), :]
        low = jnp.dot(block, wk[...], preferred_element_type=F32).astype(BF16)
        wide = low.astype(F32)
        scale = lax.rsqrt(jnp.mean(wide * wide, axis=-1, keepdims=True) + NORM_FLOOR)
        klow[pl.ds(i * rows, rows), :] = low
        kv[y, pl.ds(i * rows, rows), pl.ds(0, 256)] = (wide * scale).astype(BF16)
        kv[y, pl.ds(i * rows, rows), pl.ds(256, 256)] = jnp.dot(
            block, wv[...], preferred_element_type=F32
        ).astype(BF16)
        for way in (0, 1):
            copies.start(kv_rows(i), kv_rows(i), ys.at[way, i], yr.at[way, i], ydirs[way])

    def y_take(i):
        for way in (0, 1):
            owner = wrap(y - 1, NY) if way == 0 else wrap(y + 1, NY)
            piece = kv.at[owner, pl.ds(i * rows, rows), :]
            copies.arrived(piece, ys.at[way, i], yr.at[way, i], ydirs[way])
            if i % 2 == way:
                at = 4 + i // 2
                copies.start(piece, piece, ys.at[way, at], yr.at[way, at], ydirs[way])

    def y_last():
        owner = wrap(y + 2, NY)
        for i in range(4):
            way, at = i % 2, 4 + i // 2
            piece = kv.at[owner, pl.ds(i * rows, rows), :]
            copies.arrived(piece, ys.at[way, at], yr.at[way, at], ydirs[way])

    def x_take():
        for way in (0, 1):
            owner = wrap(x - 1, NX) if way == 0 else wrap(x + 1, NX)
            for h in (0, 1):
                piece = rows_of(toks, owner, h)
                copies.arrived(piece, xs.at[way, h], xr.at[way, h], xdirs[way])
                if h == way:
                    copies.start(piece, piece, xs.at[way, 2], xr.at[way, 2], xdirs[way])

    def x_last():
        owner = wrap(x + 2, NX)
        for way in (0, 1):
            piece = rows_of(toks, owner, way)
            copies.arrived(piece, xs.at[way, 2], xr.at[way, 2], xdirs[way])

    def project(owner):
        block = toks[owner]
        at = pl.ds(pl.multiple_of(owner * 512, 512), 512)
        return (
            jnp.dot(block, wq[at, :], preferred_element_type=F32),
            lax.dot_general(gw[:, at], block, CONTRACT_LAST, preferred_element_type=F32),
        )

    z_take(0, ca, 1)
    y_take(0)
    acc = project(x)
    x_take()
    z_take(0, ca, 2)
    for owner in (wrap(x - 1, NX), wrap(x + 1, NX)):
        more = project(owner)
        acc = (acc[0] + more[0], acc[1] + more[1])
    y_take(1)
    x_last()
    more = project(wrap(x + 2, NX))
    low = (acc[0] + more[0]).astype(BF16)
    gate = jax.nn.sigmoid(acc[1] + more[1])
    wide = low.astype(F32)
    scale = lax.rsqrt(jnp.mean(wide * wide, axis=-1, keepdims=True) + NORM_FLOOR)
    qlow[...] = low
    qa[me] = (wide * scale).astype(BF16)
    own_send(1, qa)
    z_take(0, ca, 3)
    grow[...] = gate[0:8]
    tl[me] = jnp.zeros((8, 128), F32)
    for b in range(6):
        tl[me, b : b + 1, 0:64] = gate[0:1, b * 64 : b * 64 + 64]
    tl[me, 6:7, 0:64] = tbl[...]
    for step, peer in enumerate(peers):
        copies.start(tl.at[me], tl.at[me], ts.at[step], tr.at[step], peer)
    y_take(2)
    z_take(1, qa, 1)
    y_take(3)
    z_take(1, qa, 2)
    z_take(0, ca, 4)
    z_take(1, qa, 3)
    z_take(1, qa, 4)
    for step in range(2 * NZ - 1):
        other = wrap(me - (step + 1), 2 * NZ)
        copies.arrived(tl.at[other], ts.at[step], tr.at[step], peers[step])
    partner_take(0, ca)
    partner_take(1, qa)
    y_last()
    copies.finish()


def score_kernel(tb, kv, qa, ca, tl, eg, tot, own, sent, parts, total, ss, sr, bs, br):
    z, y, c, x = place()
    me = z * 2 + c
    peers = column_peers(z, c)
    greet(peers)
    copies = Copies()
    gain = SCORE_GAIN * 256 ** (-0.5)
    line = lax.broadcasted_iota(jnp.int32, (8, 128), 0)

    def reader(r, carry):
        tile = tl[r]
        stats = jnp.zeros((8, 128), F32)
        for yy in range(NY):
            entry = tb[r, (z * NY + yy) * 2 + c]
            used = entry >= 0
            safe = jnp.maximum(entry, 0)
            b, loc = safe // 64, lax.rem(safe, 16)
            keys_values = kv[yy * 16 + loc]
            scores = gain * lax.dot_general(
                keys_values[:, 0:256], qa[r * 6 + b], CONTRACT_LAST, preferred_element_type=F32
            )
            here = (line == b) & used
            gate = jnp.sum(jnp.where(line == b, tile, 0.0), axis=0, keepdims=True)
            grads = gate[:, 0:64] * lax.dot_general(
                keys_values[:, 256:512], ca[r * 6 + b], CONTRACT_LAST, preferred_element_type=F32
            )
            exps = jnp.exp(scores)
            both = jnp.concatenate([exps, grads], axis=1)
            eg[r * NY + yy] = both
            row = jnp.concatenate(
                [jnp.sum(exps, axis=0, keepdims=True), jnp.sum(exps * grads, axis=0, keepdims=True)], axis=1
            )
            stats = stats + jnp.where(here, row, 0.0)
        sent[r] = stats
        return carry

    lax.fori_loop(0, 2 * NZ, reader, 0)
    for step, peer in enumerate(peers):
        other = wrap(me + step + 1, 2 * NZ)
        copies.start(sent.at[other], parts.at[step], ss.at[step], sr.at[step], peer)
    whole = sent[me]
    for step in range(2 * NZ - 1):
        copies.arrived(parts.at[step], ss.at[step], sr.at[step], peers[step])
        whole = whole + parts[step]
    total[...] = whole
    tot[me] = whole
    own[...] = whole
    for step, peer in enumerate(peers):
        copies.start(total, tot.at[me], bs.at[step], br.at[step], peer)
    for step in range(2 * NZ - 1):
        other = wrap(me - (step + 1), 2 * NZ)
        copies.arrived(tot.at[other], bs.at[step], br.at[step], peers[step])
    copies.finish()


def grads_kernel(tb, kv, qa, ca, tl, eg, tot, kvg, qp, kacc, qacc):
    z, c = lax.axis_index("st_0"), lax.axis_index("st_2")
    gain = SCORE_GAIN * 256 ** (-0.5)
    kacc[...] = jnp.zeros(kacc.shape, F32)
    qacc[...] = jnp.zeros(qacc.shape, F32)

    @pl.loop(0, 2 * NZ)
    def _(r):
        for yy in range(NY):
            entry = tb[r, (z * NY + yy) * 2 + c]

            @pl.when(entry >= 0)
            def _():
                b, loc = entry // 64, lax.rem(entry, 16)
                row = tot[r, pl.ds(b, 1), :]
                gate = tl[r, pl.ds(b, 1), 0:64]
                norm = 1.0 / row[:, 0:64]
                both = eg[r * NY + yy]
                probs = both[:, 0:64] * norm
                slope = (probs * (both[:, 64:128] - row[:, 64:128] * norm)).astype(BF16)
                gated = (probs * gate).astype(BF16)
                at, slot = r * 6 + b, yy * 16 + loc
                key = gain * jnp.dot(slope, qa[at], preferred_element_type=F32)
                value = jnp.dot(gated, ca[at], preferred_element_type=F32)
                kacc[slot, :, 0:256] += key.astype(BF16).astype(F32)
                kacc[slot, :, 256:512] += value.astype(BF16).astype(F32)
                qacc[at] += gain * lax.dot_general(
                    slope, kv[slot, :, 0:256], CONTRACT_FIRST, preferred_element_type=F32
                )

    @pl.loop(0, 64)
    def _(i):
        kvg[i] = kacc[i].astype(BF16)

    @pl.loop(0, 96)
    def _(i):
        qp[i] = qacc[i].astype(BF16)


def return_kernel(kvg, qp, kvs, qg, ybuf, ysum, px, qs, zbuf, ys, yr, zs, zr, ps, pr):
    z, y, c, x = place()
    up, down = {"st_0": wrap(z + 1, NZ)}, {"st_0": wrap(z - 1, NZ)}
    east, west = {"st_1": wrap(y + 1, NY)}, {"st_1": wrap(y - 1, NY)}
    partner = {"st_2": 1 - c}
    greet([up, down, east, west, partner])
    copies = Copies()
    zdirs, ydirs = (up, down), (east, west)
    half = 192
    order = [4, 3, 5, 2, 6, 1, 7, 0]
    for k in order:
        there = wrap(z + k, NZ)
        copies.start(qp.at[there * 2 + 1 - c], px.at[there], ps.at[k], pr.at[k], partner)
    part, sub = 512, 256
    far, beside = wrap(y + 2, NY), (wrap(y + 1, NY), wrap(y - 1, NY))
    for j in (0, 1):
        for way in (0, 1):
            at = pl.ds(way * part + j * sub, sub)
            copies.start(kvg.at[far, at, :], ybuf.at[way, pl.ds(j * sub, sub), :], ys.at[way, j], yr.at[way, j], ydirs[way])
    for way in (0, 1):
        at = pl.ds((1 - way) * part, part)
        copies.start(kvg.at[beside[way], at, :], ysum.at[way, at, :], ys.at[way, 4], yr.at[way, 4], ydirs[way])

    def q_pair(k):
        there = wrap(z + k, NZ)
        copies.arrived(px.at[there], ps.at[k], pr.at[k], partner)
        qs[there] = (qp[there * 2 + c].astype(F32) + px[there].astype(F32)).astype(BF16)

    def y_add(j):
        for way in (0, 1):
            copies.arrived(ybuf.at[way, pl.ds(j * sub, sub), :], ys.at[way, j], yr.at[way, j], ydirs[way])
            at = pl.ds(way * part + j * sub, sub)
            mine = kvg[beside[way], at, :].astype(F32)
            ybuf[way, pl.ds(j * sub, sub), :] = (
                mine + ybuf[way, pl.ds(j * sub, sub), :].astype(F32)
            ).astype(BF16)
            copies.start(
                ybuf.at[way, pl.ds(j * sub, sub), :], ysum.at[way, at, :], ys.at[way, 2 + j], yr.at[way, 2 + j], ydirs[way]
            )

    def z_step(d):
        for way in (0, 1):
            there = wrap(z + d, NZ) if way == 0 else wrap(z - d, NZ)
            if d == 3:
                piece = zbuf.at[way, 0, pl.ds(way * half, half), :]
                copies.arrived(piece, zs.at[way, 3], zr.at[way, 3], zdirs[way])
                at = pl.ds(way * half, half)
                qs[there, at, :] = (
                    qs[there, at, :].astype(F32) + zbuf[way, 0, at, :].astype(F32)
                ).astype(BF16)
            elif d < 3:
                piece = zbuf.at[way, 3 - d]
                copies.arrived(piece, zs.at[way, d], zr.at[way, d], zdirs[way])
                qs[there] = (qs[there].astype(F32) + zbuf[way, 3 - d].astype(F32)).astype(BF16)
            if d == 4:
                at = pl.ds(way * half, half)
                copies.start(qs.at[there, at, :], zbuf.at[way, 0, at, :], zs.at[way, 3], zr.at[way, 3], zdirs[way])
            else:
                copies.start(qs.at[there], zbuf.at[way, 4 - d], zs.at[way, d - 1], zr.at[way, d - 1], zdirs[way])

    q_pair(4)
    z_step(4)
    q_pair(3)
    q_pair(5)
    q_pair(2)
    q_pair(6)
    z_step(3)
    q_pair(1)
    q_pair(7)
    q_pair(0)
    y_add(0)
    z_step(2)
    y_add(1)
    z_step(1)
    grad = qs[z].astype(F32)
    for way in (0, 1):
        copies.arrived(zbuf.at[way, 3], zs.at[way, 0], zr.at[way, 0], zdirs[way])
        grad = grad + zbuf[way, 3].astype(F32)
    qg[...] = grad
    for way in (0, 1):
        at = pl.ds((1 - way) * part, part)
        copies.arrived(ysum.at[way, at, :], ys.at[way, 4], yr.at[way, 4], ydirs[way])
    for way in (0, 1):
        for j in (0, 1):
            at = pl.ds(way * part + j * sub, sub)
            copies.arrived(ysum.at[way, at, :], ys.at[way, 2 + j], yr.at[way, 2 + j], ydirs[way])
    for i in range(4):
        at = pl.ds(i * 256, 256)
        kvs[at, :] = kvg[y, at, :].astype(F32) + ysum[0, at, :].astype(F32) + ysum[1, at, :].astype(F32)
    copies.finish()


def shaped(shape, dtype):
    return jax.ShapeDtypeStruct(shape, dtype)


def dma(*shape):
    return pltpu.SemaphoreType.DMA(shape)


def call(kernel, outs, scratch, collective, smem=0, limit=48, count=0, **extra):
    in_specs = [pl.BlockSpec(memory_space=pltpu.SMEM)] * smem + [pl.BlockSpec(memory_space=VMEM)] * (count - smem)
    params = dict(vmem_limit_bytes=limit * 2**20)
    if collective is not None:
        params.update(collective_id=collective, has_side_effects=True)
    return pl.pallas_call(
        kernel,
        out_shape=outs,
        in_specs=in_specs,
        out_specs=[pl.BlockSpec(memory_space=VMEM)] * len(outs),
        scratch_shapes=scratch,
        compiler_params=pltpu.CompilerParams(**params),
        **extra,
    )


def in_blocks(shard, dim, devices):
    before, after = (shard.shape[:dim], shard.shape[dim + 1 :])
    return jnp.moveaxis(shard.reshape(*before, devices, -1, *after), dim, 0)


def sum_at_owner(shard, axis, dim):
    parts = in_blocks(shard, dim, lax.axis_size(axis))
    arrived = lax.all_to_all(parts, axis, split_axis=0, concat_axis=0, tiled=True)
    return arrived.astype(jnp.float32).sum(axis=0)


def sum_by_axis(shard, axes, dim):
    for axis in axes:
        shard = lax.psum_scatter(shard, axis, scatter_dimension=dim, tiled=True)
    return shard


def neumann_inverse(strict_part):
    span_size = strict_part.shape[-1]
    unit_eye = jnp.eye(span_size, dtype=jnp.float32)
    running = unit_eye - strict_part
    power_term = strict_part
    for _ in range(span_size.bit_length() - 2):
        power_term = jnp.einsum("...ij,...jk->...ik", power_term, power_term)
        running = jnp.einsum("...ij,...jk->...ik", running, unit_eye + power_term)
    return running


def delta_mixer(queries, keys_in, values_in, strength, log_decay):
    heads_n, length, key_dim = queries.shape
    blocks_n = length // SPAN

    def to_blocks(tensor):
        return tensor.reshape(heads_n, blocks_n, SPAN, *tensor.shape[2:])

    queries, keys_in, values_in = (to_blocks(queries), to_blocks(keys_in), to_blocks(values_in))
    strength, log_decay = (to_blocks(strength), to_blocks(log_decay))
    cumulative = jnp.cumsum(log_decay, axis=-1)
    position = jnp.arange(SPAN)
    inclusive = position[:, None] >= position[None, :]
    strictly = position[:, None] > position[None, :]
    spread = jnp.where(inclusive, cumulative[..., :, None] - cumulative[..., None, :], -jnp.inf)
    decay_map = jnp.exp(spread)
    key_gram = jnp.einsum("hncd,hnmd->hncm", keys_in, keys_in)
    strict_part = jnp.where(strictly, strength[..., :, None] * key_gram * decay_map, 0.0)
    inverse = neumann_inverse(strict_part)
    fresh_vals = jnp.einsum("hncm,hnme->hnce", inverse, values_in * strength[..., None])
    correction = jnp.einsum(
        "hncm,hnmd->hncd", inverse, keys_in * (strength * jnp.exp(cumulative))[..., None]
    )
    attend_map = jnp.where(
        inclusive, jnp.einsum("hncd,hnmd->hncm", queries, keys_in) * decay_map, 0.0
    )
    query_dec = queries * jnp.exp(cumulative)[..., None]
    key_dec = keys_in * jnp.exp(cumulative[..., -1:] - cumulative)[..., None]
    carry_decay = jnp.exp(cumulative[..., -1])

    def advance(memory_state, inputs):
        fresh_blk, correct_blk, attend_blk, query_blk, key_blk, decay_blk = inputs
        new_values = fresh_blk - jnp.einsum("hcd,hde->hce", correct_blk, memory_state)
        output = jnp.einsum("hcd,hde->hce", query_blk, memory_state) + jnp.einsum(
            "hcm,hme->hce", attend_blk, new_values
        )
        memory_state = memory_state * decay_blk[:, None, None] + jnp.einsum(
            "hcd,hce->hde", key_blk, new_values
        )
        return (memory_state, output)

    stacked = tuple(
        (
            jnp.moveaxis(tensor, 1, 0)
            for tensor in (fresh_vals, correction, attend_map, query_dec, key_dec, carry_decay)
        )
    )
    initial = jnp.zeros((heads_n, key_dim, values_in.shape[-1]), jnp.float32)
    _, outputs = lax.scan(advance, initial, stacked)
    return jnp.transpose(outputs, (1, 0, 2, 3)).reshape(heads_n, length, -1)


def mixer_output(query_raw, key_raw, value_raw, beta_raw, decay_raw, rate_vals):
    length = query_raw.shape[0]
    heads_n = beta_raw.shape[0]

    def heads_first(matrix):
        return jnp.transpose(matrix.astype(jnp.float32).reshape(length, heads_n, -1), (1, 0, 2))

    queries = heads_first(query_raw)
    keys_in = heads_first(key_raw)
    values_in = heads_first(value_raw)
    queries = (
        queries
        * lax.rsqrt(jnp.sum(queries * queries, axis=-1, keepdims=True) + NORM_FLOOR)
        * queries.shape[-1] ** (-0.5)
    )
    keys_in = keys_in * lax.rsqrt(jnp.sum(keys_in * keys_in, axis=-1, keepdims=True) + NORM_FLOOR)
    strength = jax.nn.sigmoid(beta_raw)
    log_decay = -rate_vals[:, None] * jax.nn.softplus(decay_raw)
    mixer_out = delta_mixer(queries, keys_in, values_in, strength, log_decay)
    return jnp.transpose(mixer_out, (1, 0, 2)).reshape(length, -1)


def body(
    tokens, cotangent, mix_query, mix_key, mix_value, beta_pre, decay_pre, decay_rate,
    passages, passage_ids, query_weight, key_weight, value_weight, gate_weight,
):
    pass_local, span_rows, model_width = passages.shape
    flat_rows = passages.reshape(pass_local * span_rows, model_width)
    ids = passage_ids.reshape(24)
    place_of = jnp.arange(24, dtype=jnp.int32) * 16 + ids % 16
    wanted = (ids // 16)[:, None] == jnp.arange(64, dtype=jnp.int32)[None, :]
    table = jnp.max(jnp.where(wanted, place_of[:, None], -1), axis=0).astype(F32)[None, :]
    gate_rows = jnp.broadcast_to(gate_weight, (16, model_width))
    kv, qa, ca, tl, key_low, query_low, gate_row = call(
        gather_kernel,
        [
            shaped((NY, 1024, 512), BF16), shaped((16, 384, 256), BF16), shaped((16, 384, 256), BF16),
            shaped((16, 8, 128), F32), shaped((1024, 256), BF16), shaped((384, 256), BF16), shaped((8, 384), F32),
        ],
        [
            VMEM((NX, 384, 512), BF16), dma(2, 3), dma(2, 3), dma(2, 6), dma(2, 6), dma(2, 2, 7), dma(2, 2, 7),
            dma(2, 16), dma(2, 16), dma(15), dma(15),
        ],
        1, count=8,
    )(flat_rows, key_weight, value_weight, tokens, query_weight, gate_rows, cotangent, table)
    mixer_out = mixer_output(mix_query, mix_key, mix_value, beta_pre, decay_pre, decay_rate)
    lookup = tl[:, 6, 0:64].astype(jnp.int32)
    kv_one, qa_one, ca_one = kv.reshape(64, 64, 512), qa.reshape(96, 64, 256), ca.reshape(96, 64, 256)
    eg, tot, own = call(
        score_kernel,
        [shaped((64, 64, 128), F32), shaped((16, 8, 128), F32), shaped((8, 128), F32)],
        [
            VMEM((16, 8, 128), F32), VMEM((15, 8, 128), F32), VMEM((8, 128), F32),
            dma(15), dma(15), dma(15), dma(15),
        ],
        2, smem=1, count=5,
    )(lookup, kv_one, qa_one, ca_one, tl)
    kvg, qp = call(
        grads_kernel,
        [shaped((64, 64, 512), BF16), shaped((96, 64, 256), BF16)],
        [VMEM((64, 64, 512), F32), VMEM((96, 64, 256), F32)],
        None, smem=1, count=7,
    )(lookup, kv_one, qa_one, ca_one, tl, eg, tot)
    kvs, qhat_grad = call(
        return_kernel,
        [shaped((1024, 512), F32), shaped((384, 256), F32)],
        [
            VMEM((2, 512, 512), BF16), VMEM((2, 1024, 512), BF16), VMEM((NZ, 384, 256), BF16),
            VMEM((NZ, 384, 256), BF16), VMEM((2, 4, 384, 256), BF16),
            dma(2, 5), dma(2, 5), dma(2, 4), dma(2, 4), dma(8), dma(8),
        ],
        3, count=2,
    )(kvg.reshape(NY, 1024, 512), qp.reshape(16, 384, 256))

    query_float = query_low.astype(F32)
    query_scale = lax.rsqrt(jnp.mean(query_float * query_float, axis=-1, keepdims=True) + NORM_FLOOR)
    key_float = key_low.astype(F32)
    key_scale = lax.rsqrt(jnp.mean(key_float * key_float, axis=-1, keepdims=True) + NORM_FLOOR)
    gate_open = gate_row[0]
    dots = (own[0:6, 64:128] / own[0:6, 0:64]).reshape(384)
    grad_out = cotangent.astype(F32)
    gate_grad = (1.0 - gate_open) * (dots - gate_open * jnp.sum(grad_out * mixer_out, axis=-1))
    query_grad = (
        query_scale * qhat_grad
        - query_scale**3 * query_float * jnp.mean(query_float * qhat_grad, axis=-1, keepdims=True)
    ).astype(BF16)
    token_term = (
        lax.dot_general(query_grad, query_weight, CONTRACT_LAST, preferred_element_type=F32)
        + gate_grad[:, None] * gate_weight[0].astype(F32)[None, :]
    )
    token_grad = sum_at_owner(token_term.astype(BF16), "tp", 1).astype(BF16)
    key_hat_grad, value_grad = kvs[:, 0:256], kvs[:, 256:512]
    key_grad = (
        key_scale * key_hat_grad
        - key_scale**3 * key_float * jnp.mean(key_float * key_hat_grad, axis=-1, keepdims=True)
    ).astype(BF16)
    value_grad_low = value_grad.astype(BF16)
    row_term = lax.dot_general(
        key_grad, key_weight, CONTRACT_LAST, preferred_element_type=F32
    ) + lax.dot_general(value_grad_low, value_weight, CONTRACT_LAST, preferred_element_type=F32)
    passage_grad = sum_at_owner(
        row_term.reshape(pass_local, span_rows, model_width).astype(BF16), "tp", 2
    ).astype(BF16)
    weight_term = lax.dot_general(flat_rows, key_grad, CONTRACT_FIRST, preferred_element_type=F32)
    key_weight_grad = sum_by_axis(weight_term, ST, 0)
    return (token_grad, passage_grad, key_weight_grad)


def solution(mesh):
    torus = Mesh(mesh.devices.reshape(8, 4, 2, mesh.shape["tp"]), ("st_0", "st_1", "st_2", "tp"))
    return jax.shard_map(
        body,
        mesh=torus,
        in_specs=(
            P(ST, "tp"),
            P(ST, "tp"),
            P(ST, "tp"),
            P(ST, "tp"),
            P(ST, "tp"),
            P("tp", ST),
            P("tp", ST),
            P("tp"),
            P(ST, None, None),
            P(ST, None),
            P(None, "tp"),
            P(None, "tp"),
            P(None, "tp"),
            P("tp", None),
        ),
        out_specs=(P(ST, "tp"), P(ST, None, "tp"), P(ST, "tp")),
        check_vma=False,
    )
```

time: 402 us -> 326 us (0.81)
  waiting for transfers between devices: 199 us -> 43.1 us
  Pallas kernels: 0 us -> 138 us
  starting transfers between devices: 40.7 us -> 9.55 us
  other arithmetic: 31.7 us -> 18.9 us
  local copies, waits for them, and re-layouts: 55.9 us -> 46 us
  matrix products: 56.4 us -> 51.2 us
    all_to_all x3 -> x0, waiting for transfers between devices: 155 us -> none  [the longest x1 94.1 us: body(): lax.all_to_all(reply_slots, ST, split_axis=0, concat_axis=0, tiled=True)]
    pallas_call x0 -> x4, Pallas kernels: none -> 138 us  [the longest x1 57.9 us: body(): call(gather_kernel, [shaped((NY, 1024, 512), BF16), shaped((16, 384, 256)...]
    all_to_all x3 -> x0, starting transfers between devices: 31.1 us -> none  [the longest x1 13.3 us: copy_for_each(): return lax.all_to_all(copies, axis, split_axis=0, concat_axis=0, tiled=True)]
    dot_general x12 -> x0, matrix products: 18.2 us -> none  [the longest x1 3.94 us: body(): jnp.dot(flat_rows, value_weight, preferred_element_type=jnp.float32)]
    select_n x7 -> x1, other arithmetic: 9.75 us -> 0.01 us  [body(): wanted = (ids // 16)[:, None] == jnp.arange(64, dtype=jnp.int32)[None, :]]
    gather x3 -> x0, local copies, waits for them, and re-layouts: 8.65 us -> none  [the longest x1 2.96 us: body(): mine_rows = arrived[slot_of]]
    slice x2 -> x1, local copies, waits for them, and re-layouts: 5.1 us -> 0.61 us  [body(): gate_open = gate_row[0]]
    unnamed x61 -> x52, local copies, waits for them, and re-layouts: 12.7 us -> 16.4 us
  transfers between devices with their start and end apart: 9 -> 5, of which waited for: 4 -> 3; matrix products, arithmetic and copies ran while one was open for 26% -> 31% of each run, Pallas kernels for 0% -> 0%
where the time goes in v1:
time: 326 us; the launch traced here: 320 us
  Pallas kernels  138 us (42%)
  matrix products  51.2 us (16%)
  local copies, waits for them, and re-layouts  46 us (14%)
  waiting for transfers between devices  43.1 us (13%)
  other arithmetic  18.9 us (6%)
  between operations  14.1 us (4%)
  starting transfers between devices  9.55 us (3%)
    pallas_call x1, Pallas kernels, body(): call(gather_kernel, [shaped((NY, 1024, 512), BF16), shaped((16, 384, 256)...  57.9 us
    pallas_call x1, Pallas kernels, body(): call(return_kernel, [shaped((1024, 512), F32), shaped((384, 256), F32)],...  40.8 us
    unnamed x5, waiting for transfers between devices  24.9 us
    pallas_call x1, Pallas kernels, body(): call(score_kernel, [shaped((64, 64, 128), F32), shaped((16, 8, 128), F32)...  21.6 us
    all_to_all x2, waiting for transfers between devices, sum_at_owner(): lax.all_to_all(parts, axis, split_axis=0, concat_axis=0, tiled=True)  18.2 us
    pallas_call x1, Pallas kernels, body(): call(grads_kernel, [shaped((64, 64, 512), BF16), shaped((96, 64, 256), BF...  17.3 us
    unnamed x52, local copies, waits for them, and re-layouts  16.4 us
    convert_element_type x2, local copies, waits for them, and re-layouts, body(): row_term.reshape(pass_local, span_rows, model_width).astype(BF16)  12.9 us
  transfers between devices with their start and end apart: 5, of which 3 were waited for; matrix products, arithmetic and copies ran while one was open for 31% of the time, Pallas kernels for 0%

profile of v1, /device:TPU:1, one launch (start us, length us, event | category | flops | bytes accessed | tf_op | source)
XLA Modules:
  0.0 320.4 jit_solution(12099250485427990328)
XLA Ops:
  14.5 57.9 %shard_map.157 = (bf16[4,1024,512]{2,1,0:T(8,128)(2,1)}, bf16[16,384,256]{2,1,0:T(8,128)(2,1)}, bf16[16,384,256]{2,1,0:T(8,128)(2,1)}, f32[16,8,128]{2,1,0:T(8,1...) custom-call(bf16[1024,2048]{1,0:T(8,128)(2,1)} %bitcast.155, ...), custom_call_target="tpu_custom_call" | custom-call | tf_op jit(solution)/shard_map/pallas_call | solution.py:565
  74.3 21.6 %shard_map.158 = (f32[64,64,128]{2,1,0:T(8,128)S(1)}, f32[16,8,128]{2,1,0:T(8,128)S(1)}, f32[8,128]{1,0:T(8,128)S(1)}) custom-call(s32[16,64]{1,0:T(8,128)S(1)} %fusion.74.tb, bf16[64,64,512]{2,1,0:T(8,128)(2,1)} %bitcast.158, bf16[96,64,256]{2,1,0:T(8,128)(2,1)S(1)} %bitcast.153, bf16[96,64,256]{2,1,0:T(8,128)(2,1)} %bitcast.164, ...), custom_call_target="tpu_custom_call" | custom-call | tf_op jit(solution)/shard_map/pallas_call | solution.py:580
  95.9 17.3 %shard_map.159 = (bf16[64,64,512]{2,1,0:T(8,128)(2,1)}, bf16[96,64,256]{2,1,0:T(8,128)(2,1)S(1)}) custom-call(s32[16,64]{1,0:T(8,128)S(1)} %fusion.74.tb, bf16[64,64,512]{2,1,0:T(8,128)(2,1)} %bitcast.159, bf16[96,64,256]{2,1,0:T(8,128)(2,1)} %bitcast.152, bf16[96,64,256]{2,1,0:T(8,128)(2,1)} %bitcast.165, f32[16,8,128]{2,1,0:T(8,128)S(1)} %get-tuple-element.65.tl, ...), custom_call_target="tpu_custom_call" | custom-call | tf_op jit(solution)/shard_map/pallas_call | solution.py:589
  113.2 40.8 %shard_map.160 = (f32[1024,512]{1,0:T(8,128)S(1)}, f32[384,256]{1,0:T(8,128)S(1)}) custom-call(bf16[4,1024,512]{2,1,0:T(8,128)(2,1)} %bitcast.167, bf16[16,384,256]{2,1,0:T(8,128)(2,1)S(1)} %bitcast.154), custom_call_target="tpu_custom_call" | custom-call | tf_op jit(solution)/shard_map/pallas_call | solution.py:595
  155.0 2.8 convolution_bitcast_fusion
  167.2 1.9 copy.89
  173.2 1.9 copy.86
  180.4 2.2 fusion.29
  188.1 2.0 convolution_bitcast_fusion.3
  190.1 2.0 convolution_bitcast_fusion.2
  192.1 2.0 fusion.25
  194.1 2.2 multiply_bitcast_fusion
  196.3 30.8 %while.13 = (s32[]{:T(128)}, f32[2,128,128]{2,1,0:T(8,128)S(1)}, f32[6,2,64,128]{3,2,0,1:T(8,128)}, f32[6,2]{1,0:T(8,128)}, bf16[6,2,64,128]{3,2,0,1:T(8,128)(2,...) while((s32[]{:T(128)}, f32[2,128,128]{2,1,0:T(8,128)S(1)}, ...), condition=%wide.region_7.8_spmd.clone, body=%wide.region_6.7_spmd.clone.sunk | while | flops 14893059 | bytes 1018532 | solution.py:528
  230.3 2.0 add_convert_fusion.1
  233.7 4.6 %all-to-all-start = ((bf16[4,384,512]{2,1,0:T(8,128)(2,1)}), bf16[4,384,512]{2,1,0:T(8,128)(2,1)}, u32[]{:S(2)}, u32[]{:S(2)}) async-start(bf16[4,384,512]{2,1,0:T(8,128)(2,1)} %bitcast.166), calls=%async_computation | async-start | bytes 3145728 | tf_op jit(solution)/shard_map/all_to_all | solution.py:460
  238.3 2.8 fusion.79
  241.1 3.3 %add_convert_fusion = bf16[1024,2048]{1,0:T(8,128)(2,1)} fusion(f32[1024,2048]{1,0:T(8,128)S(1)} %fusion.79, bf16[2048,256]{1,0:T(8,128)(2,1)S(1)} %copy-done.2, f32[1024,512]{1,0:T(8,128)S(1)} %get-tuple-element.78), kind=kOutput, calls=%fused_computation.28 | convolution fusion | flops 1077936128 | bytes 14155776 | tf_op jit(solution)/shard_map/dot_general | solution.py:631
  244.4 7.8 %convert_element_type.82 = bf16[16,64,4,512]{3,2,1,0:T(4,128)(2,1)} reshape(bf16[1024,2048]{1,0:T(8,128)(2,1)} %add_convert_fusion) | data formatting | bytes 8388608 | tf_op jit(solution)/shard_map/convert_element_type | solution.py:633
  252.2 5.1 %copy.123 = bf16[16,64,4,512]{3,1,0,2:T(8,128)(2,1)} copy(bf16[16,64,4,512]{3,2,1,0:T(4,128)(2,1)} %convert_element_type.82) | data formatting | bytes 8388608 | tf_op jit(solution)/shard_map/convert_element_type | solution.py:633
  257.8 4.8 %all-to-all-start.1 = ((bf16[4,16,64,512]{3,2,1,0:T(8,128)(2,1)}), bf16[4,16,64,512]{3,2,1,0:T(8,128)(2,1)}, u32[]{:S(2)}, u32[]{:S(2)}) async-start(bf16[4,16,64,512]{3,2,1,0:T(8,128)(2,1)} %bitcast.157), calls=%async_computation.1 | async-start | bytes 8388608 | tf_op jit(solution)/shard_map/all_to_all | solution.py:460
  264.6 24.8 %reduce-scatter.10.cloned.1.call-done = f32[64,256]{1,0:T(8,128)} async-done(((f32[256,256]{1,0:T(8,128)}), f32[64,256]{1,0:T(8,128)}) %reduce-scatter.10.cloned.1.call-update) | async-done | bytes 65552
  289.5 2.5 reduce_sum.92
  292.0 17.7 %all-to-all-done.1 = bf16[4,16,64,512]{3,2,1,0:T(8,128)(2,1)} async-done(((bf16[4,16,64,512]{3,2,1,0:T(8,128)(2,1)}), bf16[4,16,64,512]{3,2,1,0:T(8,128)(2,1)}, u32[]{:S(2)}, u32[]{:S(2)}) %all-to-all-start.1) | async-done | bytes 4194336 | tf_op jit(solution)/shard_map/all_to_all | solution.py:460
  309.7 4.2 %reduce_sum.95 = bf16[16,64,512]{2,1,0:T(8,128)(2,1)} reduce(bf16[4,16,64,512]{3,2,1,0:T(8,128)(2,1)} %all-to-all-done.1, bf16[]{:T(256)} %constant.77.clone.1), dimensions={0}, to_apply=%region_12.13 | reduce | flops 1572864 | bytes 5242882 | tf_op jit(solution)/shard_map/reduce_sum | solution.py:461
  (139 shorter events, 71.9 us)
Async XLA Ops:
  7.2 255.6 %reduce-scatter.8.cloned.1.call-start = ((), (), s32[]{:S(2)}) async-start(), calls=%async_computation.5 | async-start | bytes 2359296 | tf_op jit(solution)/shard_map/reduce_scatter | solution.py:466
  8.9 1.2 copy-start.1
  10.1 1.2 copy-start.3
  11.4 1.2 copy-start.4
  12.6 0.9 copy-start.5
  13.5 1.0 copy-start.7
  72.4 1.9 copy-start
  113.2 41.8 %copy-start.8 = (bf16[16,64,2048]{2,1,0:T(8,128)(2,1)S(1)}, bf16[16,64,2048]{2,1,0:T(8,128)(2,1)}, u32[]{:S(2)}) copy-start(bf16[16,64,2048]{2,1,0:T(8,128)(2,1)} %param.24) | copy-start | bytes 12582916
  155.0 4.7 %copy-start.6 = (bf16[384,256]{1,0:T(8,128)(2,1)S(1)}, bf16[384,256]{1,0:T(8,128)(2,1)}, u32[]{:S(2)}) copy-start(bf16[384,256]{1,0:T(8,128)(2,1)} %cot.1) | copy-start | bytes 589828
  175.1 4.5 %copy-start.11 = (f32[64,64]{1,0:T(8,128)S(1)}, f32[64,64]{1,0:T(8,128)}, u32[]{:S(2)}) copy-start(f32[64,64]{1,0:T(8,128)} %fusion.73) | copy-start | bytes 49156
  176.9 0.8 copy-start.9
  177.9 0.7 copy-start.10
  196.3 32.7 %copy-start.12 = (bf16[384,256]{0,1:T(8,128)(2,1)S(1)}, bf16[384,256]{0,1:T(8,128)(2,1)}, u32[]{:S(2)}) copy-start(bf16[384,256]{0,1:T(8,128)(2,1)} %copy.84) | copy-start | bytes 589828
  196.3 34.0 %copy-start.21 = (f32[384]{0:T(512)S(1)}, f32[384]{0:T(512)}, u32[]{:S(2)}) copy-start(f32[384]{0:T(512)} %reshape.235) | copy-start | bytes 4612
  196.3 34.0 %copy-start.22 = (f32[384]{0:T(512)S(1)}, f32[384]{0:T(512)}, u32[]{:S(2)}) copy-start(f32[384]{0:T(512)} %slice_reduce_fusion.1) | copy-start | bytes 4612
  196.3 34.0 %copy-start.20 = (f32[2048]{0:T(1024)S(1)}, f32[2048]{0:T(1024)}, u32[]{:S(2)}) copy-start(f32[2048]{0:T(1024)} %mul.239) | copy-start | bytes 24580
  232.3 6.0 %copy-start.14 = (f32[1024]{0:T(1024)S(1)}, f32[1024]{0:T(1024)}, u32[]{:S(2)}) copy-start(f32[1024]{0:T(1024)} %copy-done.13) | copy-start | bytes 12292
  232.3 6.0 %copy-start.16 = (f32[1024]{0:T(1024)S(1)}, f32[1024]{0:T(1024)}, u32[]{:S(2)}) copy-start(f32[1024]{0:T(1024)} %copy-done.15) | copy-start | bytes 12292
  232.3 6.0 %copy-start.18 = (f32[1024]{0:T(1024)S(1)}, f32[1024]{0:T(1024)}, u32[]{:S(2)}) copy-start(f32[1024]{0:T(1024)} %copy-done.17) | copy-start | bytes 12292
  233.7 24.1 %all-to-all-start = ((bf16[4,384,512]{2,1,0:T(8,128)(2,1)}), bf16[4,384,512]{2,1,0:T(8,128)(2,1)}, u32[]{:S(2)}, u32[]{:S(2)}) async-start(bf16[4,384,512]{2,1,0:T(8,128)(2,1)} %bitcast.166), calls=%async_computation | async-start | bytes 3145728 | tf_op jit(solution)/shard_map/all_to_all | solution.py:460
  238.3 2.8 copy-start.2
  257.8 51.8 %all-to-all-start.1 = ((bf16[4,16,64,512]{3,2,1,0:T(8,128)(2,1)}), bf16[4,16,64,512]{3,2,1,0:T(8,128)(2,1)}, u32[]{:S(2)}, u32[]{:S(2)}) async-start(bf16[4,16,64,512]{3,2,1,0:T(8,128)(2,1)} %bitcast.157), calls=%async_computation.1 | async-start | bytes 8388608 | tf_op jit(solution)/shard_map/all_to_all | solution.py:460
  262.7 26.8 %reduce-scatter.10.cloned.1.call-start = ((), (), s32[]{:S(2)}) async-start(), calls=%async_computation.6 | async-start | bytes 327680
  264.6 49.3 %reduce-scatter.12.cloned.1.call-start = ((), (), s32[]{:S(2)}) async-start(), calls=%async_computation.7 | async-start | bytes 98304
  (4 other events, 2.4 us)
Sparse Core Ops, SparseCore 0:
  158.0 36.6 reduce-scatter.7
  266.6 22.8 reduce-scatter.9
  292.5 14.7 reduce-scatter.11

commit v2 on v1

--- a/solution.py
+++ b/solution.py
@@ -67,10 +67,85 @@
     return peers
 
 
+def columns_of(rows):
+    return jnp.transpose(rows)
+
+
+def mixer_rows(mx):
+    strength = jax.nn.sigmoid(mx[0:8])
+    pre = mx[8:16]
+    log_decay = -mx[16:17] * (jnp.maximum(pre, 0.0) + jnp.log1p(jnp.exp(-jnp.abs(pre))))
+    lane = lax.broadcasted_iota(jnp.int32, (8, 128), 1)
+    inner = lax.rem(lane, SPAN)
+    total = log_decay
+    for shift in (1, 2, 4, 8, 16, 32):
+        total = total + jnp.where(inner >= shift, pltpu.roll(total, shift, axis=1), 0.0)
+    ends = [
+        jnp.sum(jnp.where(lane == at, total, 0.0), axis=1, keepdims=True) for at in (SPAN - 1, 2 * SPAN - 1)
+    ]
+    last = jnp.where(lane < SPAN, ends[0], ends[1])
+    grown = jnp.exp(total)
+    stacked = jnp.concatenate([strength, total, strength * grown, grown, jnp.exp(last - total)], axis=0)
+    return total, ends, stacked
+
+
+def low_dot(a, b, dims=(((1,), (0,)), ((), ()))):
+    return lax.dot_general(a.astype(BF16), b.astype(BF16), dims, preferred_element_type=F32)
+
+
+def mixer_prepare(b, mq, mk, mv, total, cols, fresh, corr, att, qdec, kdec):
+    at = slice(b * SPAN, (b + 1) * SPAN)
+
+    def both(ref):
+        return jnp.concatenate([ref[at, 0:128], ref[at, 128:256]], axis=0).astype(F32)
+
+    def unit(value):
+        return value * lax.rsqrt(jnp.sum(value * value, axis=-1, keepdims=True) + NORM_FLOOR)
+
+    def column(k):
+        return cols[:, k * 8 + b : k * 8 + b + 1]
+
+    queries, keys, values = unit(both(mq)) * 128 ** (-0.5), unit(both(mk)), both(mv)
+    row, col = lax.broadcasted_iota(jnp.int32, (128, 128), 0), lax.broadcasted_iota(jnp.int32, (128, 128), 1)
+    same = (row // SPAN) == (col // SPAN)
+    spread = jnp.where(same & (row >= col), column(1) - total[b : b + 1, :], -1e30)
+    decay = jnp.exp(spread)
+    strict = jnp.where(same & (row > col), column(0) * low_dot(keys, keys, CONTRACT_LAST) * decay, 0.0)
+    inverse = jnp.where(row == col, 1.0, 0.0) - strict
+    power = strict
+    for _ in range(SPAN.bit_length() - 2):
+        power = low_dot(power, power)
+        inverse = inverse + low_dot(inverse, power)
+    fresh[b] = low_dot(inverse, values * column(0))
+    corr[b] = low_dot(inverse, keys * column(2)).astype(BF16)
+    att[b] = (low_dot(queries, keys, CONTRACT_LAST) * decay).astype(BF16)
+    qdec[b] = (queries * column(3)).astype(BF16)
+    kdec[b] = (keys * column(4)).astype(BF16)
+
+
+def mixer_advance(b, state, cot, ends, fresh, corr, att, qdec, kdec, sums):
+    heads = [slice(0, 64), slice(64, 128)]
+    new = jnp.concatenate(
+        [fresh[b, h, :] - low_dot(corr[b, h, :], state[i]) for i, h in enumerate(heads)], axis=0
+    )
+    out = jnp.concatenate([low_dot(qdec[b, h, :], state[i]) for i, h in enumerate(heads)], axis=0)
+    out = out + low_dot(att[b], new)
+    state = [
+        jnp.exp(ends[i][b : b + 1, :]) * state[i] + low_dot(kdec[b, h, :], new[h], CONTRACT_FIRST)
+        for i, h in enumerate(heads)
+    ]
+    at = slice(b * SPAN, (b + 1) * SPAN)
+    grads = jnp.concatenate([cot[at, 0:128], cot[at, 128:256]], axis=0).astype(F32)
+    lane = lax.broadcasted_iota(jnp.int32, (128, 128), 1)
+    sums = jnp.where(lane == b, jnp.sum(grads * out, axis=-1, keepdims=True), sums)
+    return state, sums
+
+
 def gather_kernel(
-    pas, wk, wv, tok, wq, gw, cot, tbl,
-    kv, qa, ca, tl, klow, qlow, grow,
-    toks, xs, xr, ys, yr, zs, zr, ps, pr, ts, tr,
+    pas, wk, wv, tok, wq, gw, cot, tbl, mq, mk, mv, mx,
+    kv, qa, ca, tl, klow, qlow, gown, wall, gall, md,
+    toks, relay, fresh, corr, att, qdec, kdec,
+    xs, xr, ys, yr, zs, zr, ps, pr, ts, tr, ws, wr, vs, vr, gs, gr,
 ):
     z, y, c, x = place()
     me = z * 2 + c
@@ -79,7 +154,8 @@
     front, back = {"tp": wrap(x + 1, NX)}, {"tp": wrap(x - 1, NX)}
     partner = {"st_2": 1 - c}
     peers = column_peers(z, c)
-    greet(peers + [east, west, front, back])
+    across = {"tp": wrap(x + 2, NX)}
+    greet(peers + [east, west, front, back, across])
     copies = Copies()
     half = 192
     zdirs, ydirs, xdirs = (up, down), (east, west), (front, back)
@@ -198,14 +274,68 @@
             lax.dot_general(gw[:, at], block, CONTRACT_LAST, preferred_element_type=F32),
         )
 
+    weights = (wk, wv, wq)
+    via, behind = {"tp": wrap(x + 1 - 2 * c, NX)}, wrap(x - 1 + 2 * c, NX)
+
+    def w_rows(owner):
+        return pl.ds(pl.multiple_of(owner * 512 + c * 256, 256), 256)
+
+    mine = pl.ds(pl.multiple_of(c * 256, 256), 256)
+
+    def w_send():
+        for i, ref in enumerate(weights):
+            copies.start(ref.at[w_rows(wrap(x + 2, NX)), :], relay.at[i], ws.at[6 + i], wr.at[6 + i], via)
+        for way in (0, 1):
+            to = wrap(x + 1 - 2 * way, NX)
+            for i, ref in enumerate(weights):
+                copies.start(
+                    ref.at[w_rows(to), :], wall.at[i, x, mine, :], ws.at[way * 3 + i], wr.at[way * 3 + i], xdirs[way]
+                )
+        for step, peer in enumerate((front, across, back)):
+            at = pl.ds(pl.multiple_of(wrap(x + 1 + step, NX) * 512, 512), 512)
+            copies.start(gw.at[:, at], gall.at[x], gs.at[step], gr.at[step], peer)
+        own = pl.ds(pl.multiple_of(x * 512, 512), 512)
+        for i, ref in enumerate(weights):
+            wall[i, x] = ref[own, :]
+        gall[x] = gw[:, own]
+
+    def w_forward():
+        for i in range(3):
+            copies.arrived(relay.at[i], ws.at[6 + i], wr.at[6 + i], via)
+            copies.start(relay.at[i], wall.at[i, behind, mine, :], ws.at[9 + i], wr.at[9 + i], via)
+
+    def w_share(n, owner, first):
+        for i in range(3):
+            piece = wall.at[i, owner, mine, :]
+            copies.arrived(piece, ws.at[first + i], wr.at[first + i], via)
+            copies.start(piece, piece, vs.at[n * 3 + i], vr.at[n * 3 + i], partner)
+
+    def w_last():
+        theirs = pl.ds(pl.multiple_of((1 - c) * 256, 256), 256)
+        for n, owner in enumerate((wrap(x - 1, NX), wrap(x + 1, NX), wrap(x + 2, NX))):
+            for i in range(3):
+                copies.arrived(wall.at[i, owner, theirs, :], vs.at[n * 3 + i], vr.at[n * 3 + i], partner)
+        for step, peer in enumerate((front, across, back)):
+            copies.arrived(gall.at[wrap(x - 1 - step, NX)], gs.at[step], gr.at[step], peer)
+
+    total, ends, stacked = mixer_rows(mx[...])
+    cols = columns_of(stacked)
+    work = (fresh, corr, att, qdec, kdec)
+
+    def prepare(b):
+        mixer_prepare(b, mq, mk, mv, total, cols, *work)
+
     z_take(0, ca, 1)
+    prepare(0)
     y_take(0)
     acc = project(x)
     x_take()
+    w_send()
     z_take(0, ca, 2)
     for owner in (wrap(x - 1, NX), wrap(x + 1, NX)):
         more = project(owner)
         acc = (acc[0] + more[0], acc[1] + more[1])
+    prepare(1)
     y_take(1)
     x_last()
     more = project(wrap(x + 2, NX))
@@ -217,20 +347,35 @@
     qa[me] = (wide * scale).astype(BF16)
     own_send(1, qa)
     z_take(0, ca, 3)
-    grow[...] = gate[0:8]
     tl[me] = jnp.zeros((8, 128), F32)
     for b in range(6):
         tl[me, b : b + 1, 0:64] = gate[0:1, b * 64 : b * 64 + 64]
     tl[me, 6:7, 0:64] = tbl[...]
     for step, peer in enumerate(peers):
         copies.start(tl.at[me], tl.at[me], ts.at[step], tr.at[step], peer)
+    gown[...] = tl[me]
     y_take(2)
+    prepare(2)
     z_take(1, qa, 1)
+    w_forward()
+    prepare(3)
     y_take(3)
     z_take(1, qa, 2)
+    prepare(4)
+    w_share(0, wrap(x - 1, NX), 0)
+    w_share(1, wrap(x + 1, NX), 3)
     z_take(0, ca, 4)
+    prepare(5)
     z_take(1, qa, 3)
+    w_share(2, wrap(x + 2, NX), 9)
+    state = [jnp.zeros((128, 128), F32), jnp.zeros((128, 128), F32)]
+    sums = jnp.zeros((128, 128), F32)
+    for b in range(6):
+        state, sums = mixer_advance(b, state, cot, ends, *work, sums)
+    turned = jnp.transpose(sums)[0:8]
+    md[...] = turned[:, 0:64] + turned[:, 64:128]
     z_take(1, qa, 4)
+    w_last()
     for step in range(2 * NZ - 1):
         other = wrap(me - (step + 1), 2 * NZ)
         copies.arrived(tl.at[other], ts.at[step], tr.at[step], peers[step])
@@ -319,110 +464,277 @@
                 at, slot = r * 6 + b, yy * 16 + loc
                 key = gain * jnp.dot(slope, qa[at], preferred_element_type=F32)
                 value = jnp.dot(gated, ca[at], preferred_element_type=F32)
-                kacc[slot, :, 0:256] += key.astype(BF16).astype(F32)
-                kacc[slot, :, 256:512] += value.astype(BF16).astype(F32)
+                kacc[0, slot] += key.astype(BF16).astype(F32)
+                kacc[1, slot] += value.astype(BF16).astype(F32)
                 qacc[at] += gain * lax.dot_general(
                     slope, kv[slot, :, 0:256], CONTRACT_FIRST, preferred_element_type=F32
                 )
 
     @pl.loop(0, 64)
     def _(i):
-        kvg[i] = kacc[i].astype(BF16)
+        kvg[0, i] = kacc[0, i].astype(BF16)
+        kvg[1, i] = kacc[1, i].astype(BF16)
 
     @pl.loop(0, 96)
     def _(i):
         qp[i] = qacc[i].astype(BF16)
 
 
-def return_kernel(kvg, qp, kvs, qg, ybuf, ysum, px, qs, zbuf, ys, yr, zs, zr, ps, pr):
+def finish_kernel(
+    kvg, qp, klow, pas, qlow, wall, gall, own, md, gown,
+    tgrad, pgrad, wgrad,
+    ybuf, ysum, px, qs, zbuf, xall, pacc, xq, ggx, whalf, wget, wz, wbuf, wsum, wlast,
+    ys, yr, zs, zr, ps, pr, xs, xr, qxs, qxr, gs, gr, us, ur, vs, vr, ls, lr,
+):
     z, y, c, x = place()
     up, down = {"st_0": wrap(z + 1, NZ)}, {"st_0": wrap(z - 1, NZ)}
     east, west = {"st_1": wrap(y + 1, NY)}, {"st_1": wrap(y - 1, NY)}
+    front, back, across = {"tp": wrap(x + 1, NX)}, {"tp": wrap(x - 1, NX)}, {"tp": wrap(x + 2, NX)}
     partner = {"st_2": 1 - c}
-    greet([up, down, east, west, partner])
+    spot = y * 2 + c
+    plane = []
+    for step in range(1, 8):
+        other = wrap(spot + step, 8)
+        plane.append({"st_1": other // 2, "st_2": lax.rem(other, 2)})
+    greet([up, down, front, back, across] + plane)
     copies = Copies()
-    zdirs, ydirs = (up, down), (east, west)
-    half = 192
-    order = [4, 3, 5, 2, 6, 1, 7, 0]
-    for k in order:
+    zdirs, ydirs, xdirs = (up, down), (east, west), (front, back)
+
+    for k in (4, 3, 5, 2, 6, 1, 7, 0):
         there = wrap(z + k, NZ)
         copies.start(qp.at[there * 2 + 1 - c], px.at[there], ps.at[k], pr.at[k], partner)
-    part, sub = 512, 256
+
     far, beside = wrap(y + 2, NY), (wrap(y + 1, NY), wrap(y - 1, NY))
-    for j in (0, 1):
-        for way in (0, 1):
-            at = pl.ds(way * part + j * sub, sub)
-            copies.start(kvg.at[far, at, :], ybuf.at[way, pl.ds(j * sub, sub), :], ys.at[way, j], yr.at[way, j], ydirs[way])
-    for way in (0, 1):
-        at = pl.ds((1 - way) * part, part)
-        copies.start(kvg.at[beside[way], at, :], ysum.at[way, at, :], ys.at[way, 4], yr.at[way, 4], ydirs[way])
+
+    def y_rows(j, part):
+        return j // 2, pl.ds((j % 2) * 512 + part * 256, 256)
+
+    def y_open(j):
+        for way in (0, 1):
+            p, at = y_rows(j, way)
+            copies.start(kvg.at[p, far, at, :], ybuf.at[way, j], ys.at[0, way, j], yr.at[0, way, j], ydirs[way])
+        for way in (0, 1):
+            p, at = y_rows(j, 1 - way)
+            copies.start(
+                kvg.at[p, beside[way], at, :], ysum.at[way, p, at, :], ys.at[1, way, j], yr.at[1, way, j], ydirs[way]
+            )
+
+    def y_add(j):
+        for way in (0, 1):
+            p, at = y_rows(j, way)
+            copies.arrived(ybuf.at[way, j], ys.at[0, way, j], yr.at[0, way, j], ydirs[way])
+            ybuf[way, j] = (kvg[p, beside[way], at, :].astype(F32) + ybuf[way, j].astype(F32)).astype(BF16)
+            copies.start(ybuf.at[way, j], ysum.at[way, p, at, :], ys.at[2, way, j], yr.at[2, way, j], ydirs[way])
+        if j < 3:
+            y_open(j + 1)
+
+    def x_pieces(j, h):
+        return j // 2, pl.ds((j % 2) * 512 + h * 256, 256)
+
+    def y_done(j):
+        for way in (0, 1):
+            p, at = y_rows(j, 1 - way)
+            copies.arrived(ysum.at[way, p, at, :], ys.at[1, way, j], yr.at[1, way, j], ydirs[way])
+            p, at = y_rows(j, way)
+            copies.arrived(ysum.at[way, p, at, :], ys.at[2, way, j], yr.at[2, way, j], ydirs[way])
+        for h in (0, 1):
+            p, at = x_pieces(j, h)
+            grad = kvg[p, y, at, :].astype(F32) + ysum[0, p, at, :].astype(F32) + ysum[1, p, at, :].astype(F32)
+            if p == 0:
+                wide = klow[at, :].astype(F32)
+                scale = lax.rsqrt(jnp.mean(wide * wide, axis=-1, keepdims=True) + NORM_FLOOR)
+                inner = jnp.mean(wide * grad, axis=-1, keepdims=True)
+                grad = scale * grad - (scale * scale * scale * inner) * wide
+            xall[x, p, at, :] = grad.astype(BF16)
+            for way in (0, 1):
+                piece = xall.at[x, p, at, :]
+                copies.start(piece, piece, xs.at[j, way, h], xr.at[j, way, h], xdirs[way])
+
+    def x_take(j):
+        for way in (0, 1):
+            owner = wrap(x - 1 + 2 * way, NX)
+            for h in (0, 1):
+                p, at = x_pieces(j, h)
+                piece = xall.at[owner, p, at, :]
+                copies.arrived(piece, xs.at[j, way, h], xr.at[j, way, h], xdirs[way])
+                if h == way:
+                    copies.start(piece, piece, xs.at[j, way, 2], xr.at[j, way, 2], xdirs[way])
+
+    def x_last(j):
+        owner = wrap(x + 2, NX)
+        for way in (0, 1):
+            p, at = x_pieces(j, way)
+            copies.arrived(xall.at[owner, p, at, :], xs.at[j, way, 2], xr.at[j, way, 2], xdirs[way])
+        p = j // 2
+
+        @pl.loop(0, 4)
+        def _(i):
+            at = pl.ds(pl.multiple_of((j % 2) * 512 + i * 128, 128), 128)
+            term = lax.dot_general(xall[0, p, at, :], wall[p, 0], CONTRACT_LAST, preferred_element_type=F32)
+            for h in range(1, NX):
+                term += lax.dot_general(xall[h, p, at, :], wall[p, h], CONTRACT_LAST, preferred_element_type=F32)
+            if p == 0:
+                pacc[at, :] = term
+            else:
+                pgrad[at, :] = (pacc[at, :] + term).astype(BF16)
+
+    def ring_step(d, value, slots, send, recv, half):
+        for way in (0, 1):
+            there = wrap(z + d, NZ) if way == 0 else wrap(z - d, NZ)
+            at = pl.ds(way * half, half)
+            if d == 3:
+                copies.arrived(slots.at[way, 0, at, :], send.at[way, 3], recv.at[way, 3], zdirs[way])
+                value[there, at, :] = (value[there, at, :].astype(F32) + slots[way, 0, at, :].astype(F32)).astype(BF16)
+            elif d < 3:
+                copies.arrived(slots.at[way, 3 - d], send.at[way, d], recv.at[way, d], zdirs[way])
+                value[there] = (value[there].astype(F32) + slots[way, 3 - d].astype(F32)).astype(BF16)
+            if d == 4:
+                copies.start(value.at[there, at, :], slots.at[way, 0, at, :], send.at[way, 3], recv.at[way, 3], zdirs[way])
+            else:
+                copies.start(value.at[there], slots.at[way, 4 - d], send.at[way, d - 1], recv.at[way, d - 1], zdirs[way])
+
+    def ring_last(value, slots, send, recv):
+        result = value[z].astype(F32)
+        for way in (0, 1):
+            copies.arrived(slots.at[way, 3], send.at[way, 0], recv.at[way, 0], zdirs[way])
+            result = result + slots[way, 3].astype(F32)
+        return result
 
     def q_pair(k):
         there = wrap(z + k, NZ)
         copies.arrived(px.at[there], ps.at[k], pr.at[k], partner)
         qs[there] = (qp[there * 2 + c].astype(F32) + px[there].astype(F32)).astype(BF16)
 
-    def y_add(j):
-        for way in (0, 1):
-            copies.arrived(ybuf.at[way, pl.ds(j * sub, sub), :], ys.at[way, j], yr.at[way, j], ydirs[way])
-            at = pl.ds(way * part + j * sub, sub)
-            mine = kvg[beside[way], at, :].astype(F32)
-            ybuf[way, pl.ds(j * sub, sub), :] = (
-                mine + ybuf[way, pl.ds(j * sub, sub), :].astype(F32)
-            ).astype(BF16)
-            copies.start(
-                ybuf.at[way, pl.ds(j * sub, sub), :], ysum.at[way, at, :], ys.at[way, 2 + j], yr.at[way, 2 + j], ydirs[way]
+    def q_step(d):
+        ring_step(d, qs, zbuf, zs, zr, 192)
+
+    def q_done():
+        grad = ring_last(qs, zbuf, zs, zr)
+        wide = qlow[...].astype(F32)
+        scale = lax.rsqrt(jnp.mean(wide * wide, axis=-1, keepdims=True) + NORM_FLOOR)
+        inner = jnp.mean(wide * grad, axis=-1, keepdims=True)
+        xq[x] = (scale * grad - (scale * scale * scale * inner) * wide).astype(BF16)
+        for way in (0, 1):
+            for h in (0, 1):
+                piece = xq.at[x, pl.ds(h * 192, 192), :]
+                copies.start(piece, piece, qxs.at[way, h], qxr.at[way, h], xdirs[way])
+
+    def gates():
+        gate = gown[0:6, 0:64]
+        dots = own[0:6, 64:128] / own[0:6, 0:64]
+        ggx[x] = jnp.zeros((8, 128), F32)
+        ggx[x, 0:6, 0:64] = (1.0 - gate) * (dots - gate * md[0:6, :])
+        for step, peer in enumerate((front, across, back)):
+            copies.start(ggx.at[x], ggx.at[x], gs.at[step], gr.at[step], peer)
+
+    def q_take():
+        for way in (0, 1):
+            owner = wrap(x - 1 + 2 * way, NX)
+            for h in (0, 1):
+                piece = xq.at[owner, pl.ds(h * 192, 192), :]
+                copies.arrived(piece, qxs.at[way, h], qxr.at[way, h], xdirs[way])
+                if h == way:
+                    copies.start(piece, piece, qxs.at[way, 2], qxr.at[way, 2], xdirs[way])
+
+    def q_last():
+        owner = wrap(x + 2, NX)
+        for way in (0, 1):
+            copies.arrived(xq.at[owner, pl.ds(way * 192, 192), :], qxs.at[way, 2], qxr.at[way, 2], xdirs[way])
+        for step, peer in enumerate((front, across, back)):
+            copies.arrived(ggx.at[wrap(x - 1 - step, NX)], gs.at[step], gr.at[step], peer)
+        blank = [jnp.zeros((4, 64), F32)]
+        slope = jnp.concatenate(
+            [gall[h, 0:1, :].astype(F32) for h in range(NX)] + [jnp.zeros((4, 512), F32)], axis=0
+        )
+        for b in range(6):
+            at = pl.ds(b * 64, 64)
+            rows = jnp.concatenate([ggx[h, b : b + 1, 0:64] for h in range(NX)] + blank, axis=0)
+            term = lax.dot_general(
+                rows, slope, CONTRACT_FIRST, preferred_element_type=F32, precision=lax.Precision.HIGHEST
             )
-
-    def z_step(d):
-        for way in (0, 1):
-            there = wrap(z + d, NZ) if way == 0 else wrap(z - d, NZ)
-            if d == 3:
-                piece = zbuf.at[way, 0, pl.ds(way * half, half), :]
-                copies.arrived(piece, zs.at[way, 3], zr.at[way, 3], zdirs[way])
-                at = pl.ds(way * half, half)
-                qs[there, at, :] = (
-                    qs[there, at, :].astype(F32) + zbuf[way, 0, at, :].astype(F32)
-                ).astype(BF16)
-            elif d < 3:
-                piece = zbuf.at[way, 3 - d]
-                copies.arrived(piece, zs.at[way, d], zr.at[way, d], zdirs[way])
-                qs[there] = (qs[there].astype(F32) + zbuf[way, 3 - d].astype(F32)).astype(BF16)
-            if d == 4:
-                at = pl.ds(way * half, half)
-                copies.start(qs.at[there, at, :], zbuf.at[way, 0, at, :], zs.at[way, 3], zr.at[way, 3], zdirs[way])
-            else:
-                copies.start(qs.at[there], zbuf.at[way, 4 - d], zs.at[way, d - 1], zr.at[way, d - 1], zdirs[way])
-
+            for h in range(NX):
+                term += lax.dot_general(xq[h, at, :], wall[2, h], CONTRACT_LAST, preferred_element_type=F32)
+            tgrad[at, :] = term.astype(BF16)
+
+    keep = pl.ds(pl.multiple_of(c * 128, 128), 128)
+    give = pl.ds(pl.multiple_of((1 - c) * 128, 128), 128)
+
+    def w_tile(k):
+        there = wrap(z + k, NZ)
+        at = pl.ds(pl.multiple_of(there * 256, 256), 256)
+        wsum[there] = lax.dot_general(
+            pas[:, at], xall[x, 0], CONTRACT_FIRST, preferred_element_type=F32
+        )
+        whalf[there] = wsum[there, :, give]
+        copies.start(whalf.at[there], wget.at[there], us.at[k], ur.at[k], partner)
+
+    def w_pair(k):
+        there = wrap(z + k, NZ)
+        copies.arrived(wget.at[there], us.at[k], ur.at[k], partner)
+        wz[there] = (wsum[there, :, keep] + wget[there]).astype(BF16)
+
+    def w_step(d):
+        ring_step(d, wz, wbuf, vs, vr, 128)
+
+    def w_done():
+        wsum[z, :, 0:128] = ring_last(wz, wbuf, vs, vr)
+        for step, peer in enumerate(plane):
+            other = wrap(spot + step + 1, 8)
+            piece = wsum.at[z, pl.ds(pl.multiple_of(other * 32, 32), 32), pl.ds(0, 128)]
+            copies.start(piece, wlast.at[spot], ls.at[step], lr.at[step], peer)
+        wlast[spot] = wsum[z, pl.ds(pl.multiple_of(spot * 32, 32), 32), 0:128]
+
+    def w_last():
+        for step, peer in enumerate(plane):
+            copies.arrived(wlast.at[wrap(spot - step - 1, 8)], ls.at[step], lr.at[step], peer)
+        for k in (0, 1):
+            wgrad[:, k * 128 : k * 128 + 128] = wlast[k] + wlast[2 + k] + wlast[4 + k] + wlast[6 + k]
+
+    y_open(0)
     q_pair(4)
-    z_step(4)
-    q_pair(3)
-    q_pair(5)
-    q_pair(2)
-    q_pair(6)
-    z_step(3)
-    q_pair(1)
-    q_pair(7)
-    q_pair(0)
+    q_step(4)
+    for k in (3, 5):
+        q_pair(k)
     y_add(0)
-    z_step(2)
+    q_step(3)
+    for k in (2, 6, 1, 7, 0):
+        q_pair(k)
+    gates()
+    y_done(0)
+    q_step(2)
     y_add(1)
-    z_step(1)
-    grad = qs[z].astype(F32)
-    for way in (0, 1):
-        copies.arrived(zbuf.at[way, 3], zs.at[way, 0], zr.at[way, 0], zdirs[way])
-        grad = grad + zbuf[way, 3].astype(F32)
-    qg[...] = grad
-    for way in (0, 1):
-        at = pl.ds((1 - way) * part, part)
-        copies.arrived(ysum.at[way, at, :], ys.at[way, 4], yr.at[way, 4], ydirs[way])
-    for way in (0, 1):
-        for j in (0, 1):
-            at = pl.ds(way * part + j * sub, sub)
-            copies.arrived(ysum.at[way, at, :], ys.at[way, 2 + j], yr.at[way, 2 + j], ydirs[way])
-    for i in range(4):
-        at = pl.ds(i * 256, 256)
-        kvs[at, :] = kvg[y, at, :].astype(F32) + ysum[0, at, :].astype(F32) + ysum[1, at, :].astype(F32)
+    q_step(1)
+    x_take(0)
+    y_done(1)
+    for k in (4, 3, 5):
+        w_tile(k)
+    y_add(2)
+    q_done()
+    for k in (2, 6, 1, 7, 0):
+        w_tile(k)
+    x_take(1)
+    y_done(2)
+    w_pair(4)
+    w_step(4)
+    y_add(3)
+    x_last(0)
+    w_pair(3)
+    w_pair(5)
+    w_step(3)
+    q_take()
+    for k in (2, 6, 1, 7, 0):
+        w_pair(k)
+    w_step(2)
+    x_take(2)
+    x_last(1)
+    y_done(3)
+    w_step(1)
+    q_last()
+    w_done()
+    x_take(3)
+    x_last(2)
+    w_last()
+    x_last(3)
     copies.finish()
 
 
@@ -450,107 +762,6 @@
     )
 
 
-def in_blocks(shard, dim, devices):
-    before, after = (shard.shape[:dim], shard.shape[dim + 1 :])
-    return jnp.moveaxis(shard.reshape(*before, devices, -1, *after), dim, 0)
-
-
-def sum_at_owner(shard, axis, dim):
-    parts = in_blocks(shard, dim, lax.axis_size(axis))
-    arrived = lax.all_to_all(parts, axis, split_axis=0, concat_axis=0, tiled=True)
-    return arrived.astype(jnp.float32).sum(axis=0)
-
-
-def sum_by_axis(shard, axes, dim):
-    for axis in axes:
-        shard = lax.psum_scatter(shard, axis, scatter_dimension=dim, tiled=True)
-    return shard
-
-
-def neumann_inverse(strict_part):
-    span_size = strict_part.shape[-1]
-    unit_eye = jnp.eye(span_size, dtype=jnp.float32)
-    running = unit_eye - strict_part
-    power_term = strict_part
-    for _ in range(span_size.bit_length() - 2):
-        power_term = jnp.einsum("...ij,...jk->...ik", power_term, power_term)
-        running = jnp.einsum("...ij,...jk->...ik", running, unit_eye + power_term)
-    return running
-
-
-def delta_mixer(queries, keys_in, values_in, strength, log_decay):
-    heads_n, length, key_dim = queries.shape
-    blocks_n = length // SPAN
-
-    def to_blocks(tensor):
-        return tensor.reshape(heads_n, blocks_n, SPAN, *tensor.shape[2:])
-
-    queries, keys_in, values_in = (to_blocks(queries), to_blocks(keys_in), to_blocks(values_in))
-    strength, log_decay = (to_blocks(strength), to_blocks(log_decay))
-    cumulative = jnp.cumsum(log_decay, axis=-1)
-    position = jnp.arange(SPAN)
-    inclusive = position[:, None] >= position[None, :]
-    strictly = position[:, None] > position[None, :]
-    spread = jnp.where(inclusive, cumulative[..., :, None] - cumulative[..., None, :], -jnp.inf)
-    decay_map = jnp.exp(spread)
-    key_gram = jnp.einsum("hncd,hnmd->hncm", keys_in, keys_in)
-    strict_part = jnp.where(strictly, strength[..., :, None] * key_gram * decay_map, 0.0)
-    inverse = neumann_inverse(strict_part)
-    fresh_vals = jnp.einsum("hncm,hnme->hnce", inverse, values_in * strength[..., None])
-    correction = jnp.einsum(
-        "hncm,hnmd->hncd", inverse, keys_in * (strength * jnp.exp(cumulative))[..., None]
-    )
-    attend_map = jnp.where(
-        inclusive, jnp.einsum("hncd,hnmd->hncm", queries, keys_in) * decay_map, 0.0
-    )
-    query_dec = queries * jnp.exp(cumulative)[..., None]
-    key_dec = keys_in * jnp.exp(cumulative[..., -1:] - cumulative)[..., None]
-    carry_decay = jnp.exp(cumulative[..., -1])
-
-    def advance(memory_state, inputs):
-        fresh_blk, correct_blk, attend_blk, query_blk, key_blk, decay_blk = inputs
-        new_values = fresh_blk - jnp.einsum("hcd,hde->hce", correct_blk, memory_state)
-        output = jnp.einsum("hcd,hde->hce", query_blk, memory_state) + jnp.einsum(
-            "hcm,hme->hce", attend_blk, new_values
-        )
-        memory_state = memory_state * decay_blk[:, None, None] + jnp.einsum(
-            "hcd,hce->hde", key_blk, new_values
-        )
-        return (memory_state, output)
-
-    stacked = tuple(
-        (
-            jnp.moveaxis(tensor, 1, 0)
-            for tensor in (fresh_vals, correction, attend_map, query_dec, key_dec, carry_decay)
-        )
-    )
-    initial = jnp.zeros((heads_n, key_dim, values_in.shape[-1]), jnp.float32)
-    _, outputs = lax.scan(advance, initial, stacked)
-    return jnp.transpose(outputs, (1, 0, 2, 3)).reshape(heads_n, length, -1)
-
-
-def mixer_output(query_raw, key_raw, value_raw, beta_raw, decay_raw, rate_vals):
-    length = query_raw.shape[0]
-    heads_n = beta_raw.shape[0]
-
-    def heads_first(matrix):
-        return jnp.transpose(matrix.astype(jnp.float32).reshape(length, heads_n, -1), (1, 0, 2))
-
-    queries = heads_first(query_raw)
-    keys_in = heads_first(key_raw)
-    values_in = heads_first(value_raw)
-    queries = (
-        queries
-        * lax.rsqrt(jnp.sum(queries * queries, axis=-1, keepdims=True) + NORM_FLOOR)
-        * queries.shape[-1] ** (-0.5)
-    )
-    keys_in = keys_in * lax.rsqrt(jnp.sum(keys_in * keys_in, axis=-1, keepdims=True) + NORM_FLOOR)
-    strength = jax.nn.sigmoid(beta_raw)
-    log_decay = -rate_vals[:, None] * jax.nn.softplus(decay_raw)
-    mixer_out = delta_mixer(queries, keys_in, values_in, strength, log_decay)
-    return jnp.transpose(mixer_out, (1, 0, 2)).reshape(length, -1)
-
-
 def body(
     tokens, cotangent, mix_query, mix_key, mix_value, beta_pre, decay_pre, decay_rate,
     passages, passage_ids, query_weight, key_weight, value_weight, gate_weight,
@@ -562,19 +773,30 @@
     wanted = (ids // 16)[:, None] == jnp.arange(64, dtype=jnp.int32)[None, :]
     table = jnp.max(jnp.where(wanted, place_of[:, None], -1), axis=0).astype(F32)[None, :]
     gate_rows = jnp.broadcast_to(gate_weight, (16, model_width))
-    kv, qa, ca, tl, key_low, query_low, gate_row = call(
+
+    def by_block(rows):
+        return jnp.pad(rows.reshape(2, 6, 64).transpose(1, 0, 2).reshape(6, 128), ((0, 2), (0, 0)))
+
+    rates = jnp.broadcast_to(jnp.repeat(decay_rate, 64)[None, :], (8, 128))
+    scalars = jnp.concatenate([by_block(beta_pre), by_block(decay_pre), rates], axis=0)
+    kv, qa, ca, tl, key_low, query_low, gown, wall, gall, md = call(
         gather_kernel,
         [
             shaped((NY, 1024, 512), BF16), shaped((16, 384, 256), BF16), shaped((16, 384, 256), BF16),
-            shaped((16, 8, 128), F32), shaped((1024, 256), BF16), shaped((384, 256), BF16), shaped((8, 384), F32),
+            shaped((16, 8, 128), F32), shaped((1024, 256), BF16), shaped((384, 256), BF16), shaped((8, 128), F32),
+            shaped((3, NX, 512, 256), BF16), shaped((NX, 16, 512), BF16), shaped((8, 64), F32),
         ],
         [
-            VMEM((NX, 384, 512), BF16), dma(2, 3), dma(2, 3), dma(2, 6), dma(2, 6), dma(2, 2, 7), dma(2, 2, 7),
-            dma(2, 16), dma(2, 16), dma(15), dma(15),
+            VMEM((NX, 384, 512), BF16), VMEM((3, 256, 256), BF16), VMEM((6, 128, 128), F32),
+            VMEM((6, 128, 128), BF16), VMEM((6, 128, 128), BF16), VMEM((6, 128, 128), BF16), VMEM((6, 128, 128), BF16),
+            dma(2, 3), dma(2, 3), dma(2, 6), dma(2, 6), dma(2, 2, 7), dma(2, 2, 7),
+            dma(2, 16), dma(2, 16), dma(15), dma(15), dma(12), dma(12), dma(9), dma(9), dma(3), dma(3),
         ],
-        1, count=8,
-    )(flat_rows, key_weight, value_weight, tokens, query_weight, gate_rows, cotangent, table)
-    mixer_out = mixer_output(mix_query, mix_key, mix_value, beta_pre, decay_pre, decay_rate)
+        1, count=12,
+    )(
+        flat_rows, key_weight, value_weight, tokens, query_weight, gate_rows, cotangent, table,
+        mix_query, mix_key, mix_value, scalars,
+    )
     lookup = tl[:, 6, 0:64].astype(jnp.int32)
     kv_one, qa_one, ca_one = kv.reshape(64, 64, 512), qa.reshape(96, 64, 256), ca.reshape(96, 64, 256)
     eg, tot, own = call(
@@ -588,53 +810,28 @@
     )(lookup, kv_one, qa_one, ca_one, tl)
     kvg, qp = call(
         grads_kernel,
-        [shaped((64, 64, 512), BF16), shaped((96, 64, 256), BF16)],
-        [VMEM((64, 64, 512), F32), VMEM((96, 64, 256), F32)],
+        [shaped((2, 64, 64, 256), BF16), shaped((96, 64, 256), BF16)],
+        [VMEM((2, 64, 64, 256), F32), VMEM((96, 64, 256), F32)],
         None, smem=1, count=7,
     )(lookup, kv_one, qa_one, ca_one, tl, eg, tot)
-    kvs, qhat_grad = call(
-        return_kernel,
-        [shaped((1024, 512), F32), shaped((384, 256), F32)],
+    token_grad, passage_grad, key_weight_grad = call(
+        finish_kernel,
+        [shaped((384, 512), BF16), shaped((1024, 512), BF16), shaped((32, 256), F32)],
         [
-            VMEM((2, 512, 512), BF16), VMEM((2, 1024, 512), BF16), VMEM((NZ, 384, 256), BF16),
-            VMEM((NZ, 384, 256), BF16), VMEM((2, 4, 384, 256), BF16),
-            dma(2, 5), dma(2, 5), dma(2, 4), dma(2, 4), dma(8), dma(8),
+            VMEM((2, 4, 256, 256), BF16), VMEM((2, 2, 1024, 256), BF16), VMEM((NZ, 384, 256), BF16),
+            VMEM((NZ, 384, 256), BF16), VMEM((2, 4, 384, 256), BF16), VMEM((NX, 2, 1024, 256), BF16),
+            VMEM((1024, 512), F32), VMEM((NX, 384, 256), BF16), VMEM((NX, 8, 128), F32),
+            VMEM((NZ, 256, 128), F32), VMEM((NZ, 256, 128), F32), VMEM((NZ, 256, 128), BF16),
+            VMEM((2, 4, 256, 128), BF16), VMEM((NZ, 256, 256), F32), VMEM((8, 32, 128), F32),
+            dma(3, 2, 4), dma(3, 2, 4), dma(2, 4), dma(2, 4), dma(8), dma(8), dma(4, 2, 3), dma(4, 2, 3),
+            dma(2, 3), dma(2, 3), dma(3), dma(3), dma(8), dma(8), dma(2, 4), dma(2, 4), dma(7), dma(7),
         ],
-        3, count=2,
-    )(kvg.reshape(NY, 1024, 512), qp.reshape(16, 384, 256))
-
-    query_float = query_low.astype(F32)
-    query_scale = lax.rsqrt(jnp.mean(query_float * query_float, axis=-1, keepdims=True) + NORM_FLOOR)
-    key_float = key_low.astype(F32)
-    key_scale = lax.rsqrt(jnp.mean(key_float * key_float, axis=-1, keepdims=True) + NORM_FLOOR)
-    gate_open = gate_row[0]
-    dots = (own[0:6, 64:128] / own[0:6, 0:64]).reshape(384)
-    grad_out = cotangent.astype(F32)
-    gate_grad = (1.0 - gate_open) * (dots - gate_open * jnp.sum(grad_out * mixer_out, axis=-1))
-    query_grad = (
-        query_scale * qhat_grad
-        - query_scale**3 * query_float * jnp.mean(query_float * qhat_grad, axis=-1, keepdims=True)
-    ).astype(BF16)
-    token_term = (
-        lax.dot_general(query_grad, query_weight, CONTRACT_LAST, preferred_element_type=F32)
-        + gate_grad[:, None] * gate_weight[0].astype(F32)[None, :]
+        3, count=10,
+    )(
+        kvg.reshape(2, NY, 1024, 256), qp.reshape(16, 384, 256), key_low, flat_rows, query_low,
+        wall, gall, own, md, gown,
     )
-    token_grad = sum_at_owner(token_term.astype(BF16), "tp", 1).astype(BF16)
-    key_hat_grad, value_grad = kvs[:, 0:256], kvs[:, 256:512]
-    key_grad = (
-        key_scale * key_hat_grad
-        - key_scale**3 * key_float * jnp.mean(key_float * key_hat_grad, axis=-1, keepdims=True)
-    ).astype(BF16)
-    value_grad_low = value_grad.astype(BF16)
-    row_term = lax.dot_general(
-        key_grad, key_weight, CONTRACT_LAST, preferred_element_type=F32
-    ) + lax.dot_general(value_grad_low, value_weight, CONTRACT_LAST, preferred_element_type=F32)
-    passage_grad = sum_at_owner(
-        row_term.reshape(pass_local, span_rows, model_width).astype(BF16), "tp", 2
-    ).astype(BF16)
-    weight_term = lax.dot_general(flat_rows, key_grad, CONTRACT_FIRST, preferred_element_type=F32)
-    key_weight_grad = sum_by_axis(weight_term, ST, 0)
-    return (token_grad, passage_grad, key_weight_grad)
+    return (token_grad, passage_grad.reshape(pass_local, span_rows, 512), key_weight_grad)
 
 
 def solution(mesh):

time: 326 us -> 186 us (0.57); the launches traced: 320 us -> 185 us
  matrix products: 51.2 us -> 0 us
  waiting for transfers between devices: 43.1 us -> 0 us
  Pallas kernels: 138 us -> 168 us
  local copies, waits for them, and re-layouts: 46 us -> 16 us
  other arithmetic: 18.9 us -> 0.85 us
  between operations: 14.1 us -> 0.71 us
  starting transfers between devices: 9.55 us -> 0 us
    dot_general x39 -> x0, matrix products: 51.2 us -> none  [the longest x6 9.18 us: advance(): jnp.einsum('hcm,hme->hce', attend_blk, new_values)]
    pallas_call x2, Pallas kernels: 58.1 us -> 86.8 us  [the longest x1 69.4 us: body(): call(finish_kernel, [shaped((384, 512), BF16), shaped((1024, 512), BF16),...]
    unnamed x5 -> x0, waiting for transfers between devices: 24.9 us -> none
    all_to_all x2 -> x0, waiting for transfers between devices: 18.2 us -> none  [sum_at_owner(): lax.all_to_all(parts, axis, split_axis=0, concat_axis=0, tiled=True)]
    convert_element_type x2 -> x0, local copies, waits for them, and re-layouts: 12.9 us -> none  [body(): row_term.reshape(pass_local, span_rows, model_width).astype(BF16)]
    all_to_all x2 -> x0, starting transfers between devices: 9.43 us -> none  [sum_at_owner(): lax.all_to_all(parts, axis, split_axis=0, concat_axis=0, tiled=True)]
    reduce_sum x7 -> x0, other arithmetic: 8.45 us -> none  [the longest x2 6.74 us: sum_at_owner(): return arrived.astype(jnp.float32).sum(axis=0)]
    mul x9 -> x0, local copies, waits for them, and re-layouts: 8.07 us -> none  [the longest x6 4.17 us: advance(): memory_state * decay_blk[:, None, None]]
  transfers between devices with their start and end apart: 5 -> 0, of which waited for: 3 -> 0; matrix products, arithmetic and copies ran while one was open for 31% -> 0% of each run, Pallas kernels for 0% -> 0%
where the time goes in v2:
time: 186 us; the launch traced here: 185 us
  Pallas kernels  168 us (90%)
  local copies, waits for them, and re-layouts  16 us (9%)
    pallas_call x1, Pallas kernels, body(): call(finish_kernel, [shaped((384, 512), BF16), shaped((1024, 512), BF16),...  69.4 us
    pallas_call x1, Pallas kernels, body(): call(gather_kernel, [shaped((NY, 1024, 512), BF16), shaped((16, 384, 256)...  59.7 us
    pallas_call x1, Pallas kernels, body(): call(score_kernel, [shaped((64, 64, 128), F32), shaped((16, 8, 128), F32)...  21.4 us
    pallas_call x1, Pallas kernels, body(): call(grads_kernel, [shaped((2, 64, 64, 256), BF16), shaped((96, 64, 256),...  17.3 us
    unnamed x22, local copies, waits for them, and re-layouts  13.4 us

profile of v2, /device:TPU:1, one launch (start us, length us, event | category | flops | bytes accessed | tf_op | source)
XLA Modules:
  0.0 185.4 jit_solution(14631880593475154932)
XLA Ops:
  0.6 0.7 broadcast_in_dim.37
  1.4 0.1 broadcast_in_dim.38
  1.4 0.8 copy.25
  2.3 0.1 select_reduce_fusion
  2.4 0.7 reduce
  3.1 0.8 reshape.108
  3.9 0.1 reshape.109
  4.0 0.8 reshape.110
  4.9 1.2 copy-done.1
  6.1 1.2 copy-done.2
  7.3 1.2 copy-done.3
  8.5 1.0 copy-done.4
  9.5 0.9 copy-done.5
  10.5 0.9 copy-done.6
  11.4 0.9 copy-done.7
  12.3 0.9 copy-done.8
  13.2 59.7 %shard_map.157 = (bf16[4,1024,512]{2,1,0:T(8,128)(2,1)}, bf16[16,384,256]{2,1,0:T(8,128)(2,1)}, bf16[16,384,256]{2,1,0:T(8,128)(2,1)}, f32[16,8,128]{2,1,0:T(8,1...) custom-call(bf16[1024,2048]{1,0:T(8,128)(2,1)} %bitcast.17, ...), custom_call_target="tpu_custom_call" | custom-call | tf_op jit(solution)/shard_map/pallas_call | solution.py:782
  73.0 1.9 %copy-done = bf16[16,384,256]{2,1,0:T(8,128)(2,1)S(1)} copy-done((bf16[16,384,256]{2,1,0:T(8,128)(2,1)S(1)}, bf16[16,384,256]{2,1,0:T(8,128)(2,1)}, u32[]{:S(2)}) %copy-start) | copy-done | bytes 3145752
  74.9 21.4 %shard_map.158 = (f32[64,64,128]{2,1,0:T(8,128)S(1)}, f32[16,8,128]{2,1,0:T(8,128)S(1)}, f32[8,128]{1,0:T(8,128)S(1)}) custom-call(s32[16,64]{1,0:T(8,128)S(1)} %fusion.2.tb, bf16[64,64,512]{2,1,0:T(8,128)(2,1)} %bitcast.19, bf16[96,64,256]{2,1,0:T(8,128)(2,1)S(1)} %bitcast.14, bf16[96,64,256]{2,1,0:T(8,128)(2,1)} %bitcast.21, ...), custom_call_target="tpu_custom_call" | custom-call | tf_op jit(solution)/shard_map/pallas_call | solution.py:802
  96.3 17.3 %shard_map.159 = (bf16[2,64,64,256]{3,2,1,0:T(8,128)(2,1)}, bf16[96,64,256]{2,1,0:T(8,128)(2,1)S(1)}) custom-call(s32[16,64]{1,0:T(8,128)S(1)} %fusion.2.tb, bf16[64,64,512]{2,1,0:T(8,128)(2,1)} %bitcast.20, bf16[96,64,256]{2,1,0:T(8,128)(2,1)} %bitcast.13, bf16[96,64,256]{2,1,0:T(8,128)(2,1)} %bitcast.22, f32[16,8,128]{2,1,0:T(8,128)S(1)} %get-tuple-element.21.tl, ...), custom_call_target="tpu_custom_call" | custom-call | tf_op jit(solution)/shard_map/pallas_call | solution.py:811
  113.6 69.4 %shard_map.160 = (bf16[384,512]{1,0:T(8,128)(2,1)S(1)}, bf16[1024,512]{1,0:T(8,128)(2,1)S(1)}, f32[32,256]{1,0:T(8,128)S(1)}) custom-call(bf16[2,4,1024,256]{3,2,1,0:T(8,128)(2,1)} %bitcast.23, bf16[16,384,256]{2,1,0:T(8,128)(2,1)S(1)} %bitcast.15, bf16[1024,256]{1,0:T(8,128)(2,1)S(1)} %get-tuple-element.29.klow, bf16[1024,2048]{1,0:T(8,128)(2,1)} %bitcast.18, ...), custom_call_target="tpu_custom_call" | custom-call | tf_op jit(solution)/shard_map/pallas_call | solution.py:817
  183.1 0.7 copy.32
  183.8 1.0 copy.33
  184.8 0.6 copy.34
  (20 shorter events, 0.3 us)
Async XLA Ops:
  4.9 1.2 copy-start.1
  6.1 1.2 copy-start.2
  7.3 1.2 copy-start.3
  8.5 1.0 copy-start.4
  9.5 0.9 copy-start.5
  10.5 0.9 copy-start.6
  11.4 0.9 copy-start.7
  12.3 0.9 copy-start.8
  73.0 1.9 %copy-start = (bf16[16,384,256]{2,1,0:T(8,128)(2,1)S(1)}, bf16[16,384,256]{2,1,0:T(8,128)(2,1)}, u32[]{:S(2)}) copy-start(bf16[16,384,256]{2,1,0:T(8,128)(2,1)} %get-tuple-element.23) | copy-start | bytes 9437188

commit v3 on v2

--- a/solution.py
+++ b/solution.py
@@ -14,6 +14,7 @@
 NZ, NY, NX = 8, 4, 4
 VMEM = pltpu.VMEM
 F32, BF16 = jnp.float32, jnp.bfloat16
+LIMITS = (20, 6, 18, 24)
 
 NORM_FLOOR = 1.0
 SCORE_GAIN = 4.0
@@ -142,10 +143,11 @@
 
 
 def gather_kernel(
-    pas, wk, wv, tok, wq, gw, cot, tbl, mq, mk, mv, mx,
-    kv, qa, ca, tl, klow, qlow, gown, wall, gall, md,
+    pas_in, wk_in, wv_in, tok_in, wq_in, gw_in, cot_in, mq_in, mk_in, mv_in, ids_in, beta_in, pre_in, rate_in,
+    kv, qa, ca, tl, tb, klow, qlow, gown, wall, gall, md,
+    pas, wk, wv, wq, mq, mk, mv, gw_row, ids, beta, pre, rate, gw, mx,
     toks, relay, fresh, corr, att, qdec, kdec,
-    xs, xr, ys, yr, zs, zr, ps, pr, ts, tr, ws, wr, vs, vr, gs, gr,
+    ins, hs, hr, xs, xr, ys, yr, zs, zr, ps, pr, ts, tr, ws, wr, vs, vr, gs, gr,
 ):
     z, y, c, x = place()
     me = z * 2 + c
@@ -155,6 +157,24 @@
     partner = {"st_2": 1 - c}
     peers = column_peers(z, c)
     across = {"tp": wrap(x + 2, NX)}
+    reads = {}
+
+    def fetch(name, src, dst):
+        reads[name] = pltpu.make_async_copy(src, dst, ins.at[len(reads)])
+        reads[name].start()
+
+    fetch("tok", tok_in, toks.at[x])
+    fetch("cot", cot_in, ca.at[me])
+    fetch("wk", wk_in, wk)
+    fetch("wv", wv_in, wv)
+    for i in range(4):
+        fetch(f"pas{i}", pas_in.at[pl.ds(i * 256, 256), :], pas.at[pl.ds(i * 256, 256), :])
+    fetch("wq", wq_in, wq)
+    for name, src, dst in (
+        ("gw", gw_in, gw_row), ("ids", ids_in, ids), ("beta", beta_in, beta), ("pre", pre_in, pre),
+        ("rate", rate_in, rate), ("mq", mq_in, mq), ("mk", mk_in, mk), ("mv", mv_in, mv),
+    ):
+        fetch(name, src, dst)
     greet(peers + [east, west, front, back, across])
     copies = Copies()
     half = 192
@@ -209,12 +229,12 @@
                     piece = rows_of(ref, owner * 2 + theirs, h)
                     copies.arrived(piece, ps.at[k, to], pr.at[k, to], partner)
 
-    toks[x] = tok[...]
+    reads["tok"].wait()
     for way in (0, 1):
         for h in (0, 1):
             piece = rows_of(toks, x, h)
             copies.start(piece, piece, xs.at[way, h], xr.at[way, h], xdirs[way])
-    ca[me] = cot[...]
+    reads["cot"].wait()
     own_send(0, ca)
 
     rows = 256
@@ -222,7 +242,10 @@
     def kv_rows(i):
         return kv.at[y, pl.ds(i * rows, rows), :]
 
+    reads["wk"].wait()
+    reads["wv"].wait()
     for i in range(4):
+        reads[f"pas{i}"].wait()
         block = pas[pl.ds(i * rows, rows), :]
         low = jnp.dot(block, wk[...], preferred_element_type=F32).astype(BF16)
         wide = low.astype(F32)
@@ -318,6 +341,23 @@
         for step, peer in enumerate((front, across, back)):
             copies.arrived(gall.at[wrap(x - 1 - step, NX)], gs.at[step], gr.at[step], peer)
 
+    for name in ("wq", "gw", "ids", "beta", "pre", "rate", "mq", "mk", "mv"):
+        reads[name].wait()
+    gw[...] = jnp.broadcast_to(gw_row[...].astype(F32), (16, 2048)).astype(BF16)
+    lanes = lax.broadcasted_iota(jnp.int32, (1, 128), 1)
+    row = jnp.full((1, 128), -1, jnp.int32)
+    for b in range(6):
+        for p in range(4):
+            each = jnp.broadcast_to(ids[b : b + 1, p : p + 1], (1, 128))
+            row = jnp.where(lanes == each // 16, (b * 4 + p) * 16 + lax.rem(each, 16), row)
+    tb[me] = row
+    mx[...] = jnp.zeros((24, 128), F32)
+    for b in range(6):
+        for h in range(2):
+            mx[b : b + 1, h * 64 : h * 64 + 64] = beta[h : h + 1, b * 64 : b * 64 + 64]
+            mx[8 + b : 9 + b, h * 64 : h * 64 + 64] = pre[h : h + 1, b * 64 : b * 64 + 64]
+    for h in range(2):
+        mx[16:17, h * 64 : h * 64 + 64] = jnp.broadcast_to(rate[0:1, h : h + 1], (1, 64))
     total, ends, stacked = mixer_rows(mx[...])
     cols = columns_of(stacked)
     work = (fresh, corr, att, qdec, kdec)
@@ -350,9 +390,9 @@
     tl[me] = jnp.zeros((8, 128), F32)
     for b in range(6):
         tl[me, b : b + 1, 0:64] = gate[0:1, b * 64 : b * 64 + 64]
-    tl[me, 6:7, 0:64] = tbl[...]
     for step, peer in enumerate(peers):
         copies.start(tl.at[me], tl.at[me], ts.at[step], tr.at[step], peer)
+        copies.start(tb.at[me], tb.at[me], hs.at[step], hr.at[step], peer)
     gown[...] = tl[me]
     y_take(2)
     prepare(2)
@@ -371,7 +411,7 @@
     state = [jnp.zeros((128, 128), F32), jnp.zeros((128, 128), F32)]
     sums = jnp.zeros((128, 128), F32)
     for b in range(6):
-        state, sums = mixer_advance(b, state, cot, ends, *work, sums)
+        state, sums = mixer_advance(b, state, ca.at[me], ends, *work, sums)
     turned = jnp.transpose(sums)[0:8]
     md[...] = turned[:, 0:64] + turned[:, 64:128]
     z_take(1, qa, 4)
@@ -379,6 +419,7 @@
     for step in range(2 * NZ - 1):
         other = wrap(me - (step + 1), 2 * NZ)
         copies.arrived(tl.at[other], ts.at[step], tr.at[step], peers[step])
+        copies.arrived(tb.at[other], hs.at[step], hr.at[step], peers[step])
     partner_take(0, ca)
     partner_take(1, qa)
     y_last()
@@ -398,7 +439,7 @@
         tile = tl[r]
         stats = jnp.zeros((8, 128), F32)
         for yy in range(NY):
-            entry = tb[r, (z * NY + yy) * 2 + c]
+            entry = tb[r, 0, (z * NY + yy) * 2 + c]
             used = entry >= 0
             safe = jnp.maximum(entry, 0)
             b, loc = safe // 64, lax.rem(safe, 16)
@@ -449,7 +490,7 @@
     @pl.loop(0, 2 * NZ)
     def _(r):
         for yy in range(NY):
-            entry = tb[r, (z * NY + yy) * 2 + c]
+            entry = tb[r, 0, (z * NY + yy) * 2 + c]
 
             @pl.when(entry >= 0)
             def _():
@@ -746,8 +787,8 @@
     return pltpu.SemaphoreType.DMA(shape)
 
 
-def call(kernel, outs, scratch, collective, smem=0, limit=48, count=0, **extra):
-    in_specs = [pl.BlockSpec(memory_space=pltpu.SMEM)] * smem + [pl.BlockSpec(memory_space=VMEM)] * (count - smem)
+def call(kernel, outs, scratch, collective, smem=0, limit=48, count=0, space=VMEM, **extra):
+    in_specs = [pl.BlockSpec(memory_space=pltpu.SMEM)] * smem + [pl.BlockSpec(memory_space=space)] * (count - smem)
     params = dict(vmem_limit_bytes=limit * 2**20)
     if collective is not None:
         params.update(collective_id=collective, has_side_effects=True)
@@ -768,36 +809,28 @@
 ):
     pass_local, span_rows, model_width = passages.shape
     flat_rows = passages.reshape(pass_local * span_rows, model_width)
-    ids = passage_ids.reshape(24)
-    place_of = jnp.arange(24, dtype=jnp.int32) * 16 + ids % 16
-    wanted = (ids // 16)[:, None] == jnp.arange(64, dtype=jnp.int32)[None, :]
-    table = jnp.max(jnp.where(wanted, place_of[:, None], -1), axis=0).astype(F32)[None, :]
-    gate_rows = jnp.broadcast_to(gate_weight, (16, model_width))
-
-    def by_block(rows):
-        return jnp.pad(rows.reshape(2, 6, 64).transpose(1, 0, 2).reshape(6, 128), ((0, 2), (0, 0)))
-
-    rates = jnp.broadcast_to(jnp.repeat(decay_rate, 64)[None, :], (8, 128))
-    scalars = jnp.concatenate([by_block(beta_pre), by_block(decay_pre), rates], axis=0)
-    kv, qa, ca, tl, key_low, query_low, gown, wall, gall, md = call(
+    kv, qa, ca, tl, lookup, key_low, query_low, gown, wall, gall, md = call(
         gather_kernel,
         [
             shaped((NY, 1024, 512), BF16), shaped((16, 384, 256), BF16), shaped((16, 384, 256), BF16),
-            shaped((16, 8, 128), F32), shaped((1024, 256), BF16), shaped((384, 256), BF16), shaped((8, 128), F32),
+            shaped((16, 8, 128), F32), shaped((16, 1, 128), jnp.int32), shaped((1024, 256), BF16), shaped((384, 256), BF16), shaped((8, 128), F32),
             shaped((3, NX, 512, 256), BF16), shaped((NX, 16, 512), BF16), shaped((8, 64), F32),
         ],
         [
+            VMEM((1024, 2048), BF16), VMEM((2048, 256), BF16), VMEM((2048, 256), BF16), VMEM((2048, 256), BF16),
+            VMEM((384, 256), BF16), VMEM((384, 256), BF16), VMEM((384, 256), BF16), VMEM((1, 2048), BF16),
+            VMEM((6, 4), jnp.int32), VMEM((2, 384), F32), VMEM((2, 384), F32), VMEM((1, 2), F32),
+            VMEM((16, 2048), BF16), VMEM((24, 128), F32),
             VMEM((NX, 384, 512), BF16), VMEM((3, 256, 256), BF16), VMEM((6, 128, 128), F32),
             VMEM((6, 128, 128), BF16), VMEM((6, 128, 128), BF16), VMEM((6, 128, 128), BF16), VMEM((6, 128, 128), BF16),
-            dma(2, 3), dma(2, 3), dma(2, 6), dma(2, 6), dma(2, 2, 7), dma(2, 2, 7),
+            dma(17), dma(15), dma(15), dma(2, 3), dma(2, 3), dma(2, 6), dma(2, 6), dma(2, 2, 7), dma(2, 2, 7),
             dma(2, 16), dma(2, 16), dma(15), dma(15), dma(12), dma(12), dma(9), dma(9), dma(3), dma(3),
         ],
-        1, count=12,
-    )(
-        flat_rows, key_weight, value_weight, tokens, query_weight, gate_rows, cotangent, table,
-        mix_query, mix_key, mix_value, scalars,
-    )
-    lookup = tl[:, 6, 0:64].astype(jnp.int32)
+        1, count=14, limit=LIMITS[0], space=pltpu.HBM,
+    )(*[pltpu.with_memory_space_constraint(a, pltpu.HBM) for a in (
+        flat_rows, key_weight, value_weight, tokens, query_weight, gate_weight, cotangent,
+        mix_query, mix_key, mix_value, passage_ids, beta_pre, decay_pre, decay_rate[None, :],
+    )])
     kv_one, qa_one, ca_one = kv.reshape(64, 64, 512), qa.reshape(96, 64, 256), ca.reshape(96, 64, 256)
     eg, tot, own = call(
         score_kernel,
@@ -806,13 +839,13 @@
             VMEM((16, 8, 128), F32), VMEM((15, 8, 128), F32), VMEM((8, 128), F32),
             dma(15), dma(15), dma(15), dma(15),
         ],
-        2, smem=1, count=5,
+        2, smem=1, count=5, limit=LIMITS[1],
     )(lookup, kv_one, qa_one, ca_one, tl)
     kvg, qp = call(
         grads_kernel,
         [shaped((2, 64, 64, 256), BF16), shaped((96, 64, 256), BF16)],
         [VMEM((2, 64, 64, 256), F32), VMEM((96, 64, 256), F32)],
-        None, smem=1, count=7,
+        None, smem=1, count=7, limit=LIMITS[2],
     )(lookup, kv_one, qa_one, ca_one, tl, eg, tot)
     token_grad, passage_grad, key_weight_grad = call(
         finish_kernel,
@@ -826,7 +859,7 @@
             dma(3, 2, 4), dma(3, 2, 4), dma(2, 4), dma(2, 4), dma(8), dma(8), dma(4, 2, 3), dma(4, 2, 3),
             dma(2, 3), dma(2, 3), dma(3), dma(3), dma(8), dma(8), dma(2, 4), dma(2, 4), dma(7), dma(7),
         ],
-        3, count=10,
+        3, count=10, limit=LIMITS[3],
     )(
         kvg.reshape(2, NY, 1024, 256), qp.reshape(16, 384, 256), key_low, flat_rows, query_low,
         wall, gall, own, md, gown,

time: 186 us -> 154 us (0.83); the launches traced: 185 us -> 151 us
  Pallas kernels: 168 us -> 147 us
  local copies, waits for them, and re-layouts: 16 us -> 3.69 us
    unnamed x22 -> x6, local copies, waits for them, and re-layouts: 13.4 us -> 3.69 us
    pallas_call x1, Pallas kernels: 69.4 us -> 62.8 us  [body(): call(finish_kernel, [shaped((384, 512), BF16), shaped((1024, 512), BF16),...]
    pallas_call x1, Pallas kernels: 59.7 us -> 53.3 us  [body(): call(gather_kernel, [shaped((NY, 1024, 512), BF16), shaped((16, 384, 256)...]
    pallas_call x1, Pallas kernels: 17.3 us -> 11.6 us  [body(): call(grads_kernel, [shaped((2, 64, 64, 256), BF16), shaped((96, 64, 256),...]
    pallas_call x1, Pallas kernels: 21.4 us -> 19.1 us  [body(): call(score_kernel, [shaped((64, 64, 128), F32), shaped((16, 8, 128), F32)...]
where the time goes in v3:
time: 154 us; the launch traced here: 151 us
  Pallas kernels  147 us (95%)
  local copies, waits for them, and re-layouts  3.69 us (2%)
    pallas_call x1, Pallas kernels, body(): call(finish_kernel, [shaped((384, 512), BF16), shaped((1024, 512), BF16),...  62.8 us
    pallas_call x1, Pallas kernels, body(): call(gather_kernel, [shaped((NY, 1024, 512), BF16), shaped((16, 384, 256)...  53.3 us
    pallas_call x1, Pallas kernels, body(): call(score_kernel, [shaped((64, 64, 128), F32), shaped((16, 8, 128), F32)...  19.1 us
    pallas_call x1, Pallas kernels, body(): call(grads_kernel, [shaped((2, 64, 64, 256), BF16), shaped((96, 64, 256),...  11.6 us
    unnamed x6, local copies, waits for them, and re-layouts  3.69 us

profile of v3, /device:TPU:1, one launch (start us, length us, event | category | flops | bytes accessed | tf_op | source)
XLA Modules:
  0.0 151.0 jit_solution(12196370663822133783)
XLA Ops:
  0.6 1.4 copy.17.ids_in
  2.0 53.3 %shard_map.157 = (bf16[4,1024,512]{2,1,0:T(8,128)(2,1)S(1)}, bf16[16,384,256]{2,1,0:T(8,128)(2,1)S(1)}, bf16[16,384,256]{2,1,0:T(8,128)(2,1)S(1)}, f32[16,8,128]...) custom-call(bf16[1024,2048]{1,0:T(8,128)(2,1)} %bitcast.8, ...), custom_call_target="tpu_custom_call" | custom-call | tf_op jit(solution)/shard_map/pallas_call | solution.py:812
  55.2 19.1 %shard_map.158 = (f32[64,64,128]{2,1,0:T(8,128)S(1)}, f32[16,8,128]{2,1,0:T(8,128)S(1)}, f32[8,128]{1,0:T(8,128)S(1)}) custom-call(s32[16,1,128]{2,1,0:T(1,128)S(1)} %get-tuple-element.22.tb, bf16[64,64,512]{2,1,0:T(8,128)(2,1)S(1)} %bitcast.10, bf16[96,64,256]{2,1,0:T(8,128)(2,1)S(1)} %bitcast.12, bf16[96,64,256]{2,1,0:T(8,128)(2,1)S(1)} %bitcast.14, ...), custom_call_target="tpu_custom_call" | custom-call | tf_op jit(solution)/shard_map/pallas_call | solution.py:835
  74.3 0.0 copy-start
  74.3 11.6 %shard_map.159 = (bf16[2,64,64,256]{3,2,1,0:T(8,128)(2,1)S(1)}, bf16[96,64,256]{2,1,0:T(8,128)(2,1)S(1)}) custom-call(s32[16,1,128]{2,1,0:T(1,128)S(1)} %get-tuple-element.22.tb, bf16[64,64,512]{2,1,0:T(8,128)(2,1)S(1)} %bitcast.11, bf16[96,64,256]{2,1,0:T(8,128)(2,1)S(1)} %bitcast.13, bf16[96,64,256]{2,1,0:T(8,128)(2,1)S(1)} %bitcast.15, ...), custom_call_target="tpu_custom_call" | custom-call | tf_op jit(solution)/shard_map/pallas_call | solution.py:844
  85.9 0.0 copy-done
  85.9 62.8 %shard_map.160 = (bf16[384,512]{1,0:T(8,128)(2,1)S(1)}, bf16[1024,512]{1,0:T(8,128)(2,1)S(1)}, f32[32,256]{1,0:T(8,128)S(1)}) custom-call(bf16[2,4,1024,256]{3,2,1,0:T(8,128)(2,1)S(1)} %bitcast.16, bf16[16,384,256]{2,1,0:T(8,128)(2,1)S(1)} %bitcast.17, bf16[1024,256]{1,0:T(8,128)(2,1)S(1)} %get-tuple-element.31.klow, bf16[1024,2048]{1,0:T(8,128)(2,1)S(1)} %bitcast.9, ...), custom_call_target="tpu_custom_call" | custom-call | tf_op jit(solution)/shard_map/pallas_call | solution.py:850
  148.7 0.7 copy.21
  149.4 1.0 copy.22
  150.4 0.6 copy.23
Async XLA Ops:
  74.3 11.6 %copy-start = (bf16[16,64,2048]{2,1,0:T(8,128)(2,1)S(1)}, bf16[16,64,2048]{2,1,0:T(8,128)(2,1)}, u32[]{:S(2)}) copy-start(bf16[16,64,2048]{2,1,0:T(8,128)(2,1)} %param.22) | copy-start | bytes 12582916

commit v4 on v3

--- a/solution.py
+++ b/solution.py
@@ -14,7 +14,7 @@
 NZ, NY, NX = 8, 4, 4
 VMEM = pltpu.VMEM
 F32, BF16 = jnp.float32, jnp.bfloat16
-LIMITS = (20, 6, 18, 24)
+LIMITS = (22, 18, 24)
 
 NORM_FLOOR = 1.0
 SCORE_GAIN = 4.0
@@ -124,7 +124,7 @@
     kdec[b] = (keys * column(4)).astype(BF16)
 
 
-def mixer_advance(b, state, cot, ends, fresh, corr, att, qdec, kdec, sums):
+def mixer_advance(b, state, grads, ends, fresh, corr, att, qdec, kdec, sums):
     heads = [slice(0, 64), slice(64, 128)]
     new = jnp.concatenate(
         [fresh[b, h, :] - low_dot(corr[b, h, :], state[i]) for i, h in enumerate(heads)], axis=0
@@ -135,8 +135,7 @@
         jnp.exp(ends[i][b : b + 1, :]) * state[i] + low_dot(kdec[b, h, :], new[h], CONTRACT_FIRST)
         for i, h in enumerate(heads)
     ]
-    at = slice(b * SPAN, (b + 1) * SPAN)
-    grads = jnp.concatenate([cot[at, 0:128], cot[at, 128:256]], axis=0).astype(F32)
+    grads = jnp.concatenate([grads[:, 0:128], grads[:, 128:256]], axis=0).astype(F32)
     lane = lax.broadcasted_iota(jnp.int32, (128, 128), 1)
     sums = jnp.where(lane == b, jnp.sum(grads * out, axis=-1, keepdims=True), sums)
     return state, sums
@@ -144,7 +143,8 @@
 
 def gather_kernel(
     pas_in, wk_in, wv_in, tok_in, wq_in, gw_in, cot_in, mq_in, mk_in, mv_in, ids_in, beta_in, pre_in, rate_in,
-    kv, qa, ca, tl, tb, klow, qlow, gown, wall, gall, md,
+    kv, qa, ca, tl, tb, klow, qlow, gown, wall, gall, md, eg, tot, own,
+    tbs, sent, parts, total, ss, sr, bs, br,
     pas, wk, wv, wq, mq, mk, mv, gw_row, ids, beta, pre, rate, gw, mx,
     toks, relay, fresh, corr, att, qdec, kdec,
     ins, hs, hr, xs, xr, ys, yr, zs, zr, ps, pr, ts, tr, ws, wr, vs, vr, gs, gr,
@@ -164,7 +164,7 @@
         reads[name].start()
 
     fetch("tok", tok_in, toks.at[x])
-    fetch("cot", cot_in, ca.at[me])
+    fetch("cot", cot_in, ca.at[pl.ds(me * 6, 6)])
     fetch("wk", wk_in, wk)
     fetch("wv", wv_in, wv)
     for i in range(4):
@@ -180,8 +180,11 @@
     half = 192
     zdirs, ydirs, xdirs = (up, down), (east, west), (front, back)
 
+    def token_rows(slot, h):
+        return toks.at[slot, pl.ds(h * half, half), :]
+
     def rows_of(ref, slot, h):
-        return ref.at[slot, pl.ds(h * half, half), :]
+        return ref.at[pl.ds(slot * 6 + h * 3, 3)]
 
     def z_send(k, ref, d, h):
         for way in (0, 1):
@@ -230,17 +233,16 @@
                     copies.arrived(piece, ps.at[k, to], pr.at[k, to], partner)
 
     reads["tok"].wait()
-    for way in (0, 1):
-        for h in (0, 1):
-            piece = rows_of(toks, x, h)
-            copies.start(piece, piece, xs.at[way, h], xr.at[way, h], xdirs[way])
+    for way, h in ((0, 0), (1, 1), (0, 1), (1, 0)):
+        piece = token_rows(x, h)
+        copies.start(piece, piece, xs.at[way, h], xr.at[way, h], xdirs[way])
     reads["cot"].wait()
     own_send(0, ca)
 
     rows = 256
 
     def kv_rows(i):
-        return kv.at[y, pl.ds(i * rows, rows), :]
+        return kv.at[pl.ds(y * 16 + i * 4, 4)]
 
     reads["wk"].wait()
     reads["wv"].wait()
@@ -251,17 +253,16 @@
         wide = low.astype(F32)
         scale = lax.rsqrt(jnp.mean(wide * wide, axis=-1, keepdims=True) + NORM_FLOOR)
         klow[pl.ds(i * rows, rows), :] = low
-        kv[y, pl.ds(i * rows, rows), pl.ds(0, 256)] = (wide * scale).astype(BF16)
-        kv[y, pl.ds(i * rows, rows), pl.ds(256, 256)] = jnp.dot(
-            block, wv[...], preferred_element_type=F32
-        ).astype(BF16)
+        kv[pl.ds(y * 16 + i * 4, 4), :, 0:256] = (wide * scale).astype(BF16).reshape(4, 64, 256)
+        value = jnp.dot(block, wv[...], preferred_element_type=F32)
+        kv[pl.ds(y * 16 + i * 4, 4), :, 256:512] = value.astype(BF16).reshape(4, 64, 256)
         for way in (0, 1):
             copies.start(kv_rows(i), kv_rows(i), ys.at[way, i], yr.at[way, i], ydirs[way])
 
     def y_take(i):
         for way in (0, 1):
             owner = wrap(y - 1, NY) if way == 0 else wrap(y + 1, NY)
-            piece = kv.at[owner, pl.ds(i * rows, rows), :]
+            piece = kv.at[pl.ds(owner * 16 + i * 4, 4)]
             copies.arrived(piece, ys.at[way, i], yr.at[way, i], ydirs[way])
             if i % 2 == way:
                 at = 4 + i // 2
@@ -271,22 +272,22 @@
         owner = wrap(y + 2, NY)
         for i in range(4):
             way, at = i % 2, 4 + i // 2
-            piece = kv.at[owner, pl.ds(i * rows, rows), :]
+            piece = kv.at[pl.ds(owner * 16 + i * 4, 4)]
             copies.arrived(piece, ys.at[way, at], yr.at[way, at], ydirs[way])
 
-    def x_take():
+    def x_take(first):
         for way in (0, 1):
             owner = wrap(x - 1, NX) if way == 0 else wrap(x + 1, NX)
-            for h in (0, 1):
-                piece = rows_of(toks, owner, h)
-                copies.arrived(piece, xs.at[way, h], xr.at[way, h], xdirs[way])
-                if h == way:
-                    copies.start(piece, piece, xs.at[way, 2], xr.at[way, 2], xdirs[way])
+            h = way if first else 1 - way
+            piece = token_rows(owner, h)
+            copies.arrived(piece, xs.at[way, h], xr.at[way, h], xdirs[way])
+            if first:
+                copies.start(piece, piece, xs.at[way, 2], xr.at[way, 2], xdirs[way])
 
     def x_last():
         owner = wrap(x + 2, NX)
         for way in (0, 1):
-            piece = rows_of(toks, owner, way)
+            piece = token_rows(owner, way)
             copies.arrived(piece, xs.at[way, 2], xr.at[way, 2], xdirs[way])
 
     def project(owner):
@@ -348,9 +349,11 @@
     row = jnp.full((1, 128), -1, jnp.int32)
     for b in range(6):
         for p in range(4):
-            each = jnp.broadcast_to(ids[b : b + 1, p : p + 1], (1, 128))
+            each = jnp.broadcast_to(ids[p : p + 1, b : b + 1], (1, 128))
             row = jnp.where(lanes == each // 16, (b * 4 + p) * 16 + lax.rem(each, 16), row)
     tb[me] = row
+    for step, peer in enumerate(peers):
+        copies.start(tb.at[me], tb.at[me], hs.at[step], hr.at[step], peer)
     mx[...] = jnp.zeros((24, 128), F32)
     for b in range(6):
         for h in range(2):
@@ -358,25 +361,25 @@
             mx[8 + b : 9 + b, h * 64 : h * 64 + 64] = pre[h : h + 1, b * 64 : b * 64 + 64]
     for h in range(2):
         mx[16:17, h * 64 : h * 64 + 64] = jnp.broadcast_to(rate[0:1, h : h + 1], (1, 64))
-    total, ends, stacked = mixer_rows(mx[...])
+    decays, ends, stacked = mixer_rows(mx[...])
     cols = columns_of(stacked)
     work = (fresh, corr, att, qdec, kdec)
 
     def prepare(b):
-        mixer_prepare(b, mq, mk, mv, total, cols, *work)
+        mixer_prepare(b, mq, mk, mv, decays, cols, *work)
 
     z_take(0, ca, 1)
+    x_take(True)
+    w_send()
+    acc = project(x)
     prepare(0)
     y_take(0)
-    acc = project(x)
-    x_take()
-    w_send()
     z_take(0, ca, 2)
+    x_take(False)
     for owner in (wrap(x - 1, NX), wrap(x + 1, NX)):
         more = project(owner)
         acc = (acc[0] + more[0], acc[1] + more[1])
     prepare(1)
-    y_take(1)
     x_last()
     more = project(wrap(x + 2, NX))
     low = (acc[0] + more[0]).astype(BF16)
@@ -384,62 +387,57 @@
     wide = low.astype(F32)
     scale = lax.rsqrt(jnp.mean(wide * wide, axis=-1, keepdims=True) + NORM_FLOOR)
     qlow[...] = low
-    qa[me] = (wide * scale).astype(BF16)
+    qa[pl.ds(me * 6, 6)] = (wide * scale).astype(BF16).reshape(6, 64, 256)
     own_send(1, qa)
     z_take(0, ca, 3)
+    y_take(1)
     tl[me] = jnp.zeros((8, 128), F32)
     for b in range(6):
         tl[me, b : b + 1, 0:64] = gate[0:1, b * 64 : b * 64 + 64]
-    for step, peer in enumerate(peers):
-        copies.start(tl.at[me], tl.at[me], ts.at[step], tr.at[step], peer)
-        copies.start(tb.at[me], tb.at[me], hs.at[step], hr.at[step], peer)
     gown[...] = tl[me]
     y_take(2)
     prepare(2)
     z_take(1, qa, 1)
+    z_take(0, ca, 4)
+    prepare(3)
     w_forward()
-    prepare(3)
     y_take(3)
     z_take(1, qa, 2)
-    prepare(4)
+    for step, peer in enumerate(peers):
+        copies.start(tl.at[me], tl.at[me], ts.at[step], tr.at[step], peer)
     w_share(0, wrap(x - 1, NX), 0)
     w_share(1, wrap(x + 1, NX), 3)
-    z_take(0, ca, 4)
-    prepare(5)
+    prepare(4)
     z_take(1, qa, 3)
     w_share(2, wrap(x + 2, NX), 9)
+    prepare(5)
     state = [jnp.zeros((128, 128), F32), jnp.zeros((128, 128), F32)]
     sums = jnp.zeros((128, 128), F32)
     for b in range(6):
-        state, sums = mixer_advance(b, state, ca.at[me], ends, *work, sums)
+        state, sums = mixer_advance(b, state, ca[me * 6 + b], ends, *work, sums)
     turned = jnp.transpose(sums)[0:8]
     md[...] = turned[:, 0:64] + turned[:, 64:128]
+    w_last()
     z_take(1, qa, 4)
-    w_last()
     for step in range(2 * NZ - 1):
         other = wrap(me - (step + 1), 2 * NZ)
         copies.arrived(tl.at[other], ts.at[step], tr.at[step], peers[step])
         copies.arrived(tb.at[other], hs.at[step], hr.at[step], peers[step])
+    table = pltpu.make_async_copy(tb, tbs, ins.at[17])
+    table.start()
     partner_take(0, ca)
     partner_take(1, qa)
     y_last()
-    copies.finish()
-
-
-def score_kernel(tb, kv, qa, ca, tl, eg, tot, own, sent, parts, total, ss, sr, bs, br):
-    z, y, c, x = place()
-    me = z * 2 + c
-    peers = column_peers(z, c)
-    greet(peers)
-    copies = Copies()
+    table.wait()
+
     gain = SCORE_GAIN * 256 ** (-0.5)
     line = lax.broadcasted_iota(jnp.int32, (8, 128), 0)
 
-    def reader(r, carry):
+    def reader(r):
         tile = tl[r]
         stats = jnp.zeros((8, 128), F32)
         for yy in range(NY):
-            entry = tb[r, 0, (z * NY + yy) * 2 + c]
+            entry = tbs[r, 0, (z * NY + yy) * 2 + c]
             used = entry >= 0
             safe = jnp.maximum(entry, 0)
             b, loc = safe // 64, lax.rem(safe, 16)
@@ -460,12 +458,19 @@
             )
             stats = stats + jnp.where(here, row, 0.0)
         sent[r] = stats
+
+    def outward(i, carry):
+        near = (i + 1) // 2
+        step = NZ + near - 2 * near * lax.rem(i, 2) - 1
+        r = wrap(me + step + 1, 2 * NZ)
+        reader(r)
+        copies.make(
+            sent.at[r], parts.at[step], ss.at[step], sr.at[step], {"st_0": r // 2, "st_2": lax.rem(r, 2)}
+        ).start()
         return carry
 
-    lax.fori_loop(0, 2 * NZ, reader, 0)
-    for step, peer in enumerate(peers):
-        other = wrap(me + step + 1, 2 * NZ)
-        copies.start(sent.at[other], parts.at[step], ss.at[step], sr.at[step], peer)
+    lax.fori_loop(0, 2 * NZ - 1, outward, 0)
+    reader(me)
     whole = sent[me]
     for step in range(2 * NZ - 1):
         copies.arrived(parts.at[step], ss.at[step], sr.at[step], peers[step])
@@ -478,6 +483,7 @@
     for step in range(2 * NZ - 1):
         other = wrap(me - (step + 1), 2 * NZ)
         copies.arrived(tot.at[other], bs.at[step], br.at[step], peers[step])
+        copies.make(sent.at[0], parts.at[step], ss.at[step], sr.at[step], peers[step]).wait_send()
     copies.finish()
 
 
@@ -541,19 +547,17 @@
     copies = Copies()
     zdirs, ydirs, xdirs = (up, down), (east, west), (front, back)
 
-    for k in (4, 3, 5, 2, 6, 1, 7, 0):
-        there = wrap(z + k, NZ)
-        copies.start(qp.at[there * 2 + 1 - c], px.at[there], ps.at[k], pr.at[k], partner)
-
     far, beside = wrap(y + 2, NY), (wrap(y + 1, NY), wrap(y - 1, NY))
 
     def y_rows(j, part):
-        return j // 2, pl.ds((j % 2) * 512 + part * 256, 256)
-
-    def y_open(j):
+        return j // 4, pl.ds((j % 4) * 256 + part * 128, 128)
+
+    def y_far(j):
         for way in (0, 1):
             p, at = y_rows(j, way)
             copies.start(kvg.at[p, far, at, :], ybuf.at[way, j], ys.at[0, way, j], yr.at[0, way, j], ydirs[way])
+
+    def y_near(j):
         for way in (0, 1):
             p, at = y_rows(j, 1 - way)
             copies.start(
@@ -566,11 +570,13 @@
             copies.arrived(ybuf.at[way, j], ys.at[0, way, j], yr.at[0, way, j], ydirs[way])
             ybuf[way, j] = (kvg[p, beside[way], at, :].astype(F32) + ybuf[way, j].astype(F32)).astype(BF16)
             copies.start(ybuf.at[way, j], ysum.at[way, p, at, :], ys.at[2, way, j], yr.at[2, way, j], ydirs[way])
-        if j < 3:
-            y_open(j + 1)
+        if j + 1 < 8:
+            y_near(j + 1)
+        if j + 2 < 8:
+            y_far(j + 2)
 
     def x_pieces(j, h):
-        return j // 2, pl.ds((j % 2) * 512 + h * 256, 256)
+        return j // 4, pl.ds((j % 4) * 256 + h * 128, 128)
 
     def y_done(j):
         for way in (0, 1):
@@ -606,11 +612,11 @@
         for way in (0, 1):
             p, at = x_pieces(j, way)
             copies.arrived(xall.at[owner, p, at, :], xs.at[j, way, 2], xr.at[j, way, 2], xdirs[way])
-        p = j // 2
-
-        @pl.loop(0, 4)
+        p = j // 4
+
+        @pl.loop(0, 2)
         def _(i):
-            at = pl.ds(pl.multiple_of((j % 2) * 512 + i * 128, 128), 128)
+            at = pl.ds(pl.multiple_of((j % 4) * 256 + i * 128, 128), 128)
             term = lax.dot_general(xall[0, p, at, :], wall[p, 0], CONTRACT_LAST, preferred_element_type=F32)
             for h in range(1, NX):
                 term += lax.dot_general(xall[h, p, at, :], wall[p, h], CONTRACT_LAST, preferred_element_type=F32)
@@ -731,51 +737,72 @@
         for k in (0, 1):
             wgrad[:, k * 128 : k * 128 + 128] = wlast[k] + wlast[2 + k] + wlast[4 + k] + wlast[6 + k]
 
-    y_open(0)
+    y_far(0)
+    y_near(0)
+    y_far(1)
+    for k in (4, 3, 5, 2, 6, 1, 7, 0):
+        there = wrap(z + k, NZ)
+        copies.start(qp.at[there * 2 + 1 - c], px.at[there], ps.at[k], pr.at[k], partner)
     q_pair(4)
     q_step(4)
-    for k in (3, 5):
-        q_pair(k)
+    q_pair(3)
+    q_pair(5)
     y_add(0)
-    q_step(3)
     for k in (2, 6, 1, 7, 0):
         q_pair(k)
     gates()
+    y_add(1)
+    q_step(3)
     y_done(0)
+    y_add(2)
+    y_done(1)
     q_step(2)
-    y_add(1)
+    x_take(0)
+    y_add(3)
+    y_done(2)
+    x_take(1)
+    x_last(0)
+    y_add(4)
+    y_done(3)
     q_step(1)
-    x_take(0)
-    y_done(1)
     for k in (4, 3, 5):
         w_tile(k)
-    y_add(2)
-    q_done()
+    x_take(2)
+    x_last(1)
+    y_add(5)
+    y_done(4)
+    x_take(3)
     for k in (2, 6, 1, 7, 0):
         w_tile(k)
-    x_take(1)
-    y_done(2)
+    y_add(6)
+    q_done()
+    y_done(5)
     w_pair(4)
     w_step(4)
-    y_add(3)
-    x_last(0)
+    x_last(2)
+    y_add(7)
+    y_done(6)
+    x_take(4)
     w_pair(3)
     w_pair(5)
     w_step(3)
-    q_take()
+    y_done(7)
+    x_last(3)
+    x_take(5)
     for k in (2, 6, 1, 7, 0):
         w_pair(k)
     w_step(2)
-    x_take(2)
-    x_last(1)
-    y_done(3)
+    q_take()
+    x_last(4)
+    x_take(6)
     w_step(1)
+    x_last(5)
+    x_take(7)
+    w_done()
     q_last()
-    w_done()
-    x_take(3)
-    x_last(2)
+    x_last(6)
     w_last()
-    x_last(3)
+    x_last(7)
     copies.finish()
 
 
@@ -809,57 +836,50 @@
 ):
     pass_local, span_rows, model_width = passages.shape
     flat_rows = passages.reshape(pass_local * span_rows, model_width)
-    kv, qa, ca, tl, lookup, key_low, query_low, gown, wall, gall, md = call(
+    kv, qa, ca, tl, lookup, key_low, query_low, gown, wall, gall, md, eg, tot, own = call(
         gather_kernel,
         [
-            shaped((NY, 1024, 512), BF16), shaped((16, 384, 256), BF16), shaped((16, 384, 256), BF16),
+            shaped((64, 64, 512), BF16), shaped((96, 64, 256), BF16), shaped((96, 64, 256), BF16),
             shaped((16, 8, 128), F32), shaped((16, 1, 128), jnp.int32), shaped((1024, 256), BF16), shaped((384, 256), BF16), shaped((8, 128), F32),
             shaped((3, NX, 512, 256), BF16), shaped((NX, 16, 512), BF16), shaped((8, 64), F32),
+            shaped((64, 64, 128), F32), shaped((16, 8, 128), F32), shaped((8, 128), F32),
         ],
         [
+            pltpu.SMEM((16, 1, 128), jnp.int32), VMEM((16, 8, 128), F32), VMEM((15, 8, 128), F32), VMEM((8, 128), F32),
+            dma(15), dma(15), dma(15), dma(15),
             VMEM((1024, 2048), BF16), VMEM((2048, 256), BF16), VMEM((2048, 256), BF16), VMEM((2048, 256), BF16),
             VMEM((384, 256), BF16), VMEM((384, 256), BF16), VMEM((384, 256), BF16), VMEM((1, 2048), BF16),
-            VMEM((6, 4), jnp.int32), VMEM((2, 384), F32), VMEM((2, 384), F32), VMEM((1, 2), F32),
+            VMEM((4, 6), jnp.int32), VMEM((2, 384), F32), VMEM((2, 384), F32), VMEM((1, 2), F32),
             VMEM((16, 2048), BF16), VMEM((24, 128), F32),
             VMEM((NX, 384, 512), BF16), VMEM((3, 256, 256), BF16), VMEM((6, 128, 128), F32),
             VMEM((6, 128, 128), BF16), VMEM((6, 128, 128), BF16), VMEM((6, 128, 128), BF16), VMEM((6, 128, 128), BF16),
-            dma(17), dma(15), dma(15), dma(2, 3), dma(2, 3), dma(2, 6), dma(2, 6), dma(2, 2, 7), dma(2, 2, 7),
+            dma(18), dma(15), dma(15), dma(2, 3), dma(2, 3), dma(2, 6), dma(2, 6), dma(2, 2, 7), dma(2, 2, 7),
             dma(2, 16), dma(2, 16), dma(15), dma(15), dma(12), dma(12), dma(9), dma(9), dma(3), dma(3),
         ],
         1, count=14, limit=LIMITS[0], space=pltpu.HBM,
     )(*[pltpu.with_memory_space_constraint(a, pltpu.HBM) for a in (
-        flat_rows, key_weight, value_weight, tokens, query_weight, gate_weight, cotangent,
-        mix_query, mix_key, mix_value, passage_ids, beta_pre, decay_pre, decay_rate[None, :],
+        flat_rows, key_weight, value_weight, tokens, query_weight, gate_weight, cotangent.reshape(6, 64, 256),
+        mix_query, mix_key, mix_value, passage_ids.T, beta_pre, decay_pre, decay_rate[None, :],
     )])
-    kv_one, qa_one, ca_one = kv.reshape(64, 64, 512), qa.reshape(96, 64, 256), ca.reshape(96, 64, 256)
-    eg, tot, own = call(
-        score_kernel,
-        [shaped((64, 64, 128), F32), shaped((16, 8, 128), F32), shaped((8, 128), F32)],
-        [
-            VMEM((16, 8, 128), F32), VMEM((15, 8, 128), F32), VMEM((8, 128), F32),
-            dma(15), dma(15), dma(15), dma(15),
-        ],
-        2, smem=1, count=5, limit=LIMITS[1],
-    )(lookup, kv_one, qa_one, ca_one, tl)
     kvg, qp = call(
         grads_kernel,
         [shaped((2, 64, 64, 256), BF16), shaped((96, 64, 256), BF16)],
         [VMEM((2, 64, 64, 256), F32), VMEM((96, 64, 256), F32)],
-        None, smem=1, count=7, limit=LIMITS[2],
-    )(lookup, kv_one, qa_one, ca_one, tl, eg, tot)
+        None, smem=1, count=7, limit=LIMITS[1],
+    )(lookup, kv, qa, ca, tl, eg, tot)
     token_grad, passage_grad, key_weight_grad = call(
         finish_kernel,
         [shaped((384, 512), BF16), shaped((1024, 512), BF16), shaped((32, 256), F32)],
         [
-            VMEM((2, 4, 256, 256), BF16), VMEM((2, 2, 1024, 256), BF16), VMEM((NZ, 384, 256), BF16),
+            VMEM((2, 8, 128, 256), BF16), VMEM((2, 2, 1024, 256), BF16), VMEM((NZ, 384, 256), BF16),
             VMEM((NZ, 384, 256), BF16), VMEM((2, 4, 384, 256), BF16), VMEM((NX, 2, 1024, 256), BF16),
             VMEM((1024, 512), F32), VMEM((NX, 384, 256), BF16), VMEM((NX, 8, 128), F32),
             VMEM((NZ, 256, 128), F32), VMEM((NZ, 256, 128), F32), VMEM((NZ, 256, 128), BF16),
             VMEM((2, 4, 256, 128), BF16), VMEM((NZ, 256, 256), F32), VMEM((8, 32, 128), F32),
-            dma(3, 2, 4), dma(3, 2, 4), dma(2, 4), dma(2, 4), dma(8), dma(8), dma(4, 2, 3), dma(4, 2, 3),
+            dma(3, 2, 8), dma(3, 2, 8), dma(2, 4), dma(2, 4), dma(8), dma(8), dma(8, 2, 3), dma(8, 2, 3),
             dma(2, 3), dma(2, 3), dma(3), dma(3), dma(8), dma(8), dma(2, 4), dma(2, 4), dma(7), dma(7),
         ],
-        3, count=10, limit=LIMITS[3],
+        3, count=10, limit=LIMITS[2],
     )(
         kvg.reshape(2, NY, 1024, 256), qp.reshape(16, 384, 256), key_low, flat_rows, query_low,
         wall, gall, own, md, gown,

time: 154 us -> 142 us (0.922); the launches traced: 151 us -> 142 us
  Pallas kernels: 147 us -> 139 us
    pallas_call x2 -> x1, Pallas kernels: 72.3 us -> 64.9 us  [body(): call(gather_kernel, [shaped((64, 64, 512), BF16), shaped((96, 64, 256), B...]
    unnamed x6 -> x5, local copies, waits for them, and re-layouts: 3.69 us -> 2.34 us
where the time goes in v4:
time: 142 us
  Pallas kernels  139 us (98%)
  local copies, waits for them, and re-layouts  2.34 us (2%)
    pallas_call x1, Pallas kernels, body(): call(gather_kernel, [shaped((64, 64, 512), BF16), shaped((96, 64, 256), B...  64.9 us
    pallas_call x1, Pallas kernels, body(): call(finish_kernel, [shaped((384, 512), BF16), shaped((1024, 512), BF16),...  62.4 us
    pallas_call x1, Pallas kernels, body(): call(grads_kernel, [shaped((2, 64, 64, 256), BF16), shaped((96, 64, 256),...  11.2 us

profile of v4, /device:TPU:1, one launch (start us, length us, event | category | flops | bytes accessed | tf_op | source)
XLA Modules:
  0.0 141.6 jit_solution(15662644977084173986)
XLA Ops:
  0.6 64.9 %shard_map.157 = (bf16[64,64,512]{2,1,0:T(8,128)(2,1)S(1)}, bf16[96,64,256]{2,1,0:T(8,128)(2,1)S(1)}, bf16[96,64,256]{2,1,0:T(8,128)(2,1)S(1)}, f32[16,8,128]{2,...) custom-call(bf16[1024,2048]{1,0:T(8,128)(2,1)} %bitcast.7, ...), custom_call_target="tpu_custom_call" | custom-call | tf_op jit(solution)/shard_map/pallas_call | solution.py:839
  65.6 0.0 copy-start
  65.6 11.2 %shard_map.158 = (bf16[2,64,64,256]{3,2,1,0:T(8,128)(2,1)S(1)}, bf16[96,64,256]{2,1,0:T(8,128)(2,1)S(1)}) custom-call(s32[16,1,128]{2,1,0:T(1,128)S(1)} %get-tuple-element.22.tb, bf16[64,64,512]{2,1,0:T(8,128)(2,1)S(1)} %get-tuple-element.23.kv, bf16[96,64,256]{2,1,0:T(8,128)(2,1)S(1)} %get-tuple-element.24.qa, ...), custom_call_target="tpu_custom_call" | custom-call | tf_op jit(solution)/shard_map/pallas_call | solution.py:864
  76.8 0.0 copy-done
  76.8 62.4 %shard_map.159 = (bf16[384,512]{1,0:T(8,128)(2,1)S(1)}, bf16[1024,512]{1,0:T(8,128)(2,1)S(1)}, f32[32,256]{1,0:T(8,128)S(1)}) custom-call(bf16[2,4,1024,256]{3,2,1,0:T(8,128)(2,1)S(1)} %bitcast.9, bf16[16,384,256]{2,1,0:T(8,128)(2,1)S(1)} %bitcast.10, bf16[1024,256]{1,0:T(8,128)(2,1)S(1)} %get-tuple-element.31.klow, bf16[1024,2048]{1,0:T(8,128)(2,1)S(1)} %bitcast.8, ...), custom_call_target="tpu_custom_call" | custom-call | tf_op jit(solution)/shard_map/pallas_call | solution.py:870
  139.3 0.7 copy.20
  140.0 1.0 copy.21
  141.0 0.6 copy.22
Async XLA Ops:
  65.6 11.2 %copy-start = (bf16[16,64,2048]{2,1,0:T(8,128)(2,1)S(1)}, bf16[16,64,2048]{2,1,0:T(8,128)(2,1)}, u32[]{:S(2)}) copy-start(bf16[16,64,2048]{2,1,0:T(8,128)(2,1)} %param.22) | copy-start | bytes 12582916

commit v5 on v4

--- a/solution.py
+++ b/solution.py
@@ -14,7 +14,7 @@
 NZ, NY, NX = 8, 4, 4
 VMEM = pltpu.VMEM
 F32, BF16 = jnp.float32, jnp.bfloat16
-LIMITS = (22, 18, 24)
+LIMITS = (22, 6, 24)
 
 NORM_FLOOR = 1.0
 SCORE_GAIN = 4.0
@@ -487,50 +487,59 @@
     copies.finish()
 
 
-def grads_kernel(tb, kv, qa, ca, tl, eg, tot, kvg, qp, kacc, qacc):
+def grads_kernel(tb, kv, qa, ca, tl, eg, tot, kvg, qp, todo):
     z, c = lax.axis_index("st_0"), lax.axis_index("st_2")
     gain = SCORE_GAIN * 256 ** (-0.5)
-    kacc[...] = jnp.zeros(kacc.shape, F32)
-    qacc[...] = jnp.zeros(qacc.shape, F32)
-
-    @pl.loop(0, 2 * NZ)
-    def _(r):
-        for yy in range(NY):
-            entry = tb[r, 0, (z * NY + yy) * 2 + c]
-
-            @pl.when(entry >= 0)
-            def _():
-                b, loc = entry // 64, lax.rem(entry, 16)
-                row = tot[r, pl.ds(b, 1), :]
-                gate = tl[r, pl.ds(b, 1), 0:64]
-                norm = 1.0 / row[:, 0:64]
-                both = eg[r * NY + yy]
-                probs = both[:, 0:64] * norm
-                slope = (probs * (both[:, 64:128] - row[:, 64:128] * norm)).astype(BF16)
-                gated = (probs * gate).astype(BF16)
-                at, slot = r * 6 + b, yy * 16 + loc
-                key = gain * jnp.dot(slope, qa[at], preferred_element_type=F32)
-                value = jnp.dot(gated, ca[at], preferred_element_type=F32)
-                kacc[0, slot] += key.astype(BF16).astype(F32)
-                kacc[1, slot] += value.astype(BF16).astype(F32)
-                qacc[at] += gain * lax.dot_general(
-                    slope, kv[slot, :, 0:256], CONTRACT_FIRST, preferred_element_type=F32
-                )
-
-    @pl.loop(0, 64)
+
+    def entry_of(i):
+        return tb[i // NY, 0, (z * NY + lax.rem(i, NY)) * 2 + c]
+
+    def pick(i, count):
+        todo[count] = i
+        return count + (entry_of(i) >= 0).astype(jnp.int32)
+
+    count = lax.fori_loop(0, 64, pick, 0)
+    todo[count] = 0
+
+    @pl.loop(0, 32)
     def _(i):
-        kvg[0, i] = kacc[0, i].astype(BF16)
-        kvg[1, i] = kacc[1, i].astype(BF16)
-
-    @pl.loop(0, 96)
-    def _(i):
-        qp[i] = qacc[i].astype(BF16)
+        blank = jnp.zeros((2, 64, 256), BF16)
+        kvg[0, pl.ds(i * 2, 2)] = blank
+        kvg[1, pl.ds(i * 2, 2)] = blank
+        qp[pl.ds(i * 3, 3)] = jnp.zeros((3, 64, 256), BF16)
+
+    @pl.loop(0, (count + 1) // 2)
+    def _(pair):
+        terms = []
+        for u in range(2):
+            i = todo[pair * 2 + u]
+            live = (pair * 2 + u < count).astype(F32)
+            entry = jnp.maximum(entry_of(i), 0)
+            r, b = i // NY, entry // 64
+            at, slot = r * 6 + b, lax.rem(i, NY) * 16 + lax.rem(entry, 16)
+            row = tot[r, pl.ds(b, 1), :]
+            gate = tl[r, pl.ds(b, 1), 0:64]
+            norm = 1.0 / row[:, 0:64]
+            both = eg[i]
+            probs = both[:, 0:64] * (norm * live)
+            slope = (probs * (both[:, 64:128] - row[:, 64:128] * norm)).astype(BF16)
+            gated = (probs * gate).astype(BF16)
+            key = gain * jnp.dot(slope, qa[at], preferred_element_type=F32)
+            value = jnp.dot(gated, ca[at], preferred_element_type=F32)
+            query = gain * lax.dot_general(
+                slope, kv[slot, :, 0:256], CONTRACT_FIRST, preferred_element_type=F32
+            )
+            terms.append((at, slot, key, value, query))
+        for at, slot, key, value, query in terms:
+            kvg[0, slot] = (kvg[0, slot].astype(F32) + key).astype(BF16)
+            kvg[1, slot] = (kvg[1, slot].astype(F32) + value).astype(BF16)
+            qp[at] = (qp[at].astype(F32) + query).astype(BF16)
 
 
 def finish_kernel(
     kvg, qp, klow, pas, qlow, wall, gall, own, md, gown,
     tgrad, pgrad, wgrad,
-    ybuf, ysum, px, qs, zbuf, xall, pacc, xq, ggx, whalf, wget, wz, wbuf, wsum, wlast,
+    ybuf, ysum, px, qs, zbuf, xall, pacc, tacc, xq, ggx, whalf, wget, wz, wbuf, wsum, wlast,
     ys, yr, zs, zr, ps, pr, xs, xr, qxs, qxr, gs, gr, us, ur, vs, vr, ls, lr,
 ):
     z, y, c, x = place()
@@ -607,6 +616,20 @@
                 if h == way:
                     copies.start(piece, piece, xs.at[j, way, 2], xr.at[j, way, 2], xdirs[way])
 
+    def head_dot(rows, weight):
+        return lax.dot_general(rows, weight, CONTRACT_LAST, preferred_element_type=F32)
+
+    def x_near(j):
+        p = j // 4
+
+        @pl.loop(0, 2)
+        def _(i):
+            at = pl.ds(pl.multiple_of((j % 4) * 256 + i * 128, 128), 128)
+            term = head_dot(xall[x, p, at, :], wall[p, x])
+            for owner in (wrap(x - 1, NX), wrap(x + 1, NX)):
+                term += head_dot(xall[owner, p, at, :], wall[p, owner])
+            pacc[at, :] = term if p == 0 else pacc[at, :] + term
+
     def x_last(j):
         owner = wrap(x + 2, NX)
         for way in (0, 1):
@@ -617,13 +640,11 @@
         @pl.loop(0, 2)
         def _(i):
             at = pl.ds(pl.multiple_of((j % 4) * 256 + i * 128, 128), 128)
-            term = lax.dot_general(xall[0, p, at, :], wall[p, 0], CONTRACT_LAST, preferred_element_type=F32)
-            for h in range(1, NX):
-                term += lax.dot_general(xall[h, p, at, :], wall[p, h], CONTRACT_LAST, preferred_element_type=F32)
+            term = pacc[at, :] + head_dot(xall[owner, p, at, :], wall[p, owner])
             if p == 0:
                 pacc[at, :] = term
             else:
-                pgrad[at, :] = (pacc[at, :] + term).astype(BF16)
+                pgrad[at, :] = term.astype(BF16)
 
     def ring_step(d, value, slots, send, recv, half):
         for way in (0, 1):
@@ -687,6 +708,11 @@
         owner = wrap(x + 2, NX)
         for way in (0, 1):
             copies.arrived(xq.at[owner, pl.ds(way * 192, 192), :], qxs.at[way, 2], qxr.at[way, 2], xdirs[way])
+        for b in range(6):
+            at = pl.ds(b * 64, 64)
+            tgrad[at, :] = (tacc[at, :] + head_dot(xq[owner, at, :], wall[2, owner])).astype(BF16)
+
+    def q_near():
         for step, peer in enumerate((front, across, back)):
             copies.arrived(ggx.at[wrap(x - 1 - step, NX)], gs.at[step], gr.at[step], peer)
         blank = [jnp.zeros((4, 64), F32)]
@@ -699,9 +725,9 @@
             term = lax.dot_general(
                 rows, slope, CONTRACT_FIRST, preferred_element_type=F32, precision=lax.Precision.HIGHEST
             )
-            for h in range(NX):
-                term += lax.dot_general(xq[h, at, :], wall[2, h], CONTRACT_LAST, preferred_element_type=F32)
-            tgrad[at, :] = term.astype(BF16)
+            for owner in (x, wrap(x - 1, NX), wrap(x + 1, NX)):
+                term += head_dot(xq[owner, at, :], wall[2, owner])
+            tacc[at, :] = term
 
     keep = pl.ds(pl.multiple_of(c * 128, 128), 128)
     give = pl.ds(pl.multiple_of((1 - c) * 128, 128), 128)
@@ -761,16 +787,18 @@
     y_add(3)
     y_done(2)
     x_take(1)
-    x_last(0)
     y_add(4)
     y_done(3)
     q_step(1)
+    x_near(0)
+    x_last(0)
     for k in (4, 3, 5):
         w_tile(k)
     x_take(2)
-    x_last(1)
     y_add(5)
     y_done(4)
+    x_near(1)
+    x_last(1)
     x_take(3)
     for k in (2, 6, 1, 7, 0):
         w_tile(k)
@@ -779,7 +807,6 @@
     y_done(5)
     w_pair(4)
     w_step(4)
-    x_last(2)
     y_add(7)
     y_done(6)
     x_take(4)
@@ -787,21 +814,29 @@
     w_pair(5)
     w_step(3)
     y_done(7)
-    x_last(3)
+    x_near(2)
+    x_last(2)
+    q_take()
     x_take(5)
     for k in (2, 6, 1, 7, 0):
         w_pair(k)
     w_step(2)
-    q_take()
-    x_last(4)
+    x_near(3)
+    x_last(3)
+    x_near(4)
     x_take(6)
     w_step(1)
-    x_last(5)
+    q_near()
+    x_last(4)
+    x_near(5)
     x_take(7)
     w_done()
+    x_near(6)
+    x_near(7)
     q_last()
+    x_last(5)
+    w_last()
     x_last(6)
-    w_last()
     x_last(7)
     copies.finish()
 
@@ -864,7 +899,7 @@
     kvg, qp = call(
         grads_kernel,
         [shaped((2, 64, 64, 256), BF16), shaped((96, 64, 256), BF16)],
-        [VMEM((2, 64, 64, 256), F32), VMEM((96, 64, 256), F32)],
+        [pltpu.SMEM((66,), jnp.int32)],
         None, smem=1, count=7, limit=LIMITS[1],
     )(lookup, kv, qa, ca, tl, eg, tot)
     token_grad, passage_grad, key_weight_grad = call(
@@ -873,7 +908,7 @@
         [
             VMEM((2, 8, 128, 256), BF16), VMEM((2, 2, 1024, 256), BF16), VMEM((NZ, 384, 256), BF16),
             VMEM((NZ, 384, 256), BF16), VMEM((2, 4, 384, 256), BF16), VMEM((NX, 2, 1024, 256), BF16),
-            VMEM((1024, 512), F32), VMEM((NX, 384, 256), BF16), VMEM((NX, 8, 128), F32),
+            VMEM((1024, 512), F32), VMEM((384, 512), F32), VMEM((NX, 384, 256), BF16), VMEM((NX, 8, 128), F32),
             VMEM((NZ, 256, 128), F32), VMEM((NZ, 256, 128), F32), VMEM((NZ, 256, 128), BF16),
             VMEM((2, 4, 256, 128), BF16), VMEM((NZ, 256, 256), F32), VMEM((8, 32, 128), F32),
             dma(3, 2, 8), dma(3, 2, 8), dma(2, 4), dma(2, 4), dma(8), dma(8), dma(8, 2, 3), dma(8, 2, 3),

time: 142 us -> 134 us (0.944)
  Pallas kernels: 139 us -> 131 us
    pallas_call x1, Pallas kernels: 11.2 us -> 6.48 us  [body(): call(grads_kernel, [shaped((2, 64, 64, 256), BF16), shaped((96, 64, 256),...]
    pallas_call x1, Pallas kernels: 62.4 us -> 59.9 us  [body(): call(finish_kernel, [shaped((384, 512), BF16), shaped((1024, 512), BF16),...]
where the time goes in v5:
time: 134 us
  Pallas kernels  131 us (98%)
  local copies, waits for them, and re-layouts  2.34 us (2%)
    pallas_call x1, Pallas kernels, body(): call(gather_kernel, [shaped((64, 64, 512), BF16), shaped((96, 64, 256), B...  64.8 us
    pallas_call x1, Pallas kernels, body(): call(finish_kernel, [shaped((384, 512), BF16), shaped((1024, 512), BF16),...  59.9 us
    pallas_call x1, Pallas kernels, body(): call(grads_kernel, [shaped((2, 64, 64, 256), BF16), shaped((96, 64, 256),...  6.48 us

profile of v5, /device:TPU:1, one launch (start us, length us, event | category | flops | bytes accessed | tf_op | source)
XLA Modules:
  0.0 134.2 jit_solution(2846742850748432009)
XLA Ops:
  0.6 64.8 %shard_map.157 = (bf16[64,64,512]{2,1,0:T(8,128)(2,1)S(1)}, bf16[96,64,256]{2,1,0:T(8,128)(2,1)S(1)}, bf16[96,64,256]{2,1,0:T(8,128)(2,1)S(1)}, f32[16,8,128]{2,...) custom-call(bf16[1024,2048]{1,0:T(8,128)(2,1)} %bitcast.7, ...), custom_call_target="tpu_custom_call" | custom-call | tf_op jit(solution)/shard_map/pallas_call | solution.py:874
  65.4 0.0 copy-start
  65.4 6.5 %shard_map.158 = (bf16[2,64,64,256]{3,2,1,0:T(8,128)(2,1)S(1)}, bf16[96,64,256]{2,1,0:T(8,128)(2,1)S(1)}) custom-call(s32[16,1,128]{2,1,0:T(1,128)S(1)} %get-tuple-element.22.tb, bf16[64,64,512]{2,1,0:T(8,128)(2,1)S(1)} %get-tuple-element.23.kv, bf16[96,64,256]{2,1,0:T(8,128)(2,1)S(1)} %get-tuple-element.24.qa, ...), custom_call_target="tpu_custom_call" | custom-call | tf_op jit(solution)/shard_map/pallas_call | solution.py:899
  71.9 0.0 copy-done
  71.9 59.9 %shard_map.159 = (bf16[384,512]{1,0:T(8,128)(2,1)S(1)}, bf16[1024,512]{1,0:T(8,128)(2,1)S(1)}, f32[32,256]{1,0:T(8,128)S(1)}) custom-call(bf16[2,4,1024,256]{3,2,1,0:T(8,128)(2,1)S(1)} %bitcast.9, bf16[16,384,256]{2,1,0:T(8,128)(2,1)S(1)} %bitcast.10, bf16[1024,256]{1,0:T(8,128)(2,1)S(1)} %get-tuple-element.31.klow, bf16[1024,2048]{1,0:T(8,128)(2,1)S(1)} %bitcast.8, ...), custom_call_target="tpu_custom_call" | custom-call | tf_op jit(solution)/shard_map/pallas_call | solution.py:905
  131.8 0.7 copy.20
  132.6 1.0 copy.21
  133.5 0.6 copy.22
Async XLA Ops:
  65.4 6.5 %copy-start = (bf16[16,64,2048]{2,1,0:T(8,128)(2,1)S(1)}, bf16[16,64,2048]{2,1,0:T(8,128)(2,1)}, u32[]{:S(2)}) copy-start(bf16[16,64,2048]{2,1,0:T(8,128)(2,1)} %param.22) | copy-start | bytes 12582916

commit v6 on v5

--- a/solution.py
+++ b/solution.py
@@ -395,11 +395,11 @@
     for b in range(6):
         tl[me, b : b + 1, 0:64] = gate[0:1, b * 64 : b * 64 + 64]
     gown[...] = tl[me]
+    prepare(2)
+    prepare(3)
     y_take(2)
-    prepare(2)
     z_take(1, qa, 1)
     z_take(0, ca, 4)
-    prepare(3)
     w_forward()
     y_take(3)
     z_take(1, qa, 2)
@@ -498,7 +498,7 @@
         todo[count] = i
         return count + (entry_of(i) >= 0).astype(jnp.int32)
 
-    count = lax.fori_loop(0, 64, pick, 0)
+    count = lax.fori_loop(0, 64, pick, 0, unroll=8)
     todo[count] = 0
 
     @pl.loop(0, 32)
@@ -841,6 +841,15 @@
     copies.finish()
 
 
+def store_kernel(tgrad, pgrad, wgrad, tokens, rows, weights, sems):
+    pairs = ((pgrad, rows), (tgrad, tokens), (wgrad, weights))
+    copies = [pltpu.make_async_copy(src, dst, sems.at[i]) for i, (src, dst) in enumerate(pairs)]
+    for copy in copies:
+        copy.start()
+    for copy in copies:
+        copy.wait()
+
+
 def shaped(shape, dtype):
     return jax.ShapeDtypeStruct(shape, dtype)
 
@@ -849,7 +858,7 @@
     return pltpu.SemaphoreType.DMA(shape)
 
 
-def call(kernel, outs, scratch, collective, smem=0, limit=48, count=0, space=VMEM, **extra):
+def call(kernel, outs, scratch, collective, smem=0, limit=48, count=0, space=VMEM, out_space=VMEM, **extra):
     in_specs = [pl.BlockSpec(memory_space=pltpu.SMEM)] * smem + [pl.BlockSpec(memory_space=space)] * (count - smem)
     params = dict(vmem_limit_bytes=limit * 2**20)
     if collective is not None:
@@ -858,7 +867,7 @@
         kernel,
         out_shape=outs,
         in_specs=in_specs,
-        out_specs=[pl.BlockSpec(memory_space=VMEM)] * len(outs),
+        out_specs=[pl.BlockSpec(memory_space=out_space)] * len(outs),
         scratch_shapes=scratch,
         compiler_params=pltpu.CompilerParams(**params),
         **extra,
@@ -919,6 +928,12 @@
         kvg.reshape(2, NY, 1024, 256), qp.reshape(16, 384, 256), key_low, flat_rows, query_low,
         wall, gall, own, md, gown,
     )
+    token_grad, passage_grad, key_weight_grad = call(
+        store_kernel,
+        [shaped((384, 512), BF16), shaped((1024, 512), BF16), shaped((32, 256), F32)],
+        [dma(3)],
+        None, count=3, limit=4, out_space=pltpu.HBM,
+    )(token_grad, passage_grad, key_weight_grad)
     return (token_grad, passage_grad.reshape(pass_local, span_rows, 512), key_weight_grad)
 
 

time: 134 us -> 133 us (level)
  local copies, waits for them, and re-layouts: 2.34 us -> 0.01 us
    unnamed x5 -> x2, local copies, waits for them, and re-layouts: 2.34 us -> 0.01 us
where the time goes in v6:
time: 133 us
  Pallas kernels  132 us (99%)
    pallas_call x1, Pallas kernels, body(): call(gather_kernel, [shaped((64, 64, 512), BF16), shaped((96, 64, 256), B...  64.8 us
    pallas_call x1, Pallas kernels, body(): call(finish_kernel, [shaped((384, 512), BF16), shaped((1024, 512), BF16),...  60.4 us
    pallas_call x1, Pallas kernels, body(): call(grads_kernel, [shaped((2, 64, 64, 256), BF16), shaped((96, 64, 256),...  5.69 us

profile of v6, /device:TPU:1, one launch (start us, length us, event | category | flops | bytes accessed | tf_op | source)
XLA Modules:
  0.0 132.9 jit_solution(18224529290825288974)
XLA Ops:
  0.6 64.8 %shard_map.157 = (bf16[64,64,512]{2,1,0:T(8,128)(2,1)S(1)}, bf16[96,64,256]{2,1,0:T(8,128)(2,1)S(1)}, bf16[96,64,256]{2,1,0:T(8,128)(2,1)S(1)}, f32[16,8,128]{2,...) custom-call(bf16[1024,2048]{1,0:T(8,128)(2,1)} %bitcast.7, ...), custom_call_target="tpu_custom_call" | custom-call | tf_op jit(solution)/shard_map/pallas_call | solution.py:883
  65.4 0.0 copy-start
  65.4 5.7 %shard_map.158 = (bf16[2,64,64,256]{3,2,1,0:T(8,128)(2,1)S(1)}, bf16[96,64,256]{2,1,0:T(8,128)(2,1)S(1)}) custom-call(s32[16,1,128]{2,1,0:T(1,128)S(1)} %get-tuple-element.25.tb, bf16[64,64,512]{2,1,0:T(8,128)(2,1)S(1)} %get-tuple-element.26.kv, bf16[96,64,256]{2,1,0:T(8,128)(2,1)S(1)} %get-tuple-element.27.qa, ...), custom_call_target="tpu_custom_call" | custom-call | tf_op jit(solution)/shard_map/pallas_call | solution.py:908
  71.1 0.0 copy-done
  71.1 60.4 %shard_map.159 = (bf16[384,512]{1,0:T(8,128)(2,1)S(1)}, bf16[1024,512]{1,0:T(8,128)(2,1)S(1)}, f32[32,256]{1,0:T(8,128)S(1)}) custom-call(bf16[2,4,1024,256]{3,2,1,0:T(8,128)(2,1)S(1)} %bitcast.9, bf16[16,384,256]{2,1,0:T(8,128)(2,1)S(1)} %bitcast.10, bf16[1024,256]{1,0:T(8,128)(2,1)S(1)} %get-tuple-element.34.klow, bf16[1024,2048]{1,0:T(8,128)(2,1)S(1)} %bitcast.8, ...), custom_call_target="tpu_custom_call" | custom-call | tf_op jit(solution)/shard_map/pallas_call | solution.py:914
  131.6 1.1 shard_map.160
Async XLA Ops:
  65.4 5.7 %copy-start = (bf16[16,64,2048]{2,1,0:T(8,128)(2,1)S(1)}, bf16[16,64,2048]{2,1,0:T(8,128)(2,1)}, u32[]{:S(2)}) copy-start(bf16[16,64,2048]{2,1,0:T(8,128)(2,1)} %param.22) | copy-start | bytes 12582916

commit v7 on v6

--- a/solution.py
+++ b/solution.py
@@ -52,10 +52,12 @@
             copy.wait_send()
 
 
-def greet(peers):
+def greet(peers, meanwhile=None):
     barrier = pltpu.get_barrier_semaphore()
     for peer in peers:
         pl.semaphore_signal(barrier, inc=1, device_id=peer, device_id_type=MESH)
+    if meanwhile is not None:
+        meanwhile()
     pl.semaphore_wait(barrier, len(peers))
 
 
@@ -175,7 +177,23 @@
         ("rate", rate_in, rate), ("mq", mq_in, mq), ("mk", mk_in, mk), ("mv", mv_in, mv),
     ):
         fetch(name, src, dst)
-    greet(peers + [east, west, front, back, across])
+    rows = 256
+
+    def project_passages():
+        reads["wk"].wait()
+        reads["wv"].wait()
+        for i in range(4):
+            reads[f"pas{i}"].wait()
+            block = pas[pl.ds(i * rows, rows), :]
+            low = jnp.dot(block, wk[...], preferred_element_type=F32).astype(BF16)
+            wide = low.astype(F32)
+            scale = lax.rsqrt(jnp.mean(wide * wide, axis=-1, keepdims=True) + NORM_FLOOR)
+            klow[pl.ds(i * rows, rows), :] = low
+            kv[pl.ds(y * 16 + i * 4, 4), :, 0:256] = (wide * scale).astype(BF16).reshape(4, 64, 256)
+            value = jnp.dot(block, wv[...], preferred_element_type=F32)
+            kv[pl.ds(y * 16 + i * 4, 4), :, 256:512] = value.astype(BF16).reshape(4, 64, 256)
+
+    greet(peers + [east, west, front, back, across], project_passages)
     copies = Copies()
     half = 192
     zdirs, ydirs, xdirs = (up, down), (east, west), (front, back)
@@ -239,23 +257,10 @@
     reads["cot"].wait()
     own_send(0, ca)
 
-    rows = 256
-
     def kv_rows(i):
         return kv.at[pl.ds(y * 16 + i * 4, 4)]
 
-    reads["wk"].wait()
-    reads["wv"].wait()
     for i in range(4):
-        reads[f"pas{i}"].wait()
-        block = pas[pl.ds(i * rows, rows), :]
-        low = jnp.dot(block, wk[...], preferred_element_type=F32).astype(BF16)
-        wide = low.astype(F32)
-        scale = lax.rsqrt(jnp.mean(wide * wide, axis=-1, keepdims=True) + NORM_FLOOR)
-        klow[pl.ds(i * rows, rows), :] = low
-        kv[pl.ds(y * 16 + i * 4, 4), :, 0:256] = (wide * scale).astype(BF16).reshape(4, 64, 256)
-        value = jnp.dot(block, wv[...], preferred_element_type=F32)
-        kv[pl.ds(y * 16 + i * 4, 4), :, 256:512] = value.astype(BF16).reshape(4, 64, 256)
         for way in (0, 1):
             copies.start(kv_rows(i), kv_rows(i), ys.at[way, i], yr.at[way, i], ydirs[way])
 

time: 133 us -> 134 us (level)
  no operation moved by 1% of the time
where the time goes in v7:
time: 134 us; the launch traced here: 133 us
  Pallas kernels  132 us (99%)
    pallas_call x1, Pallas kernels, body(): call(gather_kernel, [shaped((64, 64, 512), BF16), shaped((96, 64, 256), B...  65.1 us
    pallas_call x1, Pallas kernels, body(): call(finish_kernel, [shaped((384, 512), BF16), shaped((1024, 512), BF16),...  59.4 us
    pallas_call x1, Pallas kernels, body(): call(grads_kernel, [shaped((2, 64, 64, 256), BF16), shaped((96, 64, 256),...  6.8 us

profile of v7, /device:TPU:1, one launch (start us, length us, event | category | flops | bytes accessed | tf_op | source)
XLA Modules:
  0.0 133.2 jit_solution(3161920337404722482)
XLA Ops:
  0.6 65.1 %shard_map.157 = (bf16[64,64,512]{2,1,0:T(8,128)(2,1)S(1)}, bf16[96,64,256]{2,1,0:T(8,128)(2,1)S(1)}, bf16[96,64,256]{2,1,0:T(8,128)(2,1)S(1)}, f32[16,8,128]{2,...) custom-call(bf16[1024,2048]{1,0:T(8,128)(2,1)} %bitcast.7, ...), custom_call_target="tpu_custom_call" | custom-call | tf_op jit(solution)/shard_map/pallas_call | solution.py:888
  65.7 0.0 copy-start
  65.7 6.8 %shard_map.158 = (bf16[2,64,64,256]{3,2,1,0:T(8,128)(2,1)S(1)}, bf16[96,64,256]{2,1,0:T(8,128)(2,1)S(1)}) custom-call(s32[16,1,128]{2,1,0:T(1,128)S(1)} %get-tuple-element.25.tb, bf16[64,64,512]{2,1,0:T(8,128)(2,1)S(1)} %get-tuple-element.26.kv, bf16[96,64,256]{2,1,0:T(8,128)(2,1)S(1)} %get-tuple-element.27.qa, ...), custom_call_target="tpu_custom_call" | custom-call | tf_op jit(solution)/shard_map/pallas_call | solution.py:913
  72.5 0.0 copy-done
  72.5 59.4 %shard_map.159 = (bf16[384,512]{1,0:T(8,128)(2,1)S(1)}, bf16[1024,512]{1,0:T(8,128)(2,1)S(1)}, f32[32,256]{1,0:T(8,128)S(1)}) custom-call(bf16[2,4,1024,256]{3,2,1,0:T(8,128)(2,1)S(1)} %bitcast.9, bf16[16,384,256]{2,1,0:T(8,128)(2,1)S(1)} %bitcast.10, bf16[1024,256]{1,0:T(8,128)(2,1)S(1)} %get-tuple-element.34.klow, bf16[1024,2048]{1,0:T(8,128)(2,1)S(1)} %bitcast.8, ...), custom_call_target="tpu_custom_call" | custom-call | tf_op jit(solution)/shard_map/pallas_call | solution.py:919
  132.0 1.1 shard_map.160
Async XLA Ops:
  65.7 6.8 %copy-start = (bf16[16,64,2048]{2,1,0:T(8,128)(2,1)S(1)}, bf16[16,64,2048]{2,1,0:T(8,128)(2,1)}, u32[]{:S(2)}) copy-start(bf16[16,64,2048]{2,1,0:T(8,128)(2,1)} %param.22) | copy-start | bytes 12582916
